TPU v7x, 512 devices: a 8x2x16 block of a 8x16x16 slice. The times are simulated.
512 devices in a mesh: grp: 2 (over y), kv: 16 (over z), tp: 16 (over x, core).
Axes of the slice: x: 8, y: 2, z: 16, core: 2. Of those that a mesh axis runs over, the one named last changes fastest.
The devices are a block of a 8x16x16 slice.
Arguments:
- tokens: bfloat16 [256, 4096], P('grp', ('kv', 'tp')), parts along dimension 0, may hold values from -12 to 12
- gain_in: float32 [4096], P('kv'), may hold values from 0.1 to 1.9
- w_query: bfloat16 [4096, 1024], P('kv', 'tp'), may hold values from -0.09375 to 0.09375
- w_key: bfloat16 [4096, 1024], P('kv', 'tp'), may hold values from -0.09375 to 0.09375
- w_value: bfloat16 [4096, 2048], P('kv', 'tp'), may hold values from -0.09375 to 0.09375
- w_outgate: bfloat16 [4096, 2048], P('kv', 'tp'), may hold values from -0.09375 to 0.09375
- w_input_gate: bfloat16 [4096, 16], P('kv'), may hold values from -0.09375 to 0.09375
- w_forget_gate: bfloat16 [4096, 16], P('kv'), may hold values from -0.09375 to 0.09375
- bias_input: float32 [16], replicated, may hold values from -1 to 1
- bias_forget: float32 [16], replicated, may hold values from -1 to 4
- cell_state: float32 [256, 16, 64, 128], P(('grp', 'kv'), 'tp'), parts along dimension 0, may hold values from -6 to 6
- norm_state: float32 [256, 16, 64], P(('grp', 'kv'), 'tp'), parts along dimension 0, may hold values from -18 to 18
- max_state: float32 [256, 16], P(('grp', 'kv'), 'tp'), parts along dimension 0, may hold values from -1 to 2
- w_proj: bfloat16 [2048, 4096], P('tp', 'kv'), may hold values from -0.125 to 0.125
- gain_mid: float32 [4096], P('kv'), may hold values from 0.1 to 1.9
- w_up: bfloat16 [4096, 16384], P('kv', 'tp'), may hold values from -0.09375 to 0.09375
- w_down: bfloat16 [16384, 4096], P('tp', 'kv'), may hold values from -0.046875 to 0.046875
Outputs:
- mixed: bfloat16 [256, 4096], P('grp', ('kv', 'tp')), parts along dimension 0
- cell_new: float32 [256, 16, 64, 128], P(('grp', 'kv'), 'tp'), parts along dimension 0
- norm_new: float32 [256, 16, 64], P(('grp', 'kv'), 'tp'), parts along dimension 0
- max_new: float32 [256, 16], P(('grp', 'kv'), 'tp'), parts along dimension 0
There are 2 independent parts, one for each index of `grp`. A program takes and returns all parts, laid end to end along the dimension named above; an argument that names none is the same for every part. Nothing has to cross between parts.
All inputs are finite; a program needn't handle non-finite values.
Results may differ from a plain program's by a relative error of at most 0.015.
Values may be sent and summed in bfloat16 or wider, within the bound.
No kernel may reach another device: no remote copies, remote signals or barrier semaphores. Data moves between devices by JAX's collectives and lax.ppermute only.
A program may use at most 64 MiB of HBM per device.

v0:
```python
import math

import jax
import jax.numpy as jnp
from jax import lax
from jax.sharding import PartitionSpec as P

D = 4096


EPSILON = 1e-06


def cut_along(value, dim, peers):
    before, after = (value.shape[:dim], value.shape[dim + 1 :])
    return jnp.moveaxis(value.reshape(*before, peers, -1, *after), dim, 0)


def sum_at_owner(value, axis, dim):
    peers = lax.axis_size(axis)
    tiles = lax.all_to_all(cut_along(value, dim, peers), axis, 0, 0, tiled=True)
    return jnp.sum(tiles, axis=0)


def in_one_piece(arrays, axis, dim, along):
    columns = [a.reshape(*a.shape[:along], -1) for a in arrays]
    both = jnp.concatenate(columns, axis=along)
    whole, at, done = (sum_at_owner(both, axis, dim), 0, [])
    for a, column in zip(arrays, columns):
        piece = whole[..., at : at + column.shape[along]]
        done.append(piece.reshape(*piece.shape[:along], *a.shape[along:]))
        at += column.shape[along]
    return tuple(done)


def copy_for_each(value, axis):
    copies = jnp.broadcast_to(value, (lax.axis_size(axis), *value.shape))
    return lax.all_to_all(copies, axis, split_axis=0, concat_axis=0, tiled=True)


def in_order(tiles, dim):
    shape = list(tiles.shape[1:])
    shape[dim] *= tiles.shape[0]
    return jnp.moveaxis(tiles, 0, dim).reshape(shape)


def gathered_copies(value, axis, dim):
    tiles = copy_for_each(value, axis)
    return in_order(tiles, dim)


def over_copies(value, axis):
    everything = copy_for_each(value, axis)
    return jnp.sum(everything.astype(jnp.float32), axis=0)


def sum_at_owner_2(value, axis, dim):
    peers = lax.axis_size(axis)
    tiles = lax.all_to_all(cut_along(value, dim, peers), axis, 0, 0, tiled=True)
    return jnp.sum(tiles.astype(jnp.float32), axis=0)


def sent_together(arrays, axis, dim, along):
    widths = [math.prod(a.shape[along:]) for a in arrays]
    both = jnp.concatenate(
        [a.reshape(*a.shape[:along], w) for a, w in zip(arrays, widths)], axis=along
    )
    whole = sum_at_owner_2(both, axis, dim)
    tiles = jnp.split(whole, [sum(widths[:k]) for k in range(1, len(widths))], axis=along)
    return tuple((b.reshape(*whole.shape[:along], *a.shape[along:]) for a, b in zip(arrays, tiles)))


def memory_step(
    query, keys, values, outgate, log_input, log_forget, cell_state, norm_state, max_state
):
    max_new = jnp.maximum(log_forget + max_state, log_input)
    keep = jnp.exp(log_forget + max_state - max_new)
    write = jnp.exp(log_input - max_new)
    cell_new = (
        keep[..., None, None] * cell_state
        + (write[..., None] * keys)[..., :, None] * values[..., None, :]
    )
    norm_new = keep[..., None] * norm_state + write[..., None] * keys
    numer = jnp.einsum("shk,shkv->shv", query, cell_new, precision=lax.Precision.HIGHEST)
    denom = jnp.maximum(jnp.abs(jnp.sum(query * norm_new, axis=-1)), jnp.exp(-max_new))
    heads = (jax.nn.sigmoid(outgate) * numer / denom[..., None]).astype(jnp.bfloat16)
    return (heads, cell_new, norm_new, max_new)


def matmul(left, right):
    return jnp.dot(left, right, preferred_element_type=jnp.float32)


def on_device(
    tokens,
    gain_in,
    w_query,
    w_key,
    w_value,
    w_outgate,
    w_input_gate,
    w_forget_gate,
    bias_input,
    bias_forget,
    cell_state,
    norm_state,
    max_state,
    w_proj,
    gain_mid,
    w_up,
    w_down,
):
    seq_local, head_count = (cell_state.shape[0], cell_state.shape[1])
    key_dim, value_dim = (cell_state.shape[2], cell_state.shape[3])
    head_start = lax.axis_index("tp") * head_count
    column_width = tokens.shape[1]
    gathered = lax.all_gather(tokens, "tp", axis=1, tiled=True)
    widef = gathered.astype(jnp.float32)
    part_squares = jnp.sum(widef * widef, axis=1)
    normed = (widef * gain_in).astype(jnp.bfloat16)
    gate_input = lax.dynamic_slice_in_dim(w_input_gate, head_start, head_count, 1)
    gate_forget = lax.dynamic_slice_in_dim(w_forget_gate, head_start, head_count, 1)
    terms = jnp.concatenate(
        [
            matmul(normed, w_query),
            matmul(normed, w_key),
            matmul(normed, w_value),
            matmul(normed, w_outgate),
            matmul(normed, gate_input),
            matmul(normed, gate_forget),
        ],
        axis=1,
    )
    own_terms, row_squares = in_one_piece((terms, part_squares), "kv", 0, 1)
    own_terms = own_terms * lax.rsqrt(row_squares / D + EPSILON)[:, None]
    width_qk = head_count * key_dim
    width_v = head_count * value_dim
    query = own_terms[:, :width_qk].reshape(seq_local, head_count, key_dim) * key_dim ** (-0.5)
    keys = own_terms[:, width_qk : 2 * width_qk].reshape(seq_local, head_count, key_dim)
    offset = 2 * width_qk
    values = own_terms[:, offset : offset + width_v].reshape(seq_local, head_count, value_dim)
    offset = offset + width_v
    outgate = own_terms[:, offset : offset + width_v].reshape(seq_local, head_count, value_dim)
    offset = offset + width_v
    log_input = own_terms[:, offset : offset + head_count] + lax.dynamic_slice_in_dim(
        bias_input, head_start, head_count, 0
    )
    offset = offset + head_count
    log_forget = jax.nn.log_sigmoid(
        own_terms[:, offset : offset + head_count]
        + lax.dynamic_slice_in_dim(bias_forget, head_start, head_count, 0)
    )
    heads, cell_new, norm_new, max_new = memory_step(
        query, keys, values, outgate, log_input, log_forget, cell_state, norm_state, max_state
    )
    branch_part = matmul(gathered_copies(heads.reshape(seq_local, width_v), "kv", 0), w_proj)
    branch = over_copies(branch_part.astype(jnp.bfloat16), "tp").astype(jnp.float32)
    middle = (widef + branch).astype(jnp.bfloat16)
    midf = middle.astype(jnp.float32)
    mid_squares = jnp.sum(midf * midf, axis=1)
    normed_mid = (midf * gain_mid).astype(jnp.bfloat16)
    up_part = matmul(normed_mid, w_up)
    up_rows, square_rows = sent_together(
        (up_part.astype(jnp.bfloat16), mid_squares.astype(jnp.bfloat16)), "kv", 0, 1
    )
    upward = up_rows * lax.rsqrt(square_rows / D + EPSILON)[:, None]
    hidden = jnp.square(jax.nn.relu(upward)).astype(jnp.bfloat16)
    down_part = matmul(gathered_copies(hidden, "kv", 0), w_down)
    own_down = sum_at_owner_2(down_part.astype(jnp.bfloat16), "tp", 1)
    residual = lax.dynamic_slice_in_dim(midf, lax.axis_index("tp") * column_width, column_width, 1)
    mixed = (residual + own_down).astype(jnp.bfloat16)
    return (mixed, cell_new, norm_new, max_new)


def solution(mesh):
    in_specs = (
        P("grp", ("kv", "tp")),
        P("kv"),
        P("kv", "tp"),
        P("kv", "tp"),
        P("kv", "tp"),
        P("kv", "tp"),
        P("kv", None),
        P("kv", None),
        P(),
        P(),
        P(("grp", "kv"), "tp", None, None),
        P(("grp", "kv"), "tp", None),
        P(("grp", "kv"), "tp"),
        P("tp", "kv"),
        P("kv"),
        P("kv", "tp"),
        P("tp", "kv"),
    )
    out_specs = (
        P("grp", ("kv", "tp")),
        P(("grp", "kv"), "tp", None, None),
        P(("grp", "kv"), "tp", None),
        P(("grp", "kv"), "tp"),
    )
    return jax.shard_map(
        on_device, mesh=mesh, in_specs=in_specs, out_specs=out_specs, check_vma=False
    )
```

profile of v0, /device:TPU:65, one launch (start us, length us, event | category | flops | bytes accessed | tf_op | source)
XLA Modules:
  0.0 204.7 jit_solution(3389360989945205242)
XLA Ops:
  0.7 56.1 %all_gather.3 = bf16[128,256]{0,1:T(8,128)(2,1)S(1)} all-gather(bf16[128,16]{0,1:T(8,128)(2,1)} %param.17), channel_id=1, replica_groups=mesh['grp'=2,'kv'=16,'tp'=16] {'tp'}, dimensions={1}, use_global_device_ids=true | all-gather | bytes 69632 | tf_op jit(solution)/shard_map/all_gather | solution.py:117
  57.2 0.9 convolution_bitcast_fusion.4
  58.2 1.0 convolution_bitcast_fusion.3
  59.2 1.0 convolution_bitcast_fusion.2
  60.2 0.9 convolution_bitcast_fusion.1
  61.1 0.8 convolution_bitcast_fusion
  62.1 0.9 concatenate.25
  63.0 7.2 %all-to-all-start = ((f32[16,8,387]{2,1,0:T(8,128)}), f32[16,8,387]{2,1,0:T(8,128)S(1)}, u32[]{:S(2)}, u32[]{:S(2)}) async-start(f32[16,8,387]{2,1,0:T(8,128)} %concatenate.25), calls=%async_computation | async-start | bytes 524288 | tf_op jit(solution)/shard_map/all_to_all | solution.py:21
  70.2 0.6 dynamic_slice.17
  70.8 0.6 dynamic_slice.18
  71.5 12.7 %all-to-all-done = f32[16,8,387]{2,1,0:T(8,128)S(1)} async-done(((f32[16,8,387]{2,1,0:T(8,128)}), f32[16,8,387]{2,1,0:T(8,128)S(1)}, u32[]{:S(2)}, u32[]{:S(2)}) %all-to-all-start) | async-done | bytes 198176 | tf_op jit(solution)/shard_map/all_to_all | solution.py:21
  84.4 1.5 exponential_reduce_fusion.1
  86.0 0.8 fusion.35
  87.1 0.3 fusion.2
  87.5 21.4 %all_to_all.30 = bf16[16,8,128]{2,1,0:T(8,128)(2,1)S(1)} all-to-all(bf16[16,8,128]{2,1,0:T(8,128)(2,1)S(1)} %broadcast_in_dim.6), channel_id=1, replica_groups=mesh['grp'=2,'kv'=16,'tp'=16] {'kv'}, dimensions={0} | all-to-all | bytes 65536 | tf_op jit(solution)/shard_map/all_to_all | solution.py:38
  109.2 34.4 %all_to_all.31 = bf16[16,128,256]{2,1,0:T(8,128)(2,1)S(1)} all-to-all(bf16[16,128,256]{2,1,0:T(8,128)(2,1)S(1)} %broadcast_in_dim.7), channel_id=1, replica_groups=mesh['grp'=2,'kv'=16,'tp'=16] {'tp'}, dimensions={0} | all-to-all | bytes 2097152 | tf_op jit(solution)/shard_map/all_to_all | solution.py:38
  143.9 0.2 convert_element_type.73
  144.6 22.4 %all_to_all.32 = bf16[16,8,1025]{2,1,0:T(8,128)(2,1)S(1)} all-to-all(bf16[16,8,1025]{2,1,0:T(8,128)(2,1)S(1)} %pad_maximum_fusion), channel_id=1, replica_groups=mesh['grp'=2,'kv'=16,'tp'=16] {'kv'}, dimensions={0} | all-to-all | bytes 524800 | tf_op jit(solution)/shard_map/all_to_all | solution.py:59
  167.2 19.3 %all_to_all.33 = bf16[16,8,1024]{2,1,0:T(8,128)(2,1)S(1)} all-to-all(bf16[16,8,1024]{2,1,0:T(8,128)(2,1)S(1)} %broadcast_in_dim.8), channel_id=1, replica_groups=mesh['grp'=2,'kv'=16,'tp'=16] {'kv'}, dimensions={0} | all-to-all | bytes 524288 | tf_op jit(solution)/shard_map/all_to_all | solution.py:38
  186.7 0.7 copy.86
  187.5 8.5 %all-to-all-start.5 = ((bf16[16,128,16]{1,2,0:T(8,128)(2,1)}), bf16[16,128,16]{1,2,0:T(8,128)(2,1)S(1)}, u32[]{:S(2)}, u32[]{:S(2)}) async-start(bf16[16,128,16]{1,2,0:T(8,128)(2,1)} %bitcast.24), calls=%async_computation.5 | async-start | bytes 131072 | tf_op jit(solution)/shard_map/all_to_all | solution.py:59
  195.9 0.6 copy.90
  196.5 7.3 %all-to-all-done.5 = bf16[16,128,16]{1,2,0:T(8,128)(2,1)S(1)} async-done(((bf16[16,128,16]{1,2,0:T(8,128)(2,1)}), bf16[16,128,16]{1,2,0:T(8,128)(2,1)S(1)}, u32[]{:S(2)}, u32[]{:S(2)}) %all-to-all-start.5) | async-done | bytes 65568 | tf_op jit(solution)/shard_map/all_to_all | solution.py:59
  204.1 0.7 copy.88
  (54 shorter events, 3.0 us)
Async XLA Ops:
  0.6 143.5 %copy-start = (bf16[256,1024]{1,0:T(8,128)(2,1)S(1)}, bf16[256,1024]{1,0:T(8,128)(2,1)}, u32[]{:S(2)}) copy-start(bf16[256,1024]{1,0:T(8,128)(2,1)} %param.32) | copy-start | bytes 1572868
  0.6 61.3 %copy-start.5 = (f32[256]{0:T(256)S(1)}, f32[256]{0:T(256)}, u32[]{:S(2)}) copy-start(f32[256]{0:T(256)} %param.18) | copy-start | bytes 3076
  0.7 61.3 %copy-start.6 = (bf16[256,64]{0,1:T(8,128)(2,1)S(1)}, bf16[256,64]{0,1:T(8,128)(2,1)}, u32[]{:S(2)}) copy-start(bf16[256,64]{0,1:T(8,128)(2,1)} %param.19) | copy-start | bytes 98308
  58.1 12.1 %copy-start.10 = (f32[16]{0:T(128)S(1)}, f32[16]{0:T(128)}, u32[]{:S(2)}) copy-start(f32[16]{0:T(128)} %param.26) | copy-start | bytes 196
  58.1 12.7 %copy-start.11 = (f32[16]{0:T(128)S(1)}, f32[16]{0:T(128)}, u32[]{:S(2)}) copy-start(f32[16]{0:T(128)} %param.25) | copy-start | bytes 196
  58.2 13.2 %copy-start.9 = (f32[8,1]{0,1:T(1,128)S(1)}, f32[8,1]{0,1:T(1,128)}, u32[]{:S(2)}) copy-start(f32[8,1]{0,1:T(1,128)} %param.29) | copy-start | bytes 100
  60.2 25.8 %copy-start.7 = (f32[8,1,64]{2,1,0:T(1,128)S(1)}, f32[8,1,64]{2,1,0:T(1,128)}, u32[]{:S(2)}) copy-start(f32[8,1,64]{2,1,0:T(1,128)} %param.28) | copy-start | bytes 6148
  60.2 26.7 %copy-start.3 = (f32[8,1,64,128]{3,2,1,0:T(8,128)S(1)}, f32[8,1,64,128]{3,2,1,0:T(8,128)}, u32[]{:S(2)}) copy-start(f32[8,1,64,128]{3,2,1,0:T(8,128)} %param.27) | copy-start | bytes 786436
  63.0 46.0 %copy-start.4 = (bf16[128,256]{1,0:T(8,128)(2,1)S(1)}, bf16[128,256]{1,0:T(8,128)(2,1)}, u32[]{:S(2)}) copy-start(bf16[128,256]{1,0:T(8,128)(2,1)} %param.30) | copy-start | bytes 196612
  63.0 21.2 %all-to-all-start = ((f32[16,8,387]{2,1,0:T(8,128)}), f32[16,8,387]{2,1,0:T(8,128)S(1)}, u32[]{:S(2)}, u32[]{:S(2)}) async-start(f32[16,8,387]{2,1,0:T(8,128)} %concatenate.25), calls=%async_computation | async-start | bytes 524288 | tf_op jit(solution)/shard_map/all_to_all | solution.py:21
  87.1 56.5 %copy-start.1 = (f32[8,1,64,128]{3,2,1,0:T(8,128)}, f32[8,1,64,128]{3,2,1,0:T(8,128)S(1)}, u32[]{:S(2)}) copy-start(f32[8,1,64,128]{3,2,1,0:T(8,128)S(1)} %multiply_add_fusion) | copy-start | bytes 786436
  143.6 0.7 copy-start.8
  144.5 42.0 %copy-start.2 = (bf16[1024,256]{1,0:T(8,128)(2,1)S(1)}, bf16[1024,256]{1,0:T(8,128)(2,1)}, u32[]{:S(2)}) copy-start(bf16[1024,256]{1,0:T(8,128)(2,1)} %param.33) | copy-start | bytes 1572868
  187.5 16.4 %all-to-all-start.5 = ((bf16[16,128,16]{1,2,0:T(8,128)(2,1)}), bf16[16,128,16]{1,2,0:T(8,128)(2,1)S(1)}, u32[]{:S(2)}, u32[]{:S(2)}) async-start(bf16[16,128,16]{1,2,0:T(8,128)(2,1)} %bitcast.24), calls=%async_computation.5 | async-start | bytes 131072 | tf_op jit(solution)/shard_map/all_to_all | solution.py:59
where the time goes:
time: 205 us
  blocking collectives  154 us (75%)
  waiting for transfers between devices  20 us (10%)
  starting transfers between devices  15.7 us (8%)
  matrix products  5.7 us (3%)
  local copies, waits for them, and re-layouts  5.2 us (3%)
  other arithmetic  3.64 us (2%)
    all_to_all x3, blocking collectives, copy_for_each(): return lax.all_to_all(copies, axis, split_axis=0, concat_axis=0, tiled=True)  75.1 us
    all_gather x1, blocking collectives, on_device(): gathered = lax.all_gather(tokens, 'tp', axis=1, tiled=True)  56.1 us
    all_to_all x1, blocking collectives, sum_at_owner_2(): tiles = lax.all_to_all(cut_along(value, dim, peers), axis, 0, 0, tiled=True)  22.4 us
    all_to_all x1, waiting for transfers between devices, sum_at_owner(): tiles = lax.all_to_all(cut_along(value, dim, peers), axis, 0, 0, tiled=True)  12.7 us
    all_to_all x1, starting transfers between devices, sum_at_owner_2(): tiles = lax.all_to_all(cut_along(value, dim, peers), axis, 0, 0, tiled=True)  8.46 us
    all_to_all x1, waiting for transfers between devices, sum_at_owner_2(): tiles = lax.all_to_all(cut_along(value, dim, peers), axis, 0, 0, tiled=True)  7.33 us
    all_to_all x1, starting transfers between devices, sum_at_owner(): tiles = lax.all_to_all(cut_along(value, dim, peers), axis, 0, 0, tiled=True)  7.23 us
    dot_general x9, matrix products, matmul(): return jnp.dot(left, right, preferred_element_type=jnp.float32)  5.39 us
  transfers between devices with their start and end apart: 2, of which 2 were waited for; matrix products, arithmetic and copies ran while one was open for 1% of the time, Pallas kernels for 0%

commit v1 on v0

v1 whole, which is shorter than its diff:
```python
import jax
import jax.numpy as jnp
from jax import lax
from jax.sharding import PartitionSpec as P

EPSILON = 1e-06
LANES = 128


def exchange(tiles, axis):
    return lax.all_to_all(tiles, axis, split_axis=0, concat_axis=0, tiled=True)


def spread(value, axis):
    return exchange(jnp.broadcast_to(value, (lax.axis_size(axis), *value.shape)), axis)


def contract(left, right, left_dim, right_dim):
    dims = (((left_dim,), (right_dim,)), ((), ()))
    return lax.dot_general(left, right, dims, preferred_element_type=jnp.float32)


def two_parts(value):
    high = lax.reduce_precision(value, 8, 7)
    return high, lax.reduce_precision(value - high, 8, 7)


def on_device(
    tokens,
    gain_in,
    w_query,
    w_key,
    w_value,
    w_outgate,
    w_input_gate,
    w_forget_gate,
    bias_input,
    bias_forget,
    cell_state,
    norm_state,
    max_state,
    w_proj,
    gain_mid,
    w_up,
    w_down,
):
    seqs, own_columns = tokens.shape
    key_dim, value_dim = cell_state.shape[2:]
    tp, kv = lax.axis_size("tp"), lax.axis_size("kv")
    rows = gain_in.shape[0]
    width = rows * kv
    head = lax.axis_index("tp")
    own = seqs // kv
    main = 2 * key_dim + 2 * value_dim

    own_tokens = tokens.T
    wide = spread(own_tokens, "tp").reshape(rows, seqs).astype(jnp.float32)
    normed = (wide * gain_in[:, None]).astype(jnp.bfloat16)
    squares = jnp.sum(wide * wide, axis=0)

    gate_in = lax.dynamic_slice_in_dim(w_input_gate, head, 1, 1)
    gate_forget = lax.dynamic_slice_in_dim(w_forget_gate, head, 1, 1)
    blank = jnp.zeros((rows, 1), jnp.bfloat16)
    rest = jnp.zeros((rows, LANES - 6), jnp.bfloat16)
    weights = jnp.concatenate(
        [w_query, w_key, w_value, w_outgate]
        + [gate_in, gate_forget, blank, gate_in, gate_forget, blank, rest],
        axis=1,
    )
    terms = contract(normed, weights, 0, 0)
    lane = lax.broadcasted_iota(jnp.int32, (seqs, LANES), 1)
    extra = jnp.where((lane == 2) | (lane == 5), squares[:, None], terms[:, main:])
    high, low = two_parts(extra)
    terms = jnp.concatenate([terms[:, :main], jnp.where(lane < 3, high, low)], axis=1)
    terms = exchange(terms.astype(jnp.bfloat16).reshape(kv, own, -1), "kv")
    terms = jnp.sum(terms.astype(jnp.float32), axis=0)
    extra = terms[:, main : main + 3] + terms[:, main + 3 : main + 6]
    scale = lax.rsqrt(extra[:, 2:3] / width + EPSILON)
    query = terms[:, :key_dim] * (scale * key_dim ** (-0.5))
    keys = terms[:, key_dim : 2 * key_dim] * scale
    values = terms[:, 2 * key_dim : 2 * key_dim + value_dim] * scale
    outgate = terms[:, 2 * key_dim + value_dim : main] * scale

    cell, norm = cell_state[:, 0], norm_state[:, 0]
    log_input = extra[:, 0:1] * scale + lax.dynamic_slice_in_dim(bias_input, head, 1, 0)
    log_forget = jax.nn.log_sigmoid(
        extra[:, 1:2] * scale + lax.dynamic_slice_in_dim(bias_forget, head, 1, 0)
    )
    max_new = jnp.maximum(log_forget + max_state, log_input)
    keep = jnp.exp(log_forget + max_state - max_new)
    write = jnp.exp(log_input - max_new)
    written = write * keys
    norm_new = keep * norm + written
    cell_new = keep[..., None] * cell + written[:, :, None] * values[:, None, :]
    numer = jnp.sum(query[:, :, None] * cell_new, axis=1)
    denom = jnp.maximum(
        jnp.abs(jnp.sum(query * norm_new, axis=1, keepdims=True)), jnp.exp(-max_new)
    )
    heads = (jax.nn.sigmoid(outgate) * numer / denom).astype(jnp.bfloat16)

    heads = spread(heads, "kv").reshape(seqs, value_dim)
    branch = contract(w_proj, heads, 0, 1).astype(jnp.bfloat16)
    branch = exchange(branch.reshape(tp, own_columns, seqs), "tp")
    own_middle = own_tokens.astype(jnp.float32) + jnp.sum(branch.astype(jnp.float32), axis=0)
    own_middle = own_middle.astype(jnp.bfloat16)
    middle = spread(own_middle, "tp").reshape(rows, seqs).astype(jnp.float32)
    mid_squares = jnp.sum(middle * middle, axis=0)
    normed_mid = (middle * gain_mid[:, None]).astype(jnp.bfloat16)
    upward = contract(normed_mid, w_up, 0, 0)
    upward = jnp.concatenate([upward, mid_squares[:, None]], axis=1).astype(jnp.bfloat16)
    upward = exchange(upward.reshape(kv, own, -1), "kv")
    upward = jnp.sum(upward.astype(jnp.float32), axis=0)
    scale_mid = lax.rsqrt(upward[:, -1:] / width + EPSILON)
    hidden = jnp.square(jax.nn.relu(upward[:, :-1] * scale_mid)).astype(jnp.bfloat16)

    hidden = lax.all_gather(hidden, "kv", axis=0, tiled=True)
    down = contract(w_down, hidden, 0, 1).astype(jnp.bfloat16)
    down = exchange(down.reshape(tp, own_columns, seqs), "tp")
    mixed = own_middle.astype(jnp.float32) + jnp.sum(down.astype(jnp.float32), axis=0)
    mixed = mixed.astype(jnp.bfloat16).T
    return (mixed, cell_new[:, None], norm_new[:, None], max_new)


def solution(mesh):
    in_specs = (
        P("grp", ("kv", "tp")),
        P("kv"),
        P("kv", "tp"),
        P("kv", "tp"),
        P("kv", "tp"),
        P("kv", "tp"),
        P("kv", None),
        P("kv", None),
        P(),
        P(),
        P(("grp", "kv"), "tp", None, None),
        P(("grp", "kv"), "tp", None),
        P(("grp", "kv"), "tp"),
        P("tp", "kv"),
        P("kv"),
        P("kv", "tp"),
        P("tp", "kv"),
    )
    out_specs = (
        P("grp", ("kv", "tp")),
        P(("grp", "kv"), "tp", None, None),
        P(("grp", "kv"), "tp", None),
        P(("grp", "kv"), "tp"),
    )
    return jax.shard_map(
        on_device, mesh=mesh, in_specs=in_specs, out_specs=out_specs, check_vma=False
    )
```

time: 205 us -> 192 us (0.937)
  blocking collectives: 154 us -> 68.2 us
  starting transfers between devices: 15.7 us -> 69.7 us
  waiting for transfers between devices: 20 us -> 35.5 us
  matrix products: 5.7 us -> 0.81 us
  local copies, waits for them, and re-layouts: 5.2 us -> 9.63 us
  other arithmetic: 3.64 us -> 6.45 us
    all_to_all x4 -> x3, blocking collectives: 97.5 us -> 41.2 us  [exchange(): return lax.all_to_all(tiles, axis, split_axis=0, concat_axis=0, tiled=True)]
    all_to_all x2 -> x4, starting transfers between devices: 15.7 us -> 69.7 us  [exchange(): return lax.all_to_all(tiles, axis, split_axis=0, concat_axis=0, tiled=True)]
    all_gather x1, blocking collectives: 56.1 us -> 27.1 us  [on_device(): hidden = lax.all_gather(hidden, 'kv', axis=0, tiled=True)]
    all_to_all x2 -> x4, waiting for transfers between devices: 20 us -> 35.5 us  [exchange(): return lax.all_to_all(tiles, axis, split_axis=0, concat_axis=0, tiled=True)]
    dot_general x10 -> x4, matrix products: 5.7 us -> 0.81 us  [contract(): lax.dot_general(left, right, dims, preferred_element_type=jnp.float32)]
    unnamed x27 -> x34, local copies, waits for them, and re-layouts: 1.58 us -> 4.5 us
  transfers between devices with their start and end apart: 2 -> 4, of which waited for: 2 -> 4; matrix products, arithmetic and copies ran while one was open for 1% -> 2% of each run, Pallas kernels for 0% -> 0%
where the time goes in v1:
time: 192 us; the launch traced here: 191 us
  starting transfers between devices  69.7 us (36%)
  blocking collectives  68.2 us (36%)
  waiting for transfers between devices  35.5 us (18%)
  local copies, waits for them, and re-layouts  9.63 us (5%)
  other arithmetic  6.45 us (3%)
    all_to_all x4, starting transfers between devices, exchange(): return lax.all_to_all(tiles, axis, split_axis=0, concat_axis=0, tiled=True)  69.7 us
    all_to_all x3, blocking collectives, exchange(): return lax.all_to_all(tiles, axis, split_axis=0, concat_axis=0, tiled=True)  41.2 us
    all_to_all x4, waiting for transfers between devices, exchange(): return lax.all_to_all(tiles, axis, split_axis=0, concat_axis=0, tiled=True)  35.5 us
    all_gather x1, blocking collectives, on_device(): hidden = lax.all_gather(hidden, 'kv', axis=0, tiled=True)  27.1 us
    unnamed x34, local copies, waits for them, and re-layouts  4.5 us
  transfers between devices with their start and end apart: 4, of which 4 were waited for; matrix products, arithmetic and copies ran while one was open for 2% of the time, Pallas kernels for 0%

profile of v1, /device:TPU:65, one launch (start us, length us, event | category | flops | bytes accessed | tf_op | source)
XLA Modules:
  0.0 191.2 jit_solution(14461196263840126875)
XLA Ops:
  0.6 1.4 broadcast_in_dim.20
  2.0 44.7 %all-to-all-start = ((bf16[16,16,128]{2,1,0:T(8,128)(2,1)}), bf16[16,16,128]{2,1,0:T(8,128)(2,1)S(1)}, u32[]{:S(2)}, u32[]{:S(2)}) async-start(bf16[16,16,128]{2,1,0:T(8,128)(2,1)} %broadcast_in_dim.20), calls=%async_computation | async-start | bytes 131072 | tf_op jit(solution)/shard_map/all_to_all | solution.py:11
  46.8 0.7 constant_dynamic-slice_fusion
  48.5 0.6 copy-done.8
  49.3 0.8 copy-done.4
  50.4 4.3 %all-to-all-done = bf16[16,16,128]{2,1,0:T(8,128)(2,1)S(1)} async-done(((bf16[16,16,128]{2,1,0:T(8,128)(2,1)}), bf16[16,16,128]{2,1,0:T(8,128)(2,1)S(1)}, u32[]{:S(2)}, u32[]{:S(2)}) %all-to-all-start) | async-done | bytes 65568 | tf_op jit(solution)/shard_map/all_to_all | solution.py:11
  55.2 0.7 pad_maximum_fusion.1
  55.9 7.4 %all-to-all-start.1 = ((bf16[16,8,512]{2,1,0:T(8,128)(2,1)}), bf16[16,8,512]{2,1,0:T(8,128)(2,1)S(1)}, u32[]{:S(2)}, u32[]{:S(2)}) async-start(bf16[16,8,512]{2,1,0:T(8,128)(2,1)} %pad_maximum_fusion.1), calls=%async_computation.1 | async-start | bytes 262144 | tf_op jit(solution)/shard_map/all_to_all | solution.py:11
  64.7 10.5 %all-to-all-done.1 = bf16[16,8,512]{2,1,0:T(8,128)(2,1)S(1)} async-done(((bf16[16,8,512]{2,1,0:T(8,128)(2,1)}), bf16[16,8,512]{2,1,0:T(8,128)(2,1)S(1)}, u32[]{:S(2)}, u32[]{:S(2)}) %all-to-all-start.1) | async-done | bytes 131104 | tf_op jit(solution)/shard_map/all_to_all | solution.py:11
  75.3 1.5 multiply_reduce_fusion.3
  76.9 0.7 copy-done.9
  77.6 0.8 multiply_reduce_fusion.2
  78.9 17.8 %all_to_all.35 = bf16[16,8,128]{2,1,0:T(8,128)(2,1)S(1)} all-to-all(bf16[16,8,128]{2,1,0:T(8,128)(2,1)S(1)} %broadcast_in_dim.42), channel_id=1, replica_groups=mesh['grp'=2,'kv'=16,'tp'=16] {'kv'}, dimensions={0} | all-to-all | bytes 65536 | tf_op jit(solution)/shard_map/all_to_all | solution.py:11
  97.0 12.9 %all_to_all.36 = bf16[16,16,128]{2,1,0:T(8,128)(2,1)S(1)} all-to-all(bf16[16,16,128]{2,1,0:T(8,128)(2,1)S(1)} %bitcast.61), channel_id=1, replica_groups=mesh['grp'=2,'kv'=16,'tp'=16] {'tp'}, dimensions={0} | all-to-all | bytes 131072 | tf_op jit(solution)/shard_map/all_to_all | solution.py:11
  109.9 0.7 copy-done.6
  110.6 10.5 %all_to_all.37 = bf16[16,16,128]{2,1,0:T(8,128)(2,1)S(1)} all-to-all(bf16[16,16,128]{2,1,0:T(8,128)(2,1)S(1)} %broadcast_in_dim.43), channel_id=1, replica_groups=mesh['grp'=2,'kv'=16,'tp'=16] {'tp'}, dimensions={0} | all-to-all | bytes 131072 | tf_op jit(solution)/shard_map/all_to_all | solution.py:11
  121.8 0.7 pad_maximum_fusion
  122.6 4.1 %all-to-all-start.5 = ((bf16[16,8,1025]{2,1,0:T(8,128)(2,1)}), bf16[16,8,1025]{2,1,0:T(8,128)(2,1)S(1)}, u32[]{:S(2)}, u32[]{:S(2)}) async-start(bf16[16,8,1025]{2,1,0:T(8,128)(2,1)} %pad_maximum_fusion), calls=%async_computation.5 | async-start | bytes 589824 | tf_op jit(solution)/shard_map/all_to_all | solution.py:11
  127.3 13.7 %all-to-all-done.5 = bf16[16,8,1025]{2,1,0:T(8,128)(2,1)S(1)} async-done(((bf16[16,8,1025]{2,1,0:T(8,128)(2,1)}), bf16[16,8,1025]{2,1,0:T(8,128)(2,1)S(1)}, u32[]{:S(2)}, u32[]{:S(2)}) %all-to-all-start.5) | async-done | bytes 262432 | tf_op jit(solution)/shard_map/all_to_all | solution.py:11
  141.2 27.1 %all_gather.3 = bf16[128,1024]{1,0:T(8,128)(2,1)S(1)} all-gather(bf16[8,1024]{1,0:T(8,128)(2,1)S(1)} %fusion.15), channel_id=1, replica_groups=mesh['grp'=2,'kv'=16,'tp'=16] {'kv'}, dimensions={0}, use_global_device_ids=true | all-gather | bytes 278528 | tf_op jit(solution)/shard_map/all_gather | solution.py:116
  168.5 0.7 copy.112
  169.3 13.4 %all-to-all-start.6 = ((bf16[16,16,128]{2,1,0:T(8,128)(2,1)}), bf16[16,16,128]{2,1,0:T(8,128)(2,1)S(1)}, u32[]{:S(2)}, u32[]{:S(2)}) async-start(bf16[16,16,128]{2,1,0:T(8,128)(2,1)} %bitcast.18), calls=%async_computation.6 | async-start | bytes 131072 | tf_op jit(solution)/shard_map/all_to_all | solution.py:11
  182.7 0.8 multiply_add_fusion
  183.6 7.1 %all-to-all-done.6 = bf16[16,16,128]{2,1,0:T(8,128)(2,1)S(1)} async-done(((bf16[16,16,128]{2,1,0:T(8,128)(2,1)}), bf16[16,16,128]{2,1,0:T(8,128)(2,1)S(1)}, u32[]{:S(2)}, u32[]{:S(2)}) %all-to-all-start.6) | async-done | bytes 65568 | tf_op jit(solution)/shard_map/all_to_all | solution.py:11
  (68 shorter events, 6.7 us)
Async XLA Ops:
  0.6 120.9 %copy-start = (bf16[256,1024]{1,0:T(8,128)(2,1)S(1)}, bf16[256,1024]{1,0:T(8,128)(2,1)}, u32[]{:S(2)}) copy-start(bf16[256,1024]{1,0:T(8,128)(2,1)} %param.32) | copy-start | bytes 1572868
  2.0 52.7 %all-to-all-start = ((bf16[16,16,128]{2,1,0:T(8,128)(2,1)}), bf16[16,16,128]{2,1,0:T(8,128)(2,1)S(1)}, u32[]{:S(2)}, u32[]{:S(2)}) async-start(bf16[16,16,128]{2,1,0:T(8,128)(2,1)} %broadcast_in_dim.20), calls=%async_computation | async-start | bytes 131072 | tf_op jit(solution)/shard_map/all_to_all | solution.py:11
  47.6 0.8 copy-start.7
  48.4 0.8 copy-start.8
  49.3 0.8 copy-start.4
  49.3 0.9 copy-start.5
  50.4 4.3 %copy-start.10 = (f32[256]{0:T(256)S(1)}, f32[256]{0:T(256)}, u32[]{:S(2)}) copy-start(f32[256]{0:T(256)} %param.18) | copy-start | bytes 3076
  55.2 8.1 %copy-start.13 = (f32[16]{0:T(128)S(1)}, f32[16]{0:T(128)}, u32[]{:S(2)}) copy-start(f32[16]{0:T(128)} %param.26) | copy-start | bytes 196
  55.9 22.7 %copy-start.1 = (f32[8,1,64,128]{3,2,1,0:T(8,128)S(1)}, f32[8,1,64,128]{3,2,1,0:T(8,128)}, u32[]{:S(2)}) copy-start(f32[8,1,64,128]{3,2,1,0:T(8,128)} %param.27) | copy-start | bytes 786436
  55.9 19.3 %all-to-all-start.1 = ((bf16[16,8,512]{2,1,0:T(8,128)(2,1)}), bf16[16,8,512]{2,1,0:T(8,128)(2,1)S(1)}, u32[]{:S(2)}, u32[]{:S(2)}) async-start(bf16[16,8,512]{2,1,0:T(8,128)(2,1)} %pad_maximum_fusion.1), calls=%async_computation.1 | async-start | bytes 262144 | tf_op jit(solution)/shard_map/all_to_all | solution.py:11
  63.3 0.7 copy-start.14
  63.9 0.7 copy-start.12
  76.9 0.7 copy-start.9
  78.8 17.9 %copy-start.3 = (bf16[128,256]{1,0:T(8,128)(2,1)S(1)}, bf16[128,256]{1,0:T(8,128)(2,1)}, u32[]{:S(2)}) copy-start(bf16[128,256]{1,0:T(8,128)(2,1)} %param.30) | copy-start | bytes 196612
  109.9 0.7 copy-start.6
  110.6 10.5 %copy-start.11 = (f32[256]{0:T(256)S(1)}, f32[256]{0:T(256)}, u32[]{:S(2)}) copy-start(f32[256]{0:T(256)} %param.31) | copy-start | bytes 3076
  122.6 45.7 %copy-start.2 = (bf16[1024,256]{1,0:T(8,128)(2,1)S(1)}, bf16[1024,256]{1,0:T(8,128)(2,1)}, u32[]{:S(2)}) copy-start(bf16[1024,256]{1,0:T(8,128)(2,1)} %param.33) | copy-start | bytes 1572868
  122.6 18.4 %all-to-all-start.5 = ((bf16[16,8,1025]{2,1,0:T(8,128)(2,1)}), bf16[16,8,1025]{2,1,0:T(8,128)(2,1)S(1)}, u32[]{:S(2)}, u32[]{:S(2)}) async-start(bf16[16,8,1025]{2,1,0:T(8,128)(2,1)} %pad_maximum_fusion), calls=%async_computation.5 | async-start | bytes 589824 | tf_op jit(solution)/shard_map/all_to_all | solution.py:11
  169.3 21.4 %all-to-all-start.6 = ((bf16[16,16,128]{2,1,0:T(8,128)(2,1)}), bf16[16,16,128]{2,1,0:T(8,128)(2,1)S(1)}, u32[]{:S(2)}, u32[]{:S(2)}) async-start(bf16[16,16,128]{2,1,0:T(8,128)(2,1)} %bitcast.18), calls=%async_computation.6 | async-start | bytes 131072 | tf_op jit(solution)/shard_map/all_to_all | solution.py:11

commit v2 on v1

v2 whole, which is shorter than its diff:
```python
import functools

import jax
import jax.numpy as jnp
from jax import lax
from jax.experimental import pallas as pl
from jax.experimental.pallas import tpu as pltpu
from jax.sharding import PartitionSpec as P

EPSILON = 1e-06
LANES = 128


def exchange(tiles, axis):
    return lax.all_to_all(tiles, axis, split_axis=0, concat_axis=0, tiled=True)


def spread(value, axis):
    return exchange(jnp.broadcast_to(value, (lax.axis_size(axis), *value.shape)), axis)


def contract(left, right, left_dim, right_dim):
    dims = (((left_dim,), (right_dim,)), ((), ()))
    return lax.dot_general(left, right, dims, preferred_element_type=jnp.float32)


def two_parts(value):
    high = value.astype(jnp.bfloat16).astype(jnp.float32)
    return high, (value - high).astype(jnp.bfloat16).astype(jnp.float32)


def project_body(tokens, aux, wq, wk, wv, wo, wi, wf, out):
    gain, pick = aux[0:1], aux[1:2, : wi.shape[0]]
    wide = tokens[...].reshape(-1, tokens.shape[-1]).astype(jnp.float32).T
    squares = jnp.sum(wide * wide, axis=1, keepdims=True)
    normed = (wide * gain).astype(jnp.bfloat16)
    query = contract(normed, wq[...], 1, 1)
    keys = contract(normed, wk[...], 1, 1)
    values = contract(normed, wv[...], 1, 0)
    outgate = contract(normed, wo[...], 1, 0)
    gate_in = jnp.sum(contract(normed, wi[...], 1, 1) * pick, axis=1, keepdims=True)
    gate_forget = jnp.sum(contract(normed, wf[...], 1, 1) * pick, axis=1, keepdims=True)
    lane = lax.broadcasted_iota(jnp.int32, (wide.shape[0], LANES), 1)
    extra = jnp.zeros((wide.shape[0], LANES), jnp.float32)
    for place, value in enumerate((gate_in, gate_forget, squares)):
        high, low = two_parts(value)
        extra = jnp.where(lane == place, high, extra)
        extra = jnp.where(lane == place + 3, low, extra)
    both = jnp.concatenate([query, keys], axis=1)
    peers, own, _ = out.shape
    at = 0
    for piece in (both, values, outgate, extra):
        piece = piece.astype(jnp.bfloat16)
        for peer in range(peers):
            out[peer, :, at : at + LANES] = piece[peer * own : (peer + 1) * own]
        at += LANES


def memory_body(
    width, tiles, cell, aux,
    heads, cell_out, norm_out, top_out, cell_new, norm_buf, top_buf, sems,
):
    own, key_dim, value_dim = cell.shape
    terms = jnp.sum(tiles[...].astype(jnp.float32), axis=0)
    extra = terms[:, 3 * LANES :]
    extra = extra[:, 0:3] + extra[:, 3:6]
    scale = lax.rsqrt(extra[:, 2:3] / width + EPSILON)
    side = aux[...]
    norm, top = side[:, :key_dim], side[:, key_dim : key_dim + 1]
    log_input = extra[:, 0:1] * scale + side[:, key_dim + 1 : key_dim + 2]
    forget = extra[:, 1:2] * scale + side[:, key_dim + 2 : key_dim + 3]
    log_forget = jnp.minimum(forget, 0.0) - jnp.log1p(jnp.exp(-jnp.abs(forget)))
    log_keep = log_forget + top
    max_new = jnp.maximum(log_keep, log_input)
    keep = jnp.exp(log_keep - max_new)
    write = jnp.exp(log_input - max_new)
    top_buf[...] = jnp.broadcast_to(max_new, (own, LANES)).T[0:1]
    lane = lax.broadcasted_iota(jnp.int32, (own, LANES), 1)
    is_query = lane < key_dim
    both = terms[:, :LANES] * jnp.where(is_query, scale * key_dim ** (-0.5), scale * write)
    values = terms[:, LANES : 2 * LANES] * scale
    outgate = terms[:, 2 * LANES : 3 * LANES] * scale
    turned = jnp.concatenate([both] * (LANES // own), axis=0).T
    norm_new = keep * norm + both[:, key_dim:]
    norm_buf[...] = norm_new
    copies = [
        pltpu.make_async_copy(top_buf, top_out, sems.at[own]),
        pltpu.make_async_copy(norm_buf, norm_out, sems.at[own + 1]),
    ]
    for copy in copies:
        copy.start()
    rows = []
    for s in range(own):
        fresh = keep[s : s + 1] * cell[s] + turned[key_dim:, s : s + 1] * values[s : s + 1]
        cell_new[s] = fresh
        copies.append(pltpu.make_async_copy(cell_new.at[s], cell_out.at[s], sems.at[s]))
        copies[-1].start()
        rows.append(jnp.sum(turned[:key_dim, s : s + 1] * fresh, axis=0, keepdims=True))
    numer = jnp.concatenate(rows, axis=0)
    dot = jnp.sum(both[:, :key_dim] * norm_new, axis=1, keepdims=True)
    denom = jnp.maximum(jnp.abs(dot), jnp.exp(-max_new))
    done = (numer * (1.0 / (1.0 + jnp.exp(-outgate))) / denom).astype(jnp.bfloat16)
    for peer in range(heads.shape[0]):
        heads[peer] = done
    for copy in copies:
        copy.wait()


def on_chip(*arrays):
    return [pltpu.with_memory_space_constraint(a, pltpu.VMEM) for a in arrays]


def project(tokens, aux, weights, peers):
    seqs = tokens.shape[-1]
    return pl.pallas_call(
        project_body,
        out_shape=pltpu.VMEM((peers, seqs // peers, 4 * LANES), jnp.bfloat16),
        name="project",
    )(*on_chip(tokens, aux, *weights))


def memory_step(tiles, cell, aux, width):
    peers, own, _ = tiles.shape
    _, key_dim, value_dim = cell.shape
    vmem = pl.BlockSpec(memory_space=pltpu.VMEM)
    hbm = pl.BlockSpec(memory_space=pl.ANY)
    return pl.pallas_call(
        functools.partial(memory_body, width),
        out_shape=(
            pltpu.VMEM((peers, own, value_dim), jnp.bfloat16),
            jax.ShapeDtypeStruct(cell.shape, jnp.float32),
            jax.ShapeDtypeStruct((own, key_dim), jnp.float32),
            jax.ShapeDtypeStruct((1, own), jnp.float32),
        ),
        in_specs=[vmem] * 3,
        out_specs=(vmem, hbm, hbm, hbm),
        scratch_shapes=[
            pltpu.VMEM(cell.shape, jnp.float32),
            pltpu.VMEM((own, key_dim), jnp.float32),
            pltpu.VMEM((1, own), jnp.float32),
            pltpu.SemaphoreType.DMA((own + 2,)),
        ],
        name="memory",
    )(*on_chip(tiles, cell, aux))


def on_device(
    tokens,
    gain_in,
    w_query,
    w_key,
    w_value,
    w_outgate,
    w_input_gate,
    w_forget_gate,
    bias_input,
    bias_forget,
    cell_state,
    norm_state,
    max_state,
    w_proj,
    gain_mid,
    w_up,
    w_down,
):
    seqs, own_columns = tokens.shape
    value_dim = cell_state.shape[3]
    tp, kv = lax.axis_size("tp"), lax.axis_size("kv")
    rows = gain_in.shape[0]
    width = rows * kv
    own = seqs // kv
    key_dim = cell_state.shape[2]
    heads_all = w_input_gate.shape[1]
    is_head = lax.broadcasted_iota(jnp.int32, (1, heads_all), 1) == lax.axis_index("tp")
    pick = is_head.astype(jnp.float32)
    aux_in = jnp.concatenate(
        [gain_in.reshape(1, rows), jnp.pad(pick, ((0, 0), (0, rows - heads_all)))], axis=0
    )
    biases = jnp.stack([jnp.sum(bias_input * pick[0]), jnp.sum(bias_forget * pick[0])])
    aux = jnp.concatenate(
        [norm_state[:, 0], max_state, jnp.broadcast_to(biases, (own, 2))], axis=1
    )
    aux = jnp.pad(aux, ((0, 0), (0, LANES - key_dim - 3)))

    own_tokens = tokens.T
    gathered, aux_in, aux, residual = lax.optimization_barrier(
        (spread(own_tokens, "tp"), aux_in, aux, own_tokens.astype(jnp.float32))
    )
    weights = (w_query.T, w_key.T, w_value, w_outgate, w_input_gate.T, w_forget_gate.T)
    terms = project(gathered, aux_in, weights, kv)
    heads, cell_new, norm_new, max_new = memory_step(
        exchange(terms, "kv"), cell_state[:, 0], aux, width
    )

    heads = exchange(heads, "kv").reshape(seqs, value_dim)
    branch = contract(w_proj, heads, 0, 1).astype(jnp.bfloat16)
    branch = exchange(branch.reshape(tp, own_columns, seqs), "tp")
    own_middle = residual + jnp.sum(branch.astype(jnp.float32), axis=0)
    own_middle = own_middle.astype(jnp.bfloat16)
    middle = spread(own_middle, "tp").reshape(rows, seqs).astype(jnp.float32)
    mid_squares = jnp.sum(middle * middle, axis=0)
    normed_mid = (middle * gain_mid[:, None]).astype(jnp.bfloat16)
    upward = contract(normed_mid, w_up, 0, 0)
    upward = jnp.concatenate([upward, mid_squares[:, None]], axis=1).astype(jnp.bfloat16)
    upward = exchange(upward.reshape(kv, own, -1), "kv")
    upward = jnp.sum(upward.astype(jnp.float32), axis=0)
    scale_mid = lax.rsqrt(upward[:, -1:] / width + EPSILON)
    hidden = jnp.square(jax.nn.relu(upward[:, :-1] * scale_mid)).astype(jnp.bfloat16)

    hidden = spread(hidden, "kv").reshape(seqs, -1)
    down = contract(w_down, hidden, 0, 1).astype(jnp.bfloat16)
    down = exchange(down.reshape(tp, own_columns, seqs), "tp")
    mixed = own_middle.astype(jnp.float32) + jnp.sum(down.astype(jnp.float32), axis=0)
    mixed = mixed.astype(jnp.bfloat16).T
    return (mixed, cell_new[:, None], norm_new[:, None], max_new.reshape(own, 1))


def solution(mesh):
    in_specs = (
        P("grp", ("kv", "tp")),
        P("kv"),
        P("kv", "tp"),
        P("kv", "tp"),
        P("kv", "tp"),
        P("kv", "tp"),
        P("kv", None),
        P("kv", None),
        P(),
        P(),
        P(("grp", "kv"), "tp", None, None),
        P(("grp", "kv"), "tp", None),
        P(("grp", "kv"), "tp"),
        P("tp", "kv"),
        P("kv"),
        P("kv", "tp"),
        P("tp", "kv"),
    )
    out_specs = (
        P("grp", ("kv", "tp")),
        P(("grp", "kv"), "tp", None, None),
        P(("grp", "kv"), "tp", None),
        P(("grp", "kv"), "tp"),
    )
    return jax.shard_map(
        on_device, mesh=mesh, in_specs=in_specs, out_specs=out_specs, check_vma=False
    )
```

time: 192 us -> 177 us (0.922)
  blocking collectives: 68.2 us -> 118 us
  waiting for transfers between devices: 35.5 us -> 5.68 us
  starting transfers between devices: 69.7 us -> 44.9 us
  local copies, waits for them, and re-layouts: 9.63 us -> 2.14 us
  other arithmetic: 6.45 us -> 3.13 us
  Pallas kernels: 0 us -> 1.93 us
    all_to_all x3 -> x7, blocking collectives: 41.2 us -> 118 us  [exchange(): return lax.all_to_all(tiles, axis, split_axis=0, concat_axis=0, tiled=True)]
    all_to_all x4 -> x1, waiting for transfers between devices: 35.5 us -> 5.68 us  [exchange(): return lax.all_to_all(tiles, axis, split_axis=0, concat_axis=0, tiled=True)]
    all_gather x1 -> x0, blocking collectives: 27.1 us -> none  [on_device(): hidden = lax.all_gather(hidden, 'kv', axis=0, tiled=True)]
    all_to_all x4 -> x1, starting transfers between devices: 69.7 us -> 44.9 us  [exchange(): return lax.all_to_all(tiles, axis, split_axis=0, concat_axis=0, tiled=True)]
    unnamed x34 -> x35, local copies, waits for them, and re-layouts: 4.5 us -> 0.17 us
    dynamic_slice x5 -> x0, local copies, waits for them, and re-layouts: 2.17 us -> none  [the longest x2 0.86 us: on_device(): gate_forget = lax.dynamic_slice_in_dim(w_forget_gate, head, 1, 1)]
    pallas_call x0 -> x2, Pallas kernels: none -> 1.93 us  [the longest x1 1.53 us: memory_step(): pl.pallas_call(functools.partial(memory_body, width), out_shape=(pltpu.VM...]
  transfers between devices with their start and end apart: 4 -> 1, of which waited for: 4 -> 1; matrix products, arithmetic and copies ran while one was open for 2% -> 1% of each run, Pallas kernels for 0% -> 0%
where the time goes in v2:
time: 177 us
  blocking collectives  118 us (67%)
  starting transfers between devices  44.9 us (25%)
  waiting for transfers between devices  5.68 us (3%)
  other arithmetic  3.13 us (2%)
  local copies, waits for them, and re-layouts  2.14 us (1%)
  Pallas kernels  1.93 us (1%)
    all_to_all x7, blocking collectives, exchange(): return lax.all_to_all(tiles, axis, split_axis=0, concat_axis=0, tiled=True)  118 us
    all_to_all x1, starting transfers between devices, exchange(): return lax.all_to_all(tiles, axis, split_axis=0, concat_axis=0, tiled=True)  44.9 us
    all_to_all x1, waiting for transfers between devices, exchange(): return lax.all_to_all(tiles, axis, split_axis=0, concat_axis=0, tiled=True)  5.68 us
  transfers between devices with their start and end apart: 1, of which 1 were waited for; matrix products, arithmetic and copies ran while one was open for 1% of the time, Pallas kernels for 0%

profile of v2, /device:TPU:65, one launch (start us, length us, event | category | flops | bytes accessed | tf_op | source)
XLA Modules:
  0.0 176.9 jit_solution(13468376986455481954)
XLA Ops:
  0.7 1.4 broadcast_in_dim.20
  2.1 44.9 %all-to-all-start = ((bf16[16,16,128]{2,1,0:T(8,128)(2,1)}), bf16[16,16,128]{2,1,0:T(8,128)(2,1)S(1)}, u32[]{:S(2)}, u32[]{:S(2)}) async-start(bf16[16,16,128]{2,1,0:T(8,128)(2,1)} %broadcast_in_dim.20), calls=%async_computation | async-start | bytes 131072 | tf_op jit(solution)/shard_map/all_to_all | solution.py:15
  47.1 0.6 fusion.14
  47.7 1.4 pad_maximum_fusion.2
  49.2 5.7 %all-to-all-done.tokens = bf16[16,16,128]{2,1,0:T(8,128)(2,1)S(1)} async-done(((bf16[16,16,128]{2,1,0:T(8,128)(2,1)}), bf16[16,16,128]{2,1,0:T(8,128)(2,1)S(1)}, u32[]{:S(2)}, u32[]{:S(2)}) %all-to-all-start) | async-done | bytes 65568 | tf_op jit(solution)/shard_map/all_to_all | solution.py:15
  54.9 0.4 project.1
  55.4 19.0 %all_to_all.40.tiles = bf16[16,8,512]{2,1,0:T(8,128)(2,1)S(1)} all-to-all(bf16[16,8,512]{2,1,0:T(8,128)(2,1)S(1)} %project.1), channel_id=1, replica_groups=mesh['grp'=2,'kv'=16,'tp'=16] {'kv'}, dimensions={0} | all-to-all | bytes 262144 | tf_op jit(solution)/shard_map/all_to_all | solution.py:15
  74.3 1.5 memory.1
  75.9 17.9 %all_to_all.41 = bf16[16,8,128]{2,1,0:T(8,128)(2,1)S(1)} all-to-all(bf16[16,8,128]{2,1,0:T(8,128)(2,1)S(1)} %get-tuple-element.16), channel_id=1, replica_groups=mesh['grp'=2,'kv'=16,'tp'=16] {'kv'}, dimensions={0} | all-to-all | bytes 65536 | tf_op jit(solution)/shard_map/all_to_all | solution.py:15
  93.8 0.1 fusion
  94.0 0.1 copy.51
  94.1 12.3 %all_to_all.42 = bf16[16,16,128]{2,1,0:T(8,128)(2,1)S(1)} all-to-all(bf16[16,16,128]{2,1,0:T(8,128)(2,1)S(1)} %bitcast.50), channel_id=1, replica_groups=mesh['grp'=2,'kv'=16,'tp'=16] {'tp'}, dimensions={0} | all-to-all | bytes 131072 | tf_op jit(solution)/shard_map/all_to_all | solution.py:15
  106.4 10.7 %all_to_all.43 = bf16[16,16,128]{2,1,0:T(8,128)(2,1)S(1)} all-to-all(bf16[16,16,128]{2,1,0:T(8,128)(2,1)S(1)} %broadcast_in_dim.22), channel_id=1, replica_groups=mesh['grp'=2,'kv'=16,'tp'=16] {'tp'}, dimensions={0} | all-to-all | bytes 131072 | tf_op jit(solution)/shard_map/all_to_all | solution.py:15
  117.1 0.1 fusion.4
  117.2 0.1 copy.52
  117.4 0.2 concatenate.17
  117.6 0.2 convolution_convert_fusion
  117.9 17.4 %all_to_all.44 = bf16[16,8,1025]{2,1,0:T(8,128)(2,1)S(1)} all-to-all(bf16[16,8,1025]{2,1,0:T(8,128)(2,1)S(1)} %pad_maximum_fusion), channel_id=1, replica_groups=mesh['grp'=2,'kv'=16,'tp'=16] {'kv'}, dimensions={0} | all-to-all | bytes 524800 | tf_op jit(solution)/shard_map/all_to_all | solution.py:15
  135.4 0.1 fusion.13
  135.6 24.6 %all_to_all.45 = bf16[16,8,1024]{2,1,0:T(8,128)(2,1)S(1)} all-to-all(bf16[16,8,1024]{2,1,0:T(8,128)(2,1)S(1)} %broadcast_in_dim.23), channel_id=1, replica_groups=mesh['grp'=2,'kv'=16,'tp'=16] {'kv'}, dimensions={0} | all-to-all | bytes 524288 | tf_op jit(solution)/shard_map/all_to_all | solution.py:15
  160.2 0.2 fusion.1
  160.5 0.1 copy.54
  160.6 15.7 %all_to_all.46 = bf16[16,16,128]{2,1,0:T(8,128)(2,1)S(1)} all-to-all(bf16[16,16,128]{2,1,0:T(8,128)(2,1)S(1)} %bitcast.51), channel_id=1, replica_groups=mesh['grp'=2,'kv'=16,'tp'=16] {'tp'}, dimensions={0} | all-to-all | bytes 131072 | tf_op jit(solution)/shard_map/all_to_all | solution.py:15
  176.3 0.6 fusion.10
  (50 shorter events, 0.6 us)
Async XLA Ops:
  0.6 117.0 %copy-start = (bf16[256,1024]{1,0:T(8,128)(2,1)S(1)}, bf16[256,1024]{1,0:T(8,128)(2,1)}, u32[]{:S(2)}) copy-start(bf16[256,1024]{1,0:T(8,128)(2,1)} %param.32) | copy-start | bytes 1572868
  0.6 46.3 %copy-start.10 = (bf16[128,16]{0,1:T(8,128)(2,1)S(1)}, bf16[128,16]{0,1:T(8,128)(2,1)}, u32[]{:S(2)}) copy-start(bf16[128,16]{0,1:T(8,128)(2,1)} %param.17) | copy-start | bytes 12292
  0.7 46.5 %copy-start.16 = (f32[16]{0:T(128)S(1)}, f32[16]{0:T(128)}, u32[]{:S(2)}) copy-start(f32[16]{0:T(128)} %param.26) | copy-start | bytes 196
  0.7 48.4 %copy-start.11 = (f32[8,1,64]{2,1,0:T(1,128)S(1)}, f32[8,1,64]{2,1,0:T(1,128)}, u32[]{:S(2)}) copy-start(f32[8,1,64]{2,1,0:T(1,128)} %param.28) | copy-start | bytes 6148
  0.7 54.2 %copy-start.7 = (bf16[256,16]{0,1:T(8,128)(2,1)S(1)}, bf16[256,16]{0,1:T(8,128)(2,1)}, u32[]{:S(2)}) copy-start(bf16[256,16]{0,1:T(8,128)(2,1)} %param.24) | copy-start | bytes 24580
  2.1 45.0 %copy-start.14 = (f32[8,1]{0,1:T(1,128)S(1)}, f32[8,1]{0,1:T(1,128)}, u32[]{:S(2)}) copy-start(f32[8,1]{0,1:T(1,128)} %param.29) | copy-start | bytes 100
  2.1 45.1 %copy-start.15 = (f32[16]{0:T(128)S(1)}, f32[16]{0:T(128)}, u32[]{:S(2)}) copy-start(f32[16]{0:T(128)} %param.25) | copy-start | bytes 196
  2.1 47.1 %copy-start.13 = (f32[256]{0:T(256)S(1)}, f32[256]{0:T(256)}, u32[]{:S(2)}) copy-start(f32[256]{0:T(256)} %param.18) | copy-start | bytes 3076
  2.1 52.8 %copy-start.3 = (bf16[256,128]{1,0:T(8,128)(2,1)S(1)}, bf16[256,128]{1,0:T(8,128)(2,1)}, u32[]{:S(2)}) copy-start(bf16[256,128]{1,0:T(8,128)(2,1)} %wo.1) | copy-start | bytes 196612
  2.1 52.8 %copy-start.4 = (bf16[256,64]{0,1:T(8,128)(2,1)S(1)}, bf16[256,64]{0,1:T(8,128)(2,1)}, u32[]{:S(2)}) copy-start(bf16[256,64]{0,1:T(8,128)(2,1)} %param.19) | copy-start | bytes 98308
  2.1 52.8 %copy-start.5 = (bf16[256,64]{0,1:T(8,128)(2,1)S(1)}, bf16[256,64]{0,1:T(8,128)(2,1)}, u32[]{:S(2)}) copy-start(bf16[256,64]{0,1:T(8,128)(2,1)} %param.20) | copy-start | bytes 98308
  2.1 52.8 %all-to-all-start = ((bf16[16,16,128]{2,1,0:T(8,128)(2,1)}), bf16[16,16,128]{2,1,0:T(8,128)(2,1)S(1)}, u32[]{:S(2)}, u32[]{:S(2)}) async-start(bf16[16,16,128]{2,1,0:T(8,128)(2,1)} %broadcast_in_dim.20), calls=%async_computation | async-start | bytes 131072 | tf_op jit(solution)/shard_map/all_to_all | solution.py:15
  47.0 7.9 %copy-start.2 = (bf16[256,128]{1,0:T(8,128)(2,1)S(1)}, bf16[256,128]{1,0:T(8,128)(2,1)}, u32[]{:S(2)}) copy-start(bf16[256,128]{1,0:T(8,128)(2,1)} %wv.1) | copy-start | bytes 196612
  49.2 5.7 %copy-start.6 = (bf16[256,16]{0,1:T(8,128)(2,1)S(1)}, bf16[256,16]{0,1:T(8,128)(2,1)}, u32[]{:S(2)}) copy-start(bf16[256,16]{0,1:T(8,128)(2,1)} %param.23) | copy-start | bytes 24580
  54.9 19.4 %copy-start.1 = (f32[8,1,64,128]{3,2,1,0:T(8,128)S(1)}, f32[8,1,64,128]{3,2,1,0:T(8,128)}, u32[]{:S(2)}) copy-start(f32[8,1,64,128]{3,2,1,0:T(8,128)} %param.27) | copy-start | bytes 786436
  75.9 17.9 %copy-start.9 = (bf16[128,256]{1,0:T(8,128)(2,1)S(1)}, bf16[128,256]{1,0:T(8,128)(2,1)}, u32[]{:S(2)}) copy-start(bf16[128,256]{1,0:T(8,128)(2,1)} %param.30) | copy-start | bytes 196612
  106.4 10.7 %copy-start.12 = (f32[256]{0:T(256)S(1)}, f32[256]{0:T(256)}, u32[]{:S(2)}) copy-start(f32[256]{0:T(256)} %param.31) | copy-start | bytes 3076
  135.3 24.9 %copy-start.8 = (bf16[1024,256]{1,0:T(8,128)(2,1)S(1)}, bf16[1024,256]{1,0:T(8,128)(2,1)}, u32[]{:S(2)}) copy-start(bf16[1024,256]{1,0:T(8,128)(2,1)} %param.33) | copy-start | bytes 1572868

commit v3 on v2

--- a/solution.py
+++ b/solution.py
@@ -11,6 +11,9 @@
 LANES = 128
 
 
+KV = ("kv_pair", "kv_side")
+
+
 def exchange(tiles, axis):
     return lax.all_to_all(tiles, axis, split_axis=0, concat_axis=0, tiled=True)
 
@@ -29,8 +32,25 @@
     return high, (value - high).astype(jnp.bfloat16).astype(jnp.float32)
 
 
-def project_body(tokens, aux, wq, wk, wv, wo, wi, wf, out):
-    gain, pick = aux[0:1], aux[1:2, : wi.shape[0]]
+def project_body(
+    tokens, gain, pick, norm, top, bias_in, bias_forget,
+    wq, wk, wv, wo, wi, wf, out, aux, residual,
+):
+    gain, pick = gain[...], pick[...]
+    mine = jnp.zeros(residual.shape, jnp.float32)
+    for peer in range(tokens.shape[0]):
+        mine += tokens[peer].astype(jnp.float32) * pick[:, peer : peer + 1]
+    residual[...] = mine
+    count, key_dim = norm.shape
+    place = lax.broadcasted_iota(jnp.int32, (count, LANES - key_dim), 1)
+    first = jnp.sum(bias_in[...] * pick, axis=1, keepdims=True)
+    second = jnp.sum(bias_forget[...] * pick, axis=1, keepdims=True)
+    eye = lax.broadcasted_iota(jnp.int32, (count, count), 0)
+    eye = eye == lax.broadcasted_iota(jnp.int32, (count, count), 1)
+    turned = jnp.sum(jnp.where(eye, top[...], 0.0), axis=1, keepdims=True)
+    rest = jnp.where(place == 1, first, jnp.where(place == 2, second, 0.0))
+    rest = jnp.where(place == 0, turned, rest)
+    aux[...] = jnp.concatenate([norm[...], rest], axis=1)
     wide = tokens[...].reshape(-1, tokens.shape[-1]).astype(jnp.float32).T
     squares = jnp.sum(wide * wide, axis=1, keepdims=True)
     normed = (wide * gain).astype(jnp.bfloat16)
@@ -110,13 +130,117 @@
     return [pltpu.with_memory_space_constraint(a, pltpu.VMEM) for a in arrays]
 
 
-def project(tokens, aux, weights, peers):
+def trade_body(w_up, w_down, gain, sent, gains, sems):
+    other = 1 - lax.axis_index("kv_side")
+    rows, columns = w_up.shape
+    half = columns // 2
+    at = pl.multiple_of(other * half, half)
+    copies = [
+        pltpu.make_async_copy(
+            w_up.at[:, pl.ds(at, half)], sent.at[pl.ds(0, rows), pl.ds(0, half)], sems.at[0]
+        )
+    ]
+    for part in range(half // rows):
+        first = pl.multiple_of(at + part * rows, rows)
+        copies.append(
+            pltpu.make_async_copy(
+                w_down.at[pl.ds(first, rows)],
+                sent.at[pl.ds(0, rows), pl.ds(half + part * rows, rows)],
+                sems.at[1 + part],
+            )
+        )
+    for copy in copies:
+        copy.start()
+    high, low = two_parts(gain[...])
+    line = lax.broadcasted_iota(jnp.int32, (gains.shape[0], rows), 0)
+    both = jnp.where(line == 0, high, jnp.where(line == 1, low, 0.0))
+    gains[...] = jnp.zeros(gains.shape, gains.dtype)
+    gains[:, :rows] = both.astype(jnp.bfloat16)
+    last = pltpu.make_async_copy(gains, sent.at[pl.ds(rows, gains.shape[0])], sems.at[3])
+    last.start()
+    for copy in (*copies, last):
+        copy.wait()
+
+
+def up_body(middle, gain, w_up, taken, out):
+    side = lax.axis_index("kv_side")
+    rows, columns = w_up.shape
+    half = columns // 2
+    count = middle.shape[0] // 2
+    mine = middle[pl.ds(side * count, count)].reshape(rows, -1).astype(jnp.float32).T
+    theirs = middle[pl.ds((1 - side) * count, count)].reshape(rows, -1).astype(jnp.float32).T
+    squares = jnp.sum(mine * mine + theirs * theirs, axis=1, keepdims=True)
+    gains = taken[rows : rows + 8, :rows].astype(jnp.float32)
+    mine = (mine * gain[...]).astype(jnp.bfloat16)
+    theirs = (theirs * (gains[0:1] + gains[1:2])).astype(jnp.bfloat16)
+    upward = contract(mine, w_up[:, pl.ds(pl.multiple_of(side * half, half), half)], 1, 0)
+    upward = upward + contract(theirs, taken[:rows, :half], 1, 0)
+    lane = lax.broadcasted_iota(jnp.int32, (mine.shape[0], LANES), 1)
+    high, low = two_parts(squares)
+    extra = jnp.where(lane == 0, high, jnp.where(lane == 1, low, 0.0)).astype(jnp.bfloat16)
+    upward = upward.astype(jnp.bfloat16)
+    peers, own, _ = out.shape
+    for peer in range(peers):
+        out[peer, :, :half] = upward[peer * own : (peer + 1) * own]
+        out[peer, :, half:] = extra[peer * own : (peer + 1) * own]
+
+
+def down_body(hidden, w_down, taken, out):
+    side = lax.axis_index("kv_side")
+    rows = w_down.shape[1]
+    half = hidden.shape[2]
+    count = out.shape[0] // 2
+    left = hidden[...].reshape(-1, half)
+    mine = contract(left, w_down[pl.ds(pl.multiple_of(side * half, half), half)], 1, 0)
+    theirs = contract(left[:, :rows], taken[:rows, half : half + rows], 1, 0)
+    for part in range(1, half // rows):
+        block = taken[:rows, half + part * rows : half + (part + 1) * rows]
+        theirs = theirs + contract(left[:, part * rows : (part + 1) * rows], block, 1, 0)
+    shape = (count, *out.shape[1:])
+    out[pl.ds(side * count, count)] = mine.T.astype(jnp.bfloat16).reshape(shape)
+    out[pl.ds((1 - side) * count, count)] = theirs.T.astype(jnp.bfloat16).reshape(shape)
+
+
+def trade(w_up, w_down, gain):
+    rows, columns = w_up.shape
+    hbm = pl.BlockSpec(memory_space=pl.ANY)
+    return pl.pallas_call(
+        trade_body,
+        out_shape=jax.ShapeDtypeStruct((rows + 8, columns), jnp.bfloat16),
+        in_specs=[hbm, hbm, pl.BlockSpec(memory_space=pltpu.VMEM)],
+        out_specs=hbm,
+        scratch_shapes=[pltpu.VMEM((8, columns), jnp.bfloat16), pltpu.SemaphoreType.DMA((4,))],
+        name="trade",
+    )(w_up, w_down, gain)
+
+
+def in_vmem(body, shape, *operands):
+    vmem = pl.BlockSpec(memory_space=pltpu.VMEM)
+    return pl.pallas_call(
+        body,
+        out_shape=pltpu.VMEM(shape, jnp.bfloat16),
+        in_specs=[vmem] * len(operands),
+        out_specs=vmem,
+        name=body.__name__,
+    )(*on_chip(*operands))
+
+
+def project(tokens, small, weights, peers):
     seqs = tokens.shape[-1]
+    own = seqs // peers
+    vmem = pl.BlockSpec(memory_space=pltpu.VMEM)
+    operands = on_chip(tokens, *small, *weights)
     return pl.pallas_call(
         project_body,
-        out_shape=pltpu.VMEM((peers, seqs // peers, 4 * LANES), jnp.bfloat16),
+        out_shape=(
+            pltpu.VMEM((peers, own, 4 * LANES), jnp.bfloat16),
+            pltpu.VMEM((own, LANES), jnp.float32),
+            pltpu.VMEM(tokens.shape[1:], jnp.float32),
+        ),
+        in_specs=[vmem] * len(operands),
+        out_specs=(vmem,) * 3,
         name="project",
-    )(*on_chip(tokens, aux, *weights))
+    )(*operands)
 
 
 def memory_step(tiles, cell, aux, width):
@@ -165,7 +289,9 @@
 ):
     seqs, own_columns = tokens.shape
     value_dim = cell_state.shape[3]
-    tp, kv = lax.axis_size("tp"), lax.axis_size("kv")
+    tp, kv = lax.axis_size("tp"), lax.axis_size(KV)
+    pairs = kv // 2
+    half = w_up.shape[1] // 2
     rows = gain_in.shape[0]
     width = rows * kv
     own = seqs // kv
@@ -173,73 +299,75 @@
     heads_all = w_input_gate.shape[1]
     is_head = lax.broadcasted_iota(jnp.int32, (1, heads_all), 1) == lax.axis_index("tp")
     pick = is_head.astype(jnp.float32)
-    aux_in = jnp.concatenate(
-        [gain_in.reshape(1, rows), jnp.pad(pick, ((0, 0), (0, rows - heads_all)))], axis=0
-    )
-    biases = jnp.stack([jnp.sum(bias_input * pick[0]), jnp.sum(bias_forget * pick[0])])
-    aux = jnp.concatenate(
-        [norm_state[:, 0], max_state, jnp.broadcast_to(biases, (own, 2))], axis=1
-    )
-    aux = jnp.pad(aux, ((0, 0), (0, LANES - key_dim - 3)))
-
-    own_tokens = tokens.T
-    gathered, aux_in, aux, residual = lax.optimization_barrier(
-        (spread(own_tokens, "tp"), aux_in, aux, own_tokens.astype(jnp.float32))
+
+    copies = jnp.broadcast_to(tokens.T, (tp, own_columns, seqs))
+    copies, pick = lax.optimization_barrier((copies, pick))
+    small = (
+        gain_in.reshape(1, rows),
+        pick,
+        norm_state[:, 0],
+        max_state.reshape(1, own),
+        bias_input.reshape(1, heads_all),
+        bias_forget.reshape(1, heads_all),
     )
     weights = (w_query.T, w_key.T, w_value, w_outgate, w_input_gate.T, w_forget_gate.T)
-    terms = project(gathered, aux_in, weights, kv)
+    terms, aux, residual = project(exchange(copies, "tp"), small, weights, kv)
     heads, cell_new, norm_new, max_new = memory_step(
-        exchange(terms, "kv"), cell_state[:, 0], aux, width
-    )
-
-    heads = exchange(heads, "kv").reshape(seqs, value_dim)
+        exchange(terms, KV), cell_state[:, 0], aux, width
+    )
+
+    heads = exchange(heads, KV).reshape(seqs, value_dim)
+    gain_mid = gain_mid.reshape(1, rows)
+    gain_late, heads = lax.optimization_barrier((gain_mid, heads))
+    taken = lax.ppermute(trade(w_up, w_down, gain_late), "kv_side", [(0, 1), (1, 0)])
+
     branch = contract(w_proj, heads, 0, 1).astype(jnp.bfloat16)
     branch = exchange(branch.reshape(tp, own_columns, seqs), "tp")
     own_middle = residual + jnp.sum(branch.astype(jnp.float32), axis=0)
     own_middle = own_middle.astype(jnp.bfloat16)
-    middle = spread(own_middle, "tp").reshape(rows, seqs).astype(jnp.float32)
-    mid_squares = jnp.sum(middle * middle, axis=0)
-    normed_mid = (middle * gain_mid[:, None]).astype(jnp.bfloat16)
-    upward = contract(normed_mid, w_up, 0, 0)
-    upward = jnp.concatenate([upward, mid_squares[:, None]], axis=1).astype(jnp.bfloat16)
-    upward = exchange(upward.reshape(kv, own, -1), "kv")
-    upward = jnp.sum(upward.astype(jnp.float32), axis=0)
-    scale_mid = lax.rsqrt(upward[:, -1:] / width + EPSILON)
-    hidden = jnp.square(jax.nn.relu(upward[:, :-1] * scale_mid)).astype(jnp.bfloat16)
-
-    hidden = spread(hidden, "kv").reshape(seqs, -1)
-    down = contract(w_down, hidden, 0, 1).astype(jnp.bfloat16)
-    down = exchange(down.reshape(tp, own_columns, seqs), "tp")
+    middle = spread(own_middle, ("kv_side", "tp"))
+    upward = in_vmem(up_body, (pairs, 2 * own, half + LANES), middle, gain_mid, w_up, taken)
+    upward = jnp.sum(exchange(upward, "kv_pair").astype(jnp.float32), axis=0)
+    total = upward[:, half : half + 1] + upward[:, half + 1 : half + 2]
+    scale_mid = lax.rsqrt(total / width + EPSILON)
+    hidden = jnp.square(jax.nn.relu(upward[:, :half] * scale_mid)).astype(jnp.bfloat16)
+
+    hidden = spread(hidden, "kv_pair")
+    down = in_vmem(down_body, (2 * tp, own_columns, seqs), hidden, w_down, taken)
+    down = exchange(down, ("kv_side", "tp"))
     mixed = own_middle.astype(jnp.float32) + jnp.sum(down.astype(jnp.float32), axis=0)
     mixed = mixed.astype(jnp.bfloat16).T
     return (mixed, cell_new[:, None], norm_new[:, None], max_new.reshape(own, 1))
 
 
 def solution(mesh):
+    sizes = mesh.devices.shape
+    halves = (sizes[0], sizes[1] // 2, 2, sizes[2])
+    mesh = jax.sharding.Mesh(mesh.devices.reshape(halves), ("grp", *KV, "tp"))
     in_specs = (
-        P("grp", ("kv", "tp")),
-        P("kv"),
-        P("kv", "tp"),
-        P("kv", "tp"),
-        P("kv", "tp"),
-        P("kv", "tp"),
-        P("kv", None),
-        P("kv", None),
+        P("grp", (*KV, "tp")),
+        P(KV),
+        P(KV, "tp"),
+        P(KV, "tp"),
+        P(KV, "tp"),
+        P(KV, "tp"),
+        P(KV, None),
+        P(KV, None),
         P(),
         P(),
-        P(("grp", "kv"), "tp", None, None),
-        P(("grp", "kv"), "tp", None),
-        P(("grp", "kv"), "tp"),
-        P("tp", "kv"),
-        P("kv"),
-        P("kv", "tp"),
-        P("tp", "kv"),
+        P(("grp", *KV), "tp", None, None),
+        P(("grp", *KV), "tp", None),
+        P(("grp", *KV), "tp"),
+        P("tp", KV),
+        P(KV),
+        P(KV, "tp"),
+        P("tp", KV),
     )
     out_specs = (
-        P("grp", ("kv", "tp")),
-        P(("grp", "kv"), "tp", None, None),
-        P(("grp", "kv"), "tp", None),
-        P(("grp", "kv"), "tp"),
+        P("grp", (*KV, "tp")),
+        P(("grp", *KV), "tp", None, None),
+        P(("grp", *KV), "tp", None),
+        P(("grp", *KV), "tp"),
     )
     return jax.shard_map(
         on_device, mesh=mesh, in_specs=in_specs, out_specs=out_specs, check_vma=False

time: 177 us -> 192 us (1.085)
  starting transfers between devices: 44.9 us -> 16.5 us
  blocking collectives: 118 us -> 140 us
  Pallas kernels: 1.93 us -> 20.3 us
  waiting for transfers between devices: 5.68 us -> 10.2 us
  other arithmetic: 3.13 us -> 0.96 us
    all_to_all x1 -> x2, starting transfers between devices: 44.9 us -> 14 us  [exchange(): return lax.all_to_all(tiles, axis, split_axis=0, concat_axis=0, tiled=True)]
    all_to_all x7 -> x6, blocking collectives: 118 us -> 140 us  [exchange(): return lax.all_to_all(tiles, axis, split_axis=0, concat_axis=0, tiled=True)]
    pallas_call x1 -> x4, Pallas kernels: 0.41 us -> 18.8 us  [the longest x1 17.8 us: trade(): pl.pallas_call(trade_body, out_shape=jax.ShapeDtypeStruct((rows + 8, colu...]
    ppermute x0 -> x1, waiting for transfers between devices: none -> 3.32 us  [on_device(): lax.ppermute(trade(w_up, w_down, gain_late), 'kv_side', [(0, 1), (1, 0)])]
    ppermute x0 -> x1, starting transfers between devices: none -> 2.48 us  [on_device(): lax.ppermute(trade(w_up, w_down, gain_late), 'kv_side', [(0, 1), (1, 0)])]
    all_to_all x1 -> x2, waiting for transfers between devices: 5.68 us -> 6.88 us  [exchange(): return lax.all_to_all(tiles, axis, split_axis=0, concat_axis=0, tiled=True)]
  transfers between devices with their start and end apart: 1 -> 3, of which waited for: 1 -> 2; matrix products, arithmetic and copies ran while one was open for 1% -> 0% of each run, Pallas kernels for 0% -> 9%
where the time goes in v3:
time: 192 us; the launch traced here: 191 us
  blocking collectives  140 us (73%)
  Pallas kernels  20.3 us (11%)
  starting transfers between devices  16.5 us (9%)
  waiting for transfers between devices  10.2 us (5%)
  local copies, waits for them, and re-layouts  2.77 us (1%)
    all_to_all x6, blocking collectives, exchange(): return lax.all_to_all(tiles, axis, split_axis=0, concat_axis=0, tiled=True)  140 us
    pallas_call x1, Pallas kernels, trade(): pl.pallas_call(trade_body, out_shape=jax.ShapeDtypeStruct((rows + 8, colu...  17.8 us
    all_to_all x2, starting transfers between devices, exchange(): return lax.all_to_all(tiles, axis, split_axis=0, concat_axis=0, tiled=True)  14 us
    all_to_all x2, waiting for transfers between devices, exchange(): return lax.all_to_all(tiles, axis, split_axis=0, concat_axis=0, tiled=True)  6.88 us
  transfers between devices with their start and end apart: 3, of which 2 were waited for; matrix products, arithmetic and copies ran while one was open for 0% of the time, Pallas kernels for 9%

profile of v3, /device:TPU:65, one launch (start us, length us, event | category | flops | bytes accessed | tf_op | source)
XLA Modules:
  0.0 191.4 jit_solution(14936660412132522168)
XLA Ops:
  0.7 0.7 copy-done.16
  1.4 51.9 %all_to_all.40.tokens = bf16[16,16,128]{2,1,0:T(8,128)(2,1)S(1)} all-to-all(bf16[16,16,128]{2,1,0:T(8,128)(2,1)S(1)} %broadcast_in_dim.15), channel_id=1, replica_groups=mesh['grp'=2,'kv_pair'=8,'kv_side'=2,'tp'=16] {'tp'}, dimensions={0} | all-to-all | bytes 131072 | tf_op jit(solution)/shard_map/all_to_all | solution.py:18
  53.4 0.6 copy-done.9
  54.0 0.4 project.1
  54.4 19.7 %all_to_all.41.tiles = bf16[16,8,512]{2,1,0:T(8,128)(2,1)S(1)} all-to-all(bf16[16,8,512]{2,1,0:T(8,128)(2,1)S(1)} %get-tuple-element.18), channel_id=1, replica_groups=mesh['grp'=2,'kv_pair'=8,'kv_side'=2,'tp'=16] {'kv_pair','kv_side'}, dimensions={0} | all-to-all | bytes 262144 | tf_op jit(solution)/shard_map/all_to_all | solution.py:18
  74.1 1.5 memory.1
  75.6 17.8 %all_to_all.42 = bf16[16,8,128]{2,1,0:T(8,128)(2,1)S(1)} all-to-all(bf16[16,8,128]{2,1,0:T(8,128)(2,1)S(1)} %get-tuple-element.20), channel_id=1, replica_groups=mesh['grp'=2,'kv_pair'=8,'kv_side'=2,'tp'=16] {'kv_pair','kv_side'}, dimensions={0} | all-to-all | bytes 65536 | tf_op jit(solution)/shard_map/all_to_all | solution.py:18
  93.4 0.1 fusion
  93.6 0.7 copy.31
  94.3 5.2 %all-to-all-start.3 = ((bf16[16,16,128]{2,1,0:T(8,128)(2,1)}), bf16[16,16,128]{2,1,0:T(8,128)(2,1)S(1)}, u32[]{:S(2)}, u32[]{:S(2)}) async-start(bf16[16,16,128]{2,1,0:T(8,128)(2,1)} %bitcast.14), calls=%async_computation.3 | async-start | bytes 131072 | tf_op jit(solution)/shard_map/all_to_all | solution.py:18
  99.5 17.8 %trade.1 = bf16[264,1024]{1,0:T(8,128)(2,1)} custom-call(bf16[256,1024]{1,0:T(8,128)(2,1)} %w_up.3, bf16[1024,256]{1,0:T(8,128)(2,1)} %w_down.3, f32[1,256]{1,0:T(1,128)} %bitcast.33), custom_call_target="tpu_custom_call" | custom-call | tf_op jit(solution)/shard_map/trade/pallas_call | solution.py:207
  117.3 2.5 %collective-permute-start = (bf16[264,1024]{1,0:T(8,128)(2,1)}, bf16[264,1024]{1,0:T(8,128)(2,1)S(1)}, u32[]{:S(2)}, u32[]{:S(2)}) collective-permute-start(bf16[264,1024]{1,0:T(8,128)(2,1)} %trade.1), channel_id=1, source_target_pairs={{0,16},{16,0},{1,17},{17,1},{2,18},{18,2},{3,19},{19,3},{4,20},{20... | collective-permute-start | bytes 1622024 | tf_op jit(solution)/shard_map/ppermute | solution.py:322
  119.9 0.7 broadcast_in_dim.16
  120.5 8.8 %all-to-all-start.4 = ((bf16[32,16,128]{2,1,0:T(8,128)(2,1)}), bf16[32,16,128]{2,1,0:T(8,128)(2,1)S(1)}, u32[]{:S(2)}, u32[]{:S(2)}) async-start(bf16[32,16,128]{2,1,0:T(8,128)(2,1)} %broadcast_in_dim.16), calls=%async_computation.4 | async-start | bytes 262144 | tf_op jit(solution)/shard_map/all_to_all | solution.py:18
  129.3 3.3 %collective-permute-done.taken = bf16[264,1024]{1,0:T(8,128)(2,1)S(1)} collective-permute-done((bf16[264,1024]{1,0:T(8,128)(2,1)}, bf16[264,1024]{1,0:T(8,128)(2,1)S(1)}, u32[]{:S(2)}, u32[]{:S(2)}) %collective-permute-start) | collective-permute-done | bytes 540704 | tf_op jit(solution)/shard_map/ppermute | solution.py:322
  132.6 6.9 %all-to-all-done.4.middle = bf16[32,16,128]{2,1,0:T(8,128)(2,1)S(1)} async-done(((bf16[32,16,128]{2,1,0:T(8,128)(2,1)}), bf16[32,16,128]{2,1,0:T(8,128)(2,1)S(1)}, u32[]{:S(2)}, u32[]{:S(2)}) %all-to-all-start.4) | async-done | bytes 131104 | tf_op jit(solution)/shard_map/all_to_all | solution.py:18
  139.5 0.3 up_body.1
  139.8 16.8 %all_to_all.43 = bf16[8,16,640]{2,1,0:T(8,128)(2,1)S(1)} all-to-all(bf16[8,16,640]{2,1,0:T(8,128)(2,1)S(1)} %up_body.1), channel_id=1, replica_groups=mesh['grp'=2,'kv_pair'=8,'kv_side'=2,'tp'=16] {'kv_pair'}, dimensions={0} | all-to-all | bytes 327680 | tf_op jit(solution)/shard_map/all_to_all | solution.py:18
  156.7 0.2 fusion.7
  156.9 0.1 fusion.3
  157.0 17.6 %all_to_all.44.hidden = bf16[8,16,512]{2,1,0:T(8,128)(2,1)S(1)} all-to-all(bf16[8,16,512]{2,1,0:T(8,128)(2,1)S(1)} %broadcast_in_dim.17), channel_id=1, replica_groups=mesh['grp'=2,'kv_pair'=8,'kv_side'=2,'tp'=16] {'kv_pair'}, dimensions={0} | all-to-all | bytes 262144 | tf_op jit(solution)/shard_map/all_to_all | solution.py:18
  174.5 0.3 down_body.1
  174.8 15.9 %all_to_all.45 = bf16[32,16,128]{2,1,0:T(8,128)(2,1)S(1)} all-to-all(bf16[32,16,128]{2,1,0:T(8,128)(2,1)S(1)} %down_body.1), channel_id=1, replica_groups=mesh['grp'=2,'kv_pair'=8,'kv_side'=2,'tp'=16] {'kv_side','tp'}, dimensions={0} | all-to-all | bytes 262144 | tf_op jit(solution)/shard_map/all_to_all | solution.py:18
  190.8 0.6 fusion.8
  (40 shorter events, 0.2 us)
Async XLA Ops:
  0.6 92.8 %copy-start = (bf16[128,256]{1,0:T(8,128)(2,1)S(1)}, bf16[128,256]{1,0:T(8,128)(2,1)}, u32[]{:S(2)}) copy-start(bf16[128,256]{1,0:T(8,128)(2,1)} %param.30) | copy-start | bytes 196612
  0.6 0.7 copy-start.16
  0.7 52.7 %copy-start.13 = (f32[8,1]{0,1:T(1,128)S(1)}, f32[8,1]{0,1:T(1,128)}, u32[]{:S(2)}) copy-start(f32[8,1]{0,1:T(1,128)} %param.29) | copy-start | bytes 100
  0.7 52.7 %copy-start.14 = (f32[16]{0:T(128)S(1)}, f32[16]{0:T(128)}, u32[]{:S(2)}) copy-start(f32[16]{0:T(128)} %param.25) | copy-start | bytes 196
  0.7 52.7 %copy-start.15 = (f32[16]{0:T(128)S(1)}, f32[16]{0:T(128)}, u32[]{:S(2)}) copy-start(f32[16]{0:T(128)} %param.26) | copy-start | bytes 196
  1.4 52.0 %copy-start.6 = (bf16[256,64]{0,1:T(8,128)(2,1)S(1)}, bf16[256,64]{0,1:T(8,128)(2,1)}, u32[]{:S(2)}) copy-start(bf16[256,64]{0,1:T(8,128)(2,1)} %param.19) | copy-start | bytes 98308
  1.4 52.0 %copy-start.7 = (bf16[256,64]{0,1:T(8,128)(2,1)S(1)}, bf16[256,64]{0,1:T(8,128)(2,1)}, u32[]{:S(2)}) copy-start(bf16[256,64]{0,1:T(8,128)(2,1)} %param.20) | copy-start | bytes 98308
  1.4 52.0 %copy-start.10 = (f32[8,1,64]{2,1,0:T(1,128)S(1)}, f32[8,1,64]{2,1,0:T(1,128)}, u32[]{:S(2)}) copy-start(f32[8,1,64]{2,1,0:T(1,128)} %param.28) | copy-start | bytes 6148
  1.4 52.0 %copy-start.4 = (bf16[256,128]{1,0:T(8,128)(2,1)S(1)}, bf16[256,128]{1,0:T(8,128)(2,1)}, u32[]{:S(2)}) copy-start(bf16[256,128]{1,0:T(8,128)(2,1)} %wv.1) | copy-start | bytes 196612
  1.4 52.0 %copy-start.5 = (bf16[256,128]{1,0:T(8,128)(2,1)S(1)}, bf16[256,128]{1,0:T(8,128)(2,1)}, u32[]{:S(2)}) copy-start(bf16[256,128]{1,0:T(8,128)(2,1)} %wo.1) | copy-start | bytes 196612
  53.3 0.7 copy-start.9
  53.3 0.7 copy-start.8
  53.3 0.7 copy-start.12
  54.0 20.1 %copy-start.3 = (f32[8,1,64,128]{3,2,1,0:T(8,128)S(1)}, f32[8,1,64,128]{3,2,1,0:T(8,128)}, u32[]{:S(2)}) copy-start(f32[8,1,64,128]{3,2,1,0:T(8,128)} %param.27) | copy-start | bytes 786436
  94.3 25.5 %all-to-all-start.3 = ((bf16[16,16,128]{2,1,0:T(8,128)(2,1)}), bf16[16,16,128]{2,1,0:T(8,128)(2,1)S(1)}, u32[]{:S(2)}, u32[]{:S(2)}) async-start(bf16[16,16,128]{2,1,0:T(8,128)(2,1)} %bitcast.14), calls=%async_computation.3 | async-start | bytes 131072 | tf_op jit(solution)/shard_map/all_to_all | solution.py:18
  99.5 40.0 %copy-start.1 = (bf16[256,1024]{1,0:T(8,128)(2,1)S(1)}, bf16[256,1024]{1,0:T(8,128)(2,1)}, u32[]{:S(2)}) copy-start(bf16[256,1024]{1,0:T(8,128)(2,1)} %w_up.3) | copy-start | bytes 1572868
  117.3 15.3 %collective-permute-start = (bf16[264,1024]{1,0:T(8,128)(2,1)}, bf16[264,1024]{1,0:T(8,128)(2,1)S(1)}, u32[]{:S(2)}, u32[]{:S(2)}) collective-permute-start(bf16[264,1024]{1,0:T(8,128)(2,1)} %trade.1), channel_id=1, source_target_pairs={{0,16},{16,0},{1,17},{17,1},{2,18},{18,2},{3,19},{19,3},{4,20},{20... | collective-permute-start | bytes 1622024 | tf_op jit(solution)/shard_map/ppermute | solution.py:322
  120.5 19.0 %copy-start.11 = (f32[256]{0:T(256)S(1)}, f32[256]{0:T(256)}, u32[]{:S(2)}) copy-start(f32[256]{0:T(256)} %param.31) | copy-start | bytes 3076
  120.5 19.0 %all-to-all-start.4 = ((bf16[32,16,128]{2,1,0:T(8,128)(2,1)}), bf16[32,16,128]{2,1,0:T(8,128)(2,1)S(1)}, u32[]{:S(2)}, u32[]{:S(2)}) async-start(bf16[32,16,128]{2,1,0:T(8,128)(2,1)} %broadcast_in_dim.16), calls=%async_computation.4 | async-start | bytes 262144 | tf_op jit(solution)/shard_map/all_to_all | solution.py:18
  139.8 34.7 %copy-start.2 = (bf16[1024,256]{1,0:T(8,128)(2,1)S(1)}, bf16[1024,256]{1,0:T(8,128)(2,1)}, u32[]{:S(2)}) copy-start(bf16[1024,256]{1,0:T(8,128)(2,1)} %w_down.3) | copy-start | bytes 1572868

commit v4 on v3

--- a/solution.py
+++ b/solution.py
@@ -6,6 +6,7 @@
 from jax.experimental import pallas as pl
 from jax.experimental.pallas import tpu as pltpu
 from jax.sharding import PartitionSpec as P
+
 
 EPSILON = 1e-06
 LANES = 128
@@ -77,10 +78,27 @@
 
 
 def memory_body(
-    width, tiles, cell, aux,
-    heads, cell_out, norm_out, top_out, cell_new, norm_buf, top_buf, sems,
+    width, tiles, cell, aux, gain, w_up, w_down,
+    heads, cell_out, norm_out, top_out, sent_up, sent_down, cell_new, norm_buf, top_buf, sems,
 ):
-    own, key_dim, value_dim = cell.shape
+    rows, columns = w_up.shape
+    half = columns // 2
+    at = pl.multiple_of((1 - lax.axis_index("kv_side")) * half, half)
+    last = sems.shape[0] - 1
+    copies = [
+        pltpu.make_async_copy(
+            w_up.at[:, pl.ds(at, half)], sent_up.at[pl.ds(0, rows)], sems.at[last - 1]
+        ),
+        pltpu.make_async_copy(w_down.at[pl.ds(at, half)], sent_down, sems.at[last]),
+    ]
+    for copy in copies:
+        copy.start()
+    high, low = two_parts(gain[...])
+    line = lax.broadcasted_iota(jnp.int32, (8, rows), 0)
+    both = jnp.where(line == 0, high, jnp.where(line == 1, low, 0.0))
+    sent_up[rows:, :rows] = both.astype(jnp.bfloat16)
+    sent_up[rows:, rows:] = jnp.zeros((8, half - rows), jnp.bfloat16)
+    own, key_dim, _ = cell.shape
     terms = jnp.sum(tiles[...].astype(jnp.float32), axis=0)
     extra = terms[:, 3 * LANES :]
     extra = extra[:, 0:3] + extra[:, 3:6]
@@ -103,12 +121,9 @@
     turned = jnp.concatenate([both] * (LANES // own), axis=0).T
     norm_new = keep * norm + both[:, key_dim:]
     norm_buf[...] = norm_new
-    copies = [
-        pltpu.make_async_copy(top_buf, top_out, sems.at[own]),
-        pltpu.make_async_copy(norm_buf, norm_out, sems.at[own + 1]),
-    ]
-    for copy in copies:
-        copy.start()
+    for buf, target, sem in ((top_buf, top_out, own), (norm_buf, norm_out, own + 1)):
+        copies.append(pltpu.make_async_copy(buf, target, sems.at[sem]))
+        copies[-1].start()
     rows = []
     for s in range(own):
         fresh = keep[s : s + 1] * cell[s] + turned[key_dim:, s : s + 1] * values[s : s + 1]
@@ -130,38 +145,6 @@
     return [pltpu.with_memory_space_constraint(a, pltpu.VMEM) for a in arrays]
 
 
-def trade_body(w_up, w_down, gain, sent, gains, sems):
-    other = 1 - lax.axis_index("kv_side")
-    rows, columns = w_up.shape
-    half = columns // 2
-    at = pl.multiple_of(other * half, half)
-    copies = [
-        pltpu.make_async_copy(
-            w_up.at[:, pl.ds(at, half)], sent.at[pl.ds(0, rows), pl.ds(0, half)], sems.at[0]
-        )
-    ]
-    for part in range(half // rows):
-        first = pl.multiple_of(at + part * rows, rows)
-        copies.append(
-            pltpu.make_async_copy(
-                w_down.at[pl.ds(first, rows)],
-                sent.at[pl.ds(0, rows), pl.ds(half + part * rows, rows)],
-                sems.at[1 + part],
-            )
-        )
-    for copy in copies:
-        copy.start()
-    high, low = two_parts(gain[...])
-    line = lax.broadcasted_iota(jnp.int32, (gains.shape[0], rows), 0)
-    both = jnp.where(line == 0, high, jnp.where(line == 1, low, 0.0))
-    gains[...] = jnp.zeros(gains.shape, gains.dtype)
-    gains[:, :rows] = both.astype(jnp.bfloat16)
-    last = pltpu.make_async_copy(gains, sent.at[pl.ds(rows, gains.shape[0])], sems.at[3])
-    last.start()
-    for copy in (*copies, last):
-        copy.wait()
-
-
 def up_body(middle, gain, w_up, taken, out):
     side = lax.axis_index("kv_side")
     rows, columns = w_up.shape
@@ -174,7 +157,7 @@
     mine = (mine * gain[...]).astype(jnp.bfloat16)
     theirs = (theirs * (gains[0:1] + gains[1:2])).astype(jnp.bfloat16)
     upward = contract(mine, w_up[:, pl.ds(pl.multiple_of(side * half, half), half)], 1, 0)
-    upward = upward + contract(theirs, taken[:rows, :half], 1, 0)
+    upward = upward + contract(theirs, taken[:rows], 1, 0)
     lane = lax.broadcasted_iota(jnp.int32, (mine.shape[0], LANES), 1)
     high, low = two_parts(squares)
     extra = jnp.where(lane == 0, high, jnp.where(lane == 1, low, 0.0)).astype(jnp.bfloat16)
@@ -187,31 +170,14 @@
 
 def down_body(hidden, w_down, taken, out):
     side = lax.axis_index("kv_side")
-    rows = w_down.shape[1]
     half = hidden.shape[2]
     count = out.shape[0] // 2
     left = hidden[...].reshape(-1, half)
     mine = contract(left, w_down[pl.ds(pl.multiple_of(side * half, half), half)], 1, 0)
-    theirs = contract(left[:, :rows], taken[:rows, half : half + rows], 1, 0)
-    for part in range(1, half // rows):
-        block = taken[:rows, half + part * rows : half + (part + 1) * rows]
-        theirs = theirs + contract(left[:, part * rows : (part + 1) * rows], block, 1, 0)
+    theirs = contract(left, taken[...], 1, 0)
     shape = (count, *out.shape[1:])
     out[pl.ds(side * count, count)] = mine.T.astype(jnp.bfloat16).reshape(shape)
     out[pl.ds((1 - side) * count, count)] = theirs.T.astype(jnp.bfloat16).reshape(shape)
-
-
-def trade(w_up, w_down, gain):
-    rows, columns = w_up.shape
-    hbm = pl.BlockSpec(memory_space=pl.ANY)
-    return pl.pallas_call(
-        trade_body,
-        out_shape=jax.ShapeDtypeStruct((rows + 8, columns), jnp.bfloat16),
-        in_specs=[hbm, hbm, pl.BlockSpec(memory_space=pltpu.VMEM)],
-        out_specs=hbm,
-        scratch_shapes=[pltpu.VMEM((8, columns), jnp.bfloat16), pltpu.SemaphoreType.DMA((4,))],
-        name="trade",
-    )(w_up, w_down, gain)
 
 
 def in_vmem(body, shape, *operands):
@@ -221,7 +187,6 @@
         out_shape=pltpu.VMEM(shape, jnp.bfloat16),
         in_specs=[vmem] * len(operands),
         out_specs=vmem,
-        name=body.__name__,
     )(*on_chip(*operands))
 
 
@@ -243,9 +208,10 @@
     )(*operands)
 
 
-def memory_step(tiles, cell, aux, width):
+def memory_step(tiles, cell, aux, gain, w_up, w_down, width):
     peers, own, _ = tiles.shape
     _, key_dim, value_dim = cell.shape
+    rows, columns = w_up.shape
     vmem = pl.BlockSpec(memory_space=pltpu.VMEM)
     hbm = pl.BlockSpec(memory_space=pl.ANY)
     return pl.pallas_call(
@@ -255,20 +221,22 @@
             jax.ShapeDtypeStruct(cell.shape, jnp.float32),
             jax.ShapeDtypeStruct((own, key_dim), jnp.float32),
             jax.ShapeDtypeStruct((1, own), jnp.float32),
+            pltpu.VMEM((rows + 8, columns // 2), jnp.bfloat16),
+            pltpu.VMEM((columns // 2, rows), jnp.bfloat16),
         ),
-        in_specs=[vmem] * 3,
-        out_specs=(vmem, hbm, hbm, hbm),
+        in_specs=[vmem] * 4 + [hbm] * 2,
+        out_specs=(vmem, hbm, hbm, hbm, vmem, vmem),
         scratch_shapes=[
             pltpu.VMEM(cell.shape, jnp.float32),
             pltpu.VMEM((own, key_dim), jnp.float32),
             pltpu.VMEM((1, own), jnp.float32),
-            pltpu.SemaphoreType.DMA((own + 2,)),
+            pltpu.SemaphoreType.DMA((own + 4,)),
         ],
         name="memory",
-    )(*on_chip(tiles, cell, aux))
-
-
-def on_device(
+    )(*on_chip(tiles, cell, aux, gain), w_up, w_down)
+
+
+def layer(
     tokens,
     gain_in,
     w_query,
@@ -295,13 +263,16 @@
     rows = gain_in.shape[0]
     width = rows * kv
     own = seqs // kv
-    key_dim = cell_state.shape[2]
     heads_all = w_input_gate.shape[1]
     is_head = lax.broadcasted_iota(jnp.int32, (1, heads_all), 1) == lax.axis_index("tp")
     pick = is_head.astype(jnp.float32)
 
+    gain_mid = gain_mid.reshape(1, rows)
+    swap = [(0, 1), (1, 0)]
+
     copies = jnp.broadcast_to(tokens.T, (tp, own_columns, seqs))
     copies, pick = lax.optimization_barrier((copies, pick))
+    gathered = exchange(copies, "tp")
     small = (
         gain_in.reshape(1, rows),
         pick,
@@ -311,29 +282,30 @@
         bias_forget.reshape(1, heads_all),
     )
     weights = (w_query.T, w_key.T, w_value, w_outgate, w_input_gate.T, w_forget_gate.T)
-    terms, aux, residual = project(exchange(copies, "tp"), small, weights, kv)
-    heads, cell_new, norm_new, max_new = memory_step(
-        exchange(terms, KV), cell_state[:, 0], aux, width
+    terms, aux, residual = project(gathered, small, weights, kv)
+    heads, cell_new, norm_new, max_new, sent_up, sent_down = memory_step(
+        exchange(terms, KV), cell_state[:, 0], aux, gain_mid, w_up, w_down, width
     )
 
     heads = exchange(heads, KV).reshape(seqs, value_dim)
-    gain_mid = gain_mid.reshape(1, rows)
-    gain_late, heads = lax.optimization_barrier((gain_mid, heads))
-    taken = lax.ppermute(trade(w_up, w_down, gain_late), "kv_side", [(0, 1), (1, 0)])
-
+    heads, sent_up, sent_down = lax.optimization_barrier((heads, sent_up, sent_down))
+    other_up = lax.ppermute(sent_up, "kv_side", swap)
+    other_down = lax.ppermute(sent_down, "kv_side", swap)
     branch = contract(w_proj, heads, 0, 1).astype(jnp.bfloat16)
     branch = exchange(branch.reshape(tp, own_columns, seqs), "tp")
     own_middle = residual + jnp.sum(branch.astype(jnp.float32), axis=0)
     own_middle = own_middle.astype(jnp.bfloat16)
     middle = spread(own_middle, ("kv_side", "tp"))
-    upward = in_vmem(up_body, (pairs, 2 * own, half + LANES), middle, gain_mid, w_up, taken)
-    upward = jnp.sum(exchange(upward, "kv_pair").astype(jnp.float32), axis=0)
+    upward = in_vmem(up_body, (pairs, 2 * own, half + LANES), middle, gain_mid, w_up, other_up)
+    upward = exchange(upward, "kv_pair")
+    upward = jnp.sum(upward.astype(jnp.float32), axis=0)
     total = upward[:, half : half + 1] + upward[:, half + 1 : half + 2]
     scale_mid = lax.rsqrt(total / width + EPSILON)
     hidden = jnp.square(jax.nn.relu(upward[:, :half] * scale_mid)).astype(jnp.bfloat16)
 
+    hidden, other_down = lax.optimization_barrier((hidden, other_down))
     hidden = spread(hidden, "kv_pair")
-    down = in_vmem(down_body, (2 * tp, own_columns, seqs), hidden, w_down, taken)
+    down = in_vmem(down_body, (2 * tp, own_columns, seqs), hidden, w_down, other_down)
     down = exchange(down, ("kv_side", "tp"))
     mixed = own_middle.astype(jnp.float32) + jnp.sum(down.astype(jnp.float32), axis=0)
     mixed = mixed.astype(jnp.bfloat16).T
@@ -369,6 +341,4 @@
         P(("grp", *KV), "tp", None),
         P(("grp", *KV), "tp"),
     )
-    return jax.shard_map(
-        on_device, mesh=mesh, in_specs=in_specs, out_specs=out_specs, check_vma=False
-    )
+    return jax.shard_map(layer, mesh=mesh, in_specs=in_specs, out_specs=out_specs, check_vma=False)

time: 192 us -> 185 us (0.964)
  Pallas kernels: 20.3 us -> 3.6 us
  waiting for transfers between devices: 10.2 us -> 16.7 us
  blocking collectives: 140 us -> 144 us
    pallas_call x1 -> x0, Pallas kernels: 17.8 us -> none  [trade(): pl.pallas_call(trade_body, out_shape=jax.ShapeDtypeStruct((rows + 8, colu...]
    all_to_all x2, starting transfers between devices: 14 us -> 7.9 us  [exchange(): return lax.all_to_all(tiles, axis, split_axis=0, concat_axis=0, tiled=True)]
    ppermute x1 -> x2, starting transfers between devices: 2.48 us -> 7.33 us  [the longest x1 3.83 us: layer(): other_down = lax.ppermute(sent_down, 'kv_side', swap)]
    all_to_all x6, blocking collectives: 140 us -> 144 us  [exchange(): return lax.all_to_all(tiles, axis, split_axis=0, concat_axis=0, tiled=True)]
    ppermute x1 -> x2, waiting for transfers between devices: 3.32 us -> 7.17 us  [the longest x1 5.75 us: layer(): other_up = lax.ppermute(sent_up, 'kv_side', swap)]
    all_to_all x2, waiting for transfers between devices: 6.88 us -> 9.52 us  [exchange(): return lax.all_to_all(tiles, axis, split_axis=0, concat_axis=0, tiled=True)]
  transfers between devices with their start and end apart: 3 -> 4, of which waited for: 2 -> 3; matrix products, arithmetic and copies ran while one was open for 0% -> 0% of each run, Pallas kernels for 9% -> 0%
where the time goes in v4:
time: 185 us
  blocking collectives  144 us (78%)
  waiting for transfers between devices  16.7 us (9%)
  starting transfers between devices  15.2 us (8%)
  Pallas kernels  3.6 us (2%)
  local copies, waits for them, and re-layouts  2.84 us (2%)
    all_to_all x6, blocking collectives, exchange(): return lax.all_to_all(tiles, axis, split_axis=0, concat_axis=0, tiled=True)  144 us
    all_to_all x2, waiting for transfers between devices, exchange(): return lax.all_to_all(tiles, axis, split_axis=0, concat_axis=0, tiled=True)  9.52 us
    all_to_all x2, starting transfers between devices, exchange(): return lax.all_to_all(tiles, axis, split_axis=0, concat_axis=0, tiled=True)  7.9 us
    ppermute x1, waiting for transfers between devices, layer(): other_up = lax.ppermute(sent_up, 'kv_side', swap)  5.75 us
    ppermute x1, starting transfers between devices, layer(): other_down = lax.ppermute(sent_down, 'kv_side', swap)  3.83 us
  transfers between devices with their start and end apart: 4, of which 3 were waited for; matrix products, arithmetic and copies ran while one was open for 0% of the time, Pallas kernels for 0%

profile of v4, /device:TPU:65, one launch (start us, length us, event | category | flops | bytes accessed | tf_op | source)
XLA Modules:
  0.0 184.7 jit_solution(4762941497790115750)
XLA Ops:
  0.7 0.7 copy-done.16
  1.4 51.9 %all_to_all.40.tokens = bf16[16,16,128]{2,1,0:T(8,128)(2,1)S(1)} all-to-all(bf16[16,16,128]{2,1,0:T(8,128)(2,1)S(1)} %broadcast_in_dim.15), channel_id=1, replica_groups=mesh['grp'=2,'kv_pair'=8,'kv_side'=2,'tp'=16] {'tp'}, dimensions={0} | all-to-all | bytes 131072 | tf_op jit(solution)/shard_map/all_to_all | solution.py:19
  53.4 0.6 copy-done.9
  54.0 0.4 project.1
  54.4 19.7 %all_to_all.41.tiles = bf16[16,8,512]{2,1,0:T(8,128)(2,1)S(1)} all-to-all(bf16[16,8,512]{2,1,0:T(8,128)(2,1)S(1)} %get-tuple-element.23), channel_id=1, replica_groups=mesh['grp'=2,'kv_pair'=8,'kv_side'=2,'tp'=16] {'kv_pair','kv_side'}, dimensions={0} | all-to-all | bytes 262144 | tf_op jit(solution)/shard_map/all_to_all | solution.py:19
  74.1 0.7 copy-done.11
  74.8 1.9 %memory.1 = (bf16[16,8,128]{2,1,0:T(8,128)(2,1)S(1)}, f32[8,64,128]{2,1,0:T(8,128)}, f32[8,64]{1,0:T(8,128)}, f32[1,8]{1,0:T(1,128)}, bf16[264,512]{1,0:T(8,128)(2,1)S(1)}, /*index=5*/bf16[512,256]{1,0:T(8,128)(2,1)S(1)}) custom-call(bf16[16,8,512]{2,1,0:T(8,128)(2,1)S(1)} %all_to_all.41.tiles, f32[8,64,128]{2,1,0:T(8,128)S(1)} %bitcast.27, ...), custom_call_target="tpu_custom_call" | custom-call | tf_op jit(solution)/shard_map/memory/pallas_call | solution.py:217
  76.7 17.9 %all_to_all.42 = bf16[16,8,128]{2,1,0:T(8,128)(2,1)S(1)} all-to-all(bf16[16,8,128]{2,1,0:T(8,128)(2,1)S(1)} %get-tuple-element.25), channel_id=1, replica_groups=mesh['grp'=2,'kv_pair'=8,'kv_side'=2,'tp'=16] {'kv_pair','kv_side'}, dimensions={0} | all-to-all | bytes 65536 | tf_op jit(solution)/shard_map/all_to_all | solution.py:19
  94.6 0.1 fusion
  94.9 12.3 %all_to_all.43 = bf16[16,16,128]{2,1,0:T(8,128)(2,1)S(1)} all-to-all(bf16[16,16,128]{2,1,0:T(8,128)(2,1)S(1)} %bitcast.39), channel_id=1, replica_groups=mesh['grp'=2,'kv_pair'=8,'kv_side'=2,'tp'=16] {'tp'}, dimensions={0} | all-to-all | bytes 131072 | tf_op jit(solution)/shard_map/all_to_all | solution.py:19
  107.3 0.7 broadcast_in_dim.16
  107.9 4.2 %all-to-all-start.4 = ((bf16[32,16,128]{2,1,0:T(8,128)(2,1)}), bf16[32,16,128]{2,1,0:T(8,128)(2,1)S(1)}, u32[]{:S(2)}, u32[]{:S(2)}) async-start(bf16[32,16,128]{2,1,0:T(8,128)(2,1)} %broadcast_in_dim.16), calls=%async_computation.4 | async-start | bytes 262144 | tf_op jit(solution)/shard_map/all_to_all | solution.py:19
  112.1 3.5 %collective-permute-start = (bf16[264,512]{1,0:T(8,128)(2,1)S(1)}, bf16[264,512]{1,0:T(8,128)(2,1)S(1)}, u32[]{:S(2)}, u32[]{:S(2)}) collective-permute-start(bf16[264,512]{1,0:T(8,128)(2,1)S(1)} %get-tuple-element.29), channel_id=1, source_target_pairs={{0,16},{16,0},{1,17},{17,1},{2,18},{18,2},{3,19},{19,3},{4,20},{20... | collective-permute-start | bytes 811016 | tf_op jit(solution)/shard_map/ppermute | solution.py:292
  115.6 5.7 %collective-permute-done.taken = bf16[264,512]{1,0:T(8,128)(2,1)S(1)} collective-permute-done((bf16[264,512]{1,0:T(8,128)(2,1)S(1)}, bf16[264,512]{1,0:T(8,128)(2,1)S(1)}, u32[]{:S(2)}, u32[]{:S(2)}) %collective-permute-start) | collective-permute-done | bytes 270368 | tf_op jit(solution)/shard_map/ppermute | solution.py:292
  121.4 1.0 shard_map.192
  122.3 3.7 %all-to-all-start.5 = ((bf16[8,16,640]{2,1,0:T(8,128)(2,1)}), bf16[8,16,640]{2,1,0:T(8,128)(2,1)S(1)}, u32[]{:S(2)}, u32[]{:S(2)}) async-start(bf16[8,16,640]{2,1,0:T(8,128)(2,1)} %shard_map.192), calls=%async_computation.5 | async-start | bytes 327680 | tf_op jit(solution)/shard_map/all_to_all | solution.py:19
  126.1 3.8 %collective-permute-start.1 = (bf16[512,256]{1,0:T(8,128)(2,1)S(1)}, bf16[512,256]{1,0:T(8,128)(2,1)S(1)}, u32[]{:S(2)}, u32[]{:S(2)}) collective-permute-start(bf16[512,256]{1,0:T(8,128)(2,1)S(1)} %get-tuple-element.30), channel_id=1, source_target_pairs={{0,16},{16,0},{1,17},{17,1},{2,18},{18,2},{3,19},{19,3},{4,20},{20... | collective-permute-start | bytes 786440 | tf_op jit(solution)/shard_map/ppermute | solution.py:293
  129.9 9.5 %all-to-all-done.5 = bf16[8,16,640]{2,1,0:T(8,128)(2,1)S(1)} async-done(((bf16[8,16,640]{2,1,0:T(8,128)(2,1)}), bf16[8,16,640]{2,1,0:T(8,128)(2,1)S(1)}, u32[]{:S(2)}, u32[]{:S(2)}) %all-to-all-start.5) | async-done | bytes 163872 | tf_op jit(solution)/shard_map/all_to_all | solution.py:19
  139.4 0.2 fusion.7
  139.7 1.4 collective-permute-done.1.taken
  141.1 23.7 %all_to_all.44.hidden = bf16[8,16,512]{2,1,0:T(8,128)(2,1)S(1)} all-to-all(bf16[8,16,512]{2,1,0:T(8,128)(2,1)S(1)} %broadcast_in_dim.17), channel_id=1, replica_groups=mesh['grp'=2,'kv_pair'=8,'kv_side'=2,'tp'=16] {'kv_pair'}, dimensions={0} | all-to-all | bytes 262144 | tf_op jit(solution)/shard_map/all_to_all | solution.py:19
  164.8 0.3 shard_map.193
  165.1 18.9 %all_to_all.45 = bf16[32,16,128]{2,1,0:T(8,128)(2,1)S(1)} all-to-all(bf16[32,16,128]{2,1,0:T(8,128)(2,1)S(1)} %shard_map.193), channel_id=1, replica_groups=mesh['grp'=2,'kv_pair'=8,'kv_side'=2,'tp'=16] {'kv_side','tp'}, dimensions={0} | all-to-all | bytes 262144 | tf_op jit(solution)/shard_map/all_to_all | solution.py:19
  184.1 0.6 fusion.8
  (41 shorter events, 0.4 us)
Async XLA Ops:
  0.6 94.0 %copy-start = (bf16[128,256]{1,0:T(8,128)(2,1)S(1)}, bf16[128,256]{1,0:T(8,128)(2,1)}, u32[]{:S(2)}) copy-start(bf16[128,256]{1,0:T(8,128)(2,1)} %param.30) | copy-start | bytes 196612
  0.6 0.7 copy-start.16
  0.7 52.7 %copy-start.13 = (f32[8,1]{0,1:T(1,128)S(1)}, f32[8,1]{0,1:T(1,128)}, u32[]{:S(2)}) copy-start(f32[8,1]{0,1:T(1,128)} %param.29) | copy-start | bytes 100
  0.7 52.7 %copy-start.14 = (f32[16]{0:T(128)S(1)}, f32[16]{0:T(128)}, u32[]{:S(2)}) copy-start(f32[16]{0:T(128)} %param.25) | copy-start | bytes 196
  0.7 52.7 %copy-start.15 = (f32[16]{0:T(128)S(1)}, f32[16]{0:T(128)}, u32[]{:S(2)}) copy-start(f32[16]{0:T(128)} %param.26) | copy-start | bytes 196
  1.4 52.0 %copy-start.6 = (bf16[256,64]{0,1:T(8,128)(2,1)S(1)}, bf16[256,64]{0,1:T(8,128)(2,1)}, u32[]{:S(2)}) copy-start(bf16[256,64]{0,1:T(8,128)(2,1)} %param.19) | copy-start | bytes 98308
  1.4 52.0 %copy-start.7 = (bf16[256,64]{0,1:T(8,128)(2,1)S(1)}, bf16[256,64]{0,1:T(8,128)(2,1)}, u32[]{:S(2)}) copy-start(bf16[256,64]{0,1:T(8,128)(2,1)} %param.20) | copy-start | bytes 98308
  1.4 52.0 %copy-start.10 = (f32[8,1,64]{2,1,0:T(1,128)S(1)}, f32[8,1,64]{2,1,0:T(1,128)}, u32[]{:S(2)}) copy-start(f32[8,1,64]{2,1,0:T(1,128)} %param.28) | copy-start | bytes 6148
  1.4 52.0 %copy-start.4 = (bf16[256,128]{1,0:T(8,128)(2,1)S(1)}, bf16[256,128]{1,0:T(8,128)(2,1)}, u32[]{:S(2)}) copy-start(bf16[256,128]{1,0:T(8,128)(2,1)} %wv.1) | copy-start | bytes 196612
  1.4 52.0 %copy-start.5 = (bf16[256,128]{1,0:T(8,128)(2,1)S(1)}, bf16[256,128]{1,0:T(8,128)(2,1)}, u32[]{:S(2)}) copy-start(bf16[256,128]{1,0:T(8,128)(2,1)} %wo.1) | copy-start | bytes 196612
  53.3 0.7 copy-start.9
  53.3 0.7 copy-start.8
  53.3 0.7 copy-start.12
  54.0 20.1 %copy-start.3 = (f32[8,1,64,128]{3,2,1,0:T(8,128)S(1)}, f32[8,1,64,128]{3,2,1,0:T(8,128)}, u32[]{:S(2)}) copy-start(f32[8,1,64,128]{3,2,1,0:T(8,128)} %param.27) | copy-start | bytes 786436
  74.1 0.7 copy-start.11
  76.7 44.6 %copy-start.1 = (bf16[256,1024]{1,0:T(8,128)(2,1)S(1)}, bf16[256,1024]{1,0:T(8,128)(2,1)}, u32[]{:S(2)}) copy-start(bf16[256,1024]{1,0:T(8,128)(2,1)} %w_up.3) | copy-start | bytes 1572868
  107.9 13.4 %all-to-all-start.4 = ((bf16[32,16,128]{2,1,0:T(8,128)(2,1)}), bf16[32,16,128]{2,1,0:T(8,128)(2,1)S(1)}, u32[]{:S(2)}, u32[]{:S(2)}) async-start(bf16[32,16,128]{2,1,0:T(8,128)(2,1)} %broadcast_in_dim.16), calls=%async_computation.4 | async-start | bytes 262144 | tf_op jit(solution)/shard_map/all_to_all | solution.py:19
  112.1 9.3 %collective-permute-start = (bf16[264,512]{1,0:T(8,128)(2,1)S(1)}, bf16[264,512]{1,0:T(8,128)(2,1)S(1)}, u32[]{:S(2)}, u32[]{:S(2)}) collective-permute-start(bf16[264,512]{1,0:T(8,128)(2,1)S(1)} %get-tuple-element.29), channel_id=1, source_target_pairs={{0,16},{16,0},{1,17},{17,1},{2,18},{18,2},{3,19},{19,3},{4,20},{20... | collective-permute-start | bytes 811016 | tf_op jit(solution)/shard_map/ppermute | solution.py:292
  122.3 42.5 %copy-start.2 = (bf16[1024,256]{1,0:T(8,128)(2,1)S(1)}, bf16[1024,256]{1,0:T(8,128)(2,1)}, u32[]{:S(2)}) copy-start(bf16[1024,256]{1,0:T(8,128)(2,1)} %w_down.3) | copy-start | bytes 1572868
  122.3 17.1 %all-to-all-start.5 = ((bf16[8,16,640]{2,1,0:T(8,128)(2,1)}), bf16[8,16,640]{2,1,0:T(8,128)(2,1)S(1)}, u32[]{:S(2)}, u32[]{:S(2)}) async-start(bf16[8,16,640]{2,1,0:T(8,128)(2,1)} %shard_map.192), calls=%async_computation.5 | async-start | bytes 327680 | tf_op jit(solution)/shard_map/all_to_all | solution.py:19
  126.1 15.1 %collective-permute-start.1 = (bf16[512,256]{1,0:T(8,128)(2,1)S(1)}, bf16[512,256]{1,0:T(8,128)(2,1)S(1)}, u32[]{:S(2)}, u32[]{:S(2)}) collective-permute-start(bf16[512,256]{1,0:T(8,128)(2,1)S(1)} %get-tuple-element.30), channel_id=1, source_target_pairs={{0,16},{16,0},{1,17},{17,1},{2,18},{18,2},{3,19},{19,3},{4,20},{20... | collective-permute-start | bytes 786440 | tf_op jit(solution)/shard_map/ppermute | solution.py:293

commit v5 on v4

--- a/solution.py
+++ b/solution.py
@@ -33,41 +33,70 @@
     return high, (value - high).astype(jnp.bfloat16).astype(jnp.float32)
 
 
-def project_body(
-    tokens, gain, pick, norm, top, bias_in, bias_forget,
-    wq, wk, wv, wo, wi, wf, out, aux, residual,
+def stage_body(
+    width, tokens, gain_in, gain_mid, wi, wf, bias_in, bias_forget, norm, top, wq, wk,
+    copies, gates, aux, residual, gains, first_gain, second_gain, both_qk,
+    own, wi_buf, wf_buf, bias_in_buf, bias_forget_buf, norm_buf, top_buf, sems,
 ):
-    gain, pick = gain[...], pick[...]
-    mine = jnp.zeros(residual.shape, jnp.float32)
-    for peer in range(tokens.shape[0]):
-        mine += tokens[peer].astype(jnp.float32) * pick[:, peer : peer + 1]
-    residual[...] = mine
-    count, key_dim = norm.shape
-    place = lax.broadcasted_iota(jnp.int32, (count, LANES - key_dim), 1)
-    first = jnp.sum(bias_in[...] * pick, axis=1, keepdims=True)
-    second = jnp.sum(bias_forget[...] * pick, axis=1, keepdims=True)
+    moves = (
+        (tokens, own), (gain_in, first_gain), (gain_mid, second_gain), (wi, wi_buf), (wf, wf_buf),
+        (bias_in, bias_in_buf), (bias_forget, bias_forget_buf), (norm, norm_buf), (top, top_buf),
+        (wq, both_qk.at[pl.ds(0, wq.shape[0])]), (wk, both_qk.at[pl.ds(wq.shape[0], wk.shape[0])]),
+    )
+    moves = [
+        pltpu.make_async_copy(source, target, sems.at[at])
+        for at, (source, target) in enumerate(moves)
+    ]
+    for move in moves:
+        move.start()
+    for move in moves:
+        move.wait()
+    head = lax.axis_index("tp")
+    value = own[...]
+    for peer in range(copies.shape[0]):
+        copies[peer] = value
+    residual[...] = value.astype(jnp.float32)
+    heads, rows = wi_buf.shape
+    count, key_dim = norm_buf.shape
+    down = lax.broadcasted_iota(jnp.int32, (heads, rows), 0) == head
+    line = lax.broadcasted_iota(jnp.int32, (8, rows), 0)
+    picked = [
+        jnp.sum(jnp.where(down, w[...].astype(jnp.float32), 0.0), axis=0, keepdims=True)
+        for w in (wi_buf, wf_buf)
+    ]
+    both = jnp.where(line == 0, picked[0], jnp.where(line == 1, picked[1], 0.0))
+    gates[...] = both.astype(jnp.bfloat16)
+    high, low = two_parts(second_gain[...])
+    both = jnp.where(line == 0, high, jnp.where(line == 1, low, 0.0))
+    gains[...] = both.astype(jnp.bfloat16)
+    along = lax.broadcasted_iota(jnp.int32, (1, heads), 1) == head
+    place = lax.broadcasted_iota(jnp.int32, (count, width - key_dim), 1)
+    first, second = [
+        jnp.sum(jnp.where(along, b[...], 0.0), axis=1, keepdims=True)
+        for b in (bias_in_buf, bias_forget_buf)
+    ]
     eye = lax.broadcasted_iota(jnp.int32, (count, count), 0)
     eye = eye == lax.broadcasted_iota(jnp.int32, (count, count), 1)
-    turned = jnp.sum(jnp.where(eye, top[...], 0.0), axis=1, keepdims=True)
+    turned = jnp.sum(jnp.where(eye, top_buf[...], 0.0), axis=1, keepdims=True)
     rest = jnp.where(place == 1, first, jnp.where(place == 2, second, 0.0))
     rest = jnp.where(place == 0, turned, rest)
-    aux[...] = jnp.concatenate([norm[...], rest], axis=1)
+    aux[...] = jnp.concatenate([norm_buf[...], rest], axis=1)
+
+
+def project_body(tokens, gain, gates, wqk, wv, wo, out):
     wide = tokens[...].reshape(-1, tokens.shape[-1]).astype(jnp.float32).T
     squares = jnp.sum(wide * wide, axis=1, keepdims=True)
-    normed = (wide * gain).astype(jnp.bfloat16)
-    query = contract(normed, wq[...], 1, 1)
-    keys = contract(normed, wk[...], 1, 1)
+    normed = (wide * gain[...]).astype(jnp.bfloat16)
+    both = contract(normed, wqk[...], 1, 1)
     values = contract(normed, wv[...], 1, 0)
     outgate = contract(normed, wo[...], 1, 0)
-    gate_in = jnp.sum(contract(normed, wi[...], 1, 1) * pick, axis=1, keepdims=True)
-    gate_forget = jnp.sum(contract(normed, wf[...], 1, 1) * pick, axis=1, keepdims=True)
+    gate = contract(normed, gates[...], 1, 1)
     lane = lax.broadcasted_iota(jnp.int32, (wide.shape[0], LANES), 1)
     extra = jnp.zeros((wide.shape[0], LANES), jnp.float32)
-    for place, value in enumerate((gate_in, gate_forget, squares)):
+    for place, value in enumerate((gate[:, 0:1], gate[:, 1:2], squares)):
         high, low = two_parts(value)
         extra = jnp.where(lane == place, high, extra)
         extra = jnp.where(lane == place + 3, low, extra)
-    both = jnp.concatenate([query, keys], axis=1)
     peers, own, _ = out.shape
     at = 0
     for piece in (both, values, outgate, extra):
@@ -78,7 +107,7 @@
 
 
 def memory_body(
-    width, tiles, cell, aux, gain, w_up, w_down,
+    width, tiles, cell, aux, gains, w_up, w_down,
     heads, cell_out, norm_out, top_out, sent_up, sent_down, cell_new, norm_buf, top_buf, sems,
 ):
     rows, columns = w_up.shape
@@ -93,10 +122,7 @@
     ]
     for copy in copies:
         copy.start()
-    high, low = two_parts(gain[...])
-    line = lax.broadcasted_iota(jnp.int32, (8, rows), 0)
-    both = jnp.where(line == 0, high, jnp.where(line == 1, low, 0.0))
-    sent_up[rows:, :rows] = both.astype(jnp.bfloat16)
+    sent_up[rows:, :rows] = gains[...]
     sent_up[rows:, rows:] = jnp.zeros((8, half - rows), jnp.bfloat16)
     own, key_dim, _ = cell.shape
     terms = jnp.sum(tiles[...].astype(jnp.float32), axis=0)
@@ -158,14 +184,41 @@
     theirs = (theirs * (gains[0:1] + gains[1:2])).astype(jnp.bfloat16)
     upward = contract(mine, w_up[:, pl.ds(pl.multiple_of(side * half, half), half)], 1, 0)
     upward = upward + contract(theirs, taken[:rows], 1, 0)
-    lane = lax.broadcasted_iota(jnp.int32, (mine.shape[0], LANES), 1)
     high, low = two_parts(squares)
-    extra = jnp.where(lane == 0, high, jnp.where(lane == 1, low, 0.0)).astype(jnp.bfloat16)
     upward = upward.astype(jnp.bfloat16)
-    peers, own, _ = out.shape
+    peers, tiles, lines, lanes = out.shape
+    across = half // lanes
+    own = (tiles - 1) // across * lines
+    lane = lax.broadcasted_iota(jnp.int32, (lines, lanes), 1)
     for peer in range(peers):
-        out[peer, :, :half] = upward[peer * own : (peer + 1) * own]
-        out[peer, :, half:] = extra[peer * own : (peer + 1) * own]
+        extra = jnp.zeros((lines, lanes), jnp.float32)
+        for part in range(own // lines):
+            at = peer * own + part * lines
+            for tile in range(across):
+                out[peer, part * across + tile] = upward[
+                    at : at + lines, tile * lanes : (tile + 1) * lanes
+                ]
+            extra = jnp.where(lane == 2 * part, high[at : at + lines], extra)
+            extra = jnp.where(lane == 2 * part + 1, low[at : at + lines], extra)
+        out[peer, tiles - 1] = extra.astype(jnp.bfloat16)
+
+
+def hidden_body(width, tiles, copies):
+    terms = jnp.sum(tiles[...].astype(jnp.float32), axis=0)
+    count, lines, lanes = terms.shape
+    peers, own, half = copies.shape
+    across = half // lanes
+    for part in range(own // lines):
+        total = terms[count - 1, :, 2 * part : 2 * part + 1]
+        total = total + terms[count - 1, :, 2 * part + 1 : 2 * part + 2]
+        scale = lax.rsqrt(total / width + EPSILON)
+        for tile in range(across):
+            upward = jnp.maximum(terms[part * across + tile] * scale, 0.0)
+            upward = (upward * upward).astype(jnp.bfloat16)
+            for peer in range(peers):
+                copies[
+                    peer, part * lines : (part + 1) * lines, tile * lanes : (tile + 1) * lanes
+                ] = upward
 
 
 def down_body(hidden, w_down, taken, out):
@@ -190,25 +243,32 @@
     )(*on_chip(*operands))
 
 
-def project(tokens, small, weights, peers):
-    seqs = tokens.shape[-1]
-    own = seqs // peers
+def stage(operands, peers):
+    tokens, gain = operands[0], operands[1]
+    wi, norm = operands[3], operands[7]
     vmem = pl.BlockSpec(memory_space=pltpu.VMEM)
-    operands = on_chip(tokens, *small, *weights)
+    out_shape = (
+        pltpu.VMEM((peers, *tokens.shape), jnp.bfloat16),
+        pltpu.VMEM((8, wi.shape[1]), jnp.bfloat16),
+        pltpu.VMEM((norm.shape[0], LANES), jnp.float32),
+        pltpu.VMEM(tokens.shape, jnp.float32),
+        pltpu.VMEM((8, wi.shape[1]), jnp.bfloat16),
+        pltpu.VMEM(gain.shape, jnp.float32),
+        pltpu.VMEM(gain.shape, jnp.float32),
+        pltpu.VMEM((operands[9].shape[0] + operands[10].shape[0], wi.shape[1]), jnp.bfloat16),
+    )
+    scratch = [pltpu.VMEM(a.shape, a.dtype) for a in (tokens, *operands[3:9])]
     return pl.pallas_call(
-        project_body,
-        out_shape=(
-            pltpu.VMEM((peers, own, 4 * LANES), jnp.bfloat16),
-            pltpu.VMEM((own, LANES), jnp.float32),
-            pltpu.VMEM(tokens.shape[1:], jnp.float32),
-        ),
-        in_specs=[vmem] * len(operands),
-        out_specs=(vmem,) * 3,
-        name="project",
+        functools.partial(stage_body, LANES),
+        out_shape=out_shape,
+        in_specs=[pl.BlockSpec(memory_space=pl.ANY)] * len(operands),
+        out_specs=(vmem,) * len(out_shape),
+        scratch_shapes=[*scratch, pltpu.SemaphoreType.DMA((len(operands),))],
+        name="stage",
     )(*operands)
 
 
-def memory_step(tiles, cell, aux, gain, w_up, w_down, width):
+def memory_step(tiles, cell, aux, gains, w_up, w_down, width):
     peers, own, _ = tiles.shape
     _, key_dim, value_dim = cell.shape
     rows, columns = w_up.shape
@@ -233,7 +293,7 @@
             pltpu.SemaphoreType.DMA((own + 4,)),
         ],
         name="memory",
-    )(*on_chip(tiles, cell, aux, gain), w_up, w_down)
+    )(*on_chip(tiles, cell, aux, gains), w_up, w_down)
 
 
 def layer(
@@ -264,27 +324,36 @@
     width = rows * kv
     own = seqs // kv
     heads_all = w_input_gate.shape[1]
-    is_head = lax.broadcasted_iota(jnp.int32, (1, heads_all), 1) == lax.axis_index("tp")
-    pick = is_head.astype(jnp.float32)
-
-    gain_mid = gain_mid.reshape(1, rows)
     swap = [(0, 1), (1, 0)]
 
-    copies = jnp.broadcast_to(tokens.T, (tp, own_columns, seqs))
-    copies, pick = lax.optimization_barrier((copies, pick))
-    gathered = exchange(copies, "tp")
-    small = (
-        gain_in.reshape(1, rows),
-        pick,
-        norm_state[:, 0],
-        max_state.reshape(1, own),
-        bias_input.reshape(1, heads_all),
-        bias_forget.reshape(1, heads_all),
-    )
-    weights = (w_query.T, w_key.T, w_value, w_outgate, w_input_gate.T, w_forget_gate.T)
-    terms, aux, residual = project(gathered, small, weights, kv)
+    copies, gates, aux, residual, gains, gain_in, gain_mid, w_qk = stage(
+        (
+            tokens.T,
+            gain_in.reshape(1, rows),
+            gain_mid.reshape(1, rows),
+            w_input_gate.T,
+            w_forget_gate.T,
+            bias_input.reshape(1, heads_all),
+            bias_forget.reshape(1, heads_all),
+            norm_state[:, 0],
+            max_state.reshape(1, own),
+            w_query.T,
+            w_key.T,
+        ),
+        tp,
+    )
+    terms = in_vmem(
+        project_body,
+        (kv, own, 4 * LANES),
+        exchange(copies, "tp"),
+        gain_in,
+        gates,
+        w_qk,
+        w_value,
+        w_outgate,
+    )
     heads, cell_new, norm_new, max_new, sent_up, sent_down = memory_step(
-        exchange(terms, KV), cell_state[:, 0], aux, gain_mid, w_up, w_down, width
+        exchange(terms, KV), cell_state[:, 0], aux, gains, w_up, w_down, width
     )
 
     heads = exchange(heads, KV).reshape(seqs, value_dim)
@@ -296,15 +365,12 @@
     own_middle = residual + jnp.sum(branch.astype(jnp.float32), axis=0)
     own_middle = own_middle.astype(jnp.bfloat16)
     middle = spread(own_middle, ("kv_side", "tp"))
-    upward = in_vmem(up_body, (pairs, 2 * own, half + LANES), middle, gain_mid, w_up, other_up)
+    tiles = 2 * own * half // (8 * LANES) + 1
+    upward = in_vmem(up_body, (pairs, tiles, 8, LANES), middle, gain_mid, w_up, other_up)
     upward = exchange(upward, "kv_pair")
-    upward = jnp.sum(upward.astype(jnp.float32), axis=0)
-    total = upward[:, half : half + 1] + upward[:, half + 1 : half + 2]
-    scale_mid = lax.rsqrt(total / width + EPSILON)
-    hidden = jnp.square(jax.nn.relu(upward[:, :half] * scale_mid)).astype(jnp.bfloat16)
-
-    hidden, other_down = lax.optimization_barrier((hidden, other_down))
-    hidden = spread(hidden, "kv_pair")
+    copies = in_vmem(functools.partial(hidden_body, width), (pairs, 2 * own, half), upward)
+    copies, other_down = lax.optimization_barrier((copies, other_down))
+    hidden = exchange(copies, "kv_pair")
     down = in_vmem(down_body, (2 * tp, own_columns, seqs), hidden, w_down, other_down)
     down = exchange(down, ("kv_side", "tp"))
     mixed = own_middle.astype(jnp.float32) + jnp.sum(down.astype(jnp.float32), axis=0)

time: 185 us -> 184 us (level)
  local copies, waits for them, and re-layouts: 2.84 us -> 0.82 us
    unnamed x34 -> x12, local copies, waits for them, and re-layouts: 2.04 us -> 0.04 us
where the time goes in v5:
time: 184 us; the launch traced here: 183 us
  blocking collectives  144 us (78%)
  waiting for transfers between devices  16.4 us (9%)
  starting transfers between devices  15.2 us (8%)
  Pallas kernels  4.92 us (3%)
    all_to_all x6, blocking collectives, exchange(): return lax.all_to_all(tiles, axis, split_axis=0, concat_axis=0, tiled=True)  144 us
    all_to_all x2, waiting for transfers between devices, exchange(): return lax.all_to_all(tiles, axis, split_axis=0, concat_axis=0, tiled=True)  9.45 us
    all_to_all x2, starting transfers between devices, exchange(): return lax.all_to_all(tiles, axis, split_axis=0, concat_axis=0, tiled=True)  7.88 us
    ppermute x1, waiting for transfers between devices, layer(): other_up = lax.ppermute(sent_up, 'kv_side', swap)  5.75 us
    ppermute x1, starting transfers between devices, layer(): other_down = lax.ppermute(sent_down, 'kv_side', swap)  3.83 us
  transfers between devices with their start and end apart: 4, of which 3 were waited for; matrix products, arithmetic and copies ran while one was open for 0% of the time, Pallas kernels for 0%

profile of v5, /device:TPU:65, one launch (start us, length us, event | category | flops | bytes accessed | tf_op | source)
XLA Modules:
  0.0 183.1 jit_solution(6940032083301761196)
XLA Ops:
  0.6 0.0 copy-start
  0.7 1.2 stage.1
  1.9 51.9 %all_to_all.40.tokens = bf16[16,16,128]{2,1,0:T(8,128)(2,1)S(1)} all-to-all(bf16[16,16,128]{2,1,0:T(8,128)(2,1)S(1)} %get-tuple-element.24), channel_id=1, replica_groups=mesh['grp'=2,'kv_pair'=8,'kv_side'=2,'tp'=16] {'tp'}, dimensions={0} | all-to-all | bytes 131072 | tf_op jit(solution)/shard_map/all_to_all | solution.py:19
  53.8 0.4 shard_map.192
  54.2 19.7 %all_to_all.41.tiles = bf16[16,8,512]{2,1,0:T(8,128)(2,1)S(1)} all-to-all(bf16[16,8,512]{2,1,0:T(8,128)(2,1)S(1)} %shard_map.192), channel_id=1, replica_groups=mesh['grp'=2,'kv_pair'=8,'kv_side'=2,'tp'=16] {'kv_pair','kv_side'}, dimensions={0} | all-to-all | bytes 262144 | tf_op jit(solution)/shard_map/all_to_all | solution.py:19
  73.8 1.9 %memory.1 = (bf16[16,8,128]{2,1,0:T(8,128)(2,1)S(1)}, f32[8,64,128]{2,1,0:T(8,128)}, f32[8,64]{1,0:T(8,128)}, f32[1,8]{1,0:T(1,128)}, bf16[264,512]{1,0:T(8,128)(2,1)S(1)}, /*index=5*/bf16[512,256]{1,0:T(8,128)(2,1)S(1)}) custom-call(bf16[16,8,512]{2,1,0:T(8,128)(2,1)S(1)} %all_to_all.41.tiles, f32[8,64,128]{2,1,0:T(8,128)S(1)} %bitcast.27, ...), custom_call_target="tpu_custom_call" | custom-call | tf_op jit(solution)/shard_map/memory/pallas_call | solution.py:277
  75.8 17.9 %all_to_all.42 = bf16[16,8,128]{2,1,0:T(8,128)(2,1)S(1)} all-to-all(bf16[16,8,128]{2,1,0:T(8,128)(2,1)S(1)} %get-tuple-element.30), channel_id=1, replica_groups=mesh['grp'=2,'kv_pair'=8,'kv_side'=2,'tp'=16] {'kv_pair','kv_side'}, dimensions={0} | all-to-all | bytes 65536 | tf_op jit(solution)/shard_map/all_to_all | solution.py:19
  93.7 0.1 fusion
  93.8 0.1 copy.23
  94.0 12.3 %all_to_all.43 = bf16[16,16,128]{2,1,0:T(8,128)(2,1)S(1)} all-to-all(bf16[16,16,128]{2,1,0:T(8,128)(2,1)S(1)} %bitcast.28), channel_id=1, replica_groups=mesh['grp'=2,'kv_pair'=8,'kv_side'=2,'tp'=16] {'tp'}, dimensions={0} | all-to-all | bytes 131072 | tf_op jit(solution)/shard_map/all_to_all | solution.py:19
  106.3 0.7 broadcast_in_dim.9
  107.0 4.2 %all-to-all-start.4 = ((bf16[32,16,128]{2,1,0:T(8,128)(2,1)}), bf16[32,16,128]{2,1,0:T(8,128)(2,1)S(1)}, u32[]{:S(2)}, u32[]{:S(2)}) async-start(bf16[32,16,128]{2,1,0:T(8,128)(2,1)} %broadcast_in_dim.9), calls=%async_computation.4 | async-start | bytes 262144 | tf_op jit(solution)/shard_map/all_to_all | solution.py:19
  111.1 3.5 %collective-permute-start = (bf16[264,512]{1,0:T(8,128)(2,1)S(1)}, bf16[264,512]{1,0:T(8,128)(2,1)S(1)}, u32[]{:S(2)}, u32[]{:S(2)}) collective-permute-start(bf16[264,512]{1,0:T(8,128)(2,1)S(1)} %get-tuple-element.35), channel_id=1, source_target_pairs={{0,16},{16,0},{1,17},{17,1},{2,18},{18,2},{3,19},{19,3},{4,20},{20... | collective-permute-start | bytes 811016 | tf_op jit(solution)/shard_map/ppermute | solution.py:361
  114.7 5.7 %collective-permute-done.taken = bf16[264,512]{1,0:T(8,128)(2,1)S(1)} collective-permute-done((bf16[264,512]{1,0:T(8,128)(2,1)S(1)}, bf16[264,512]{1,0:T(8,128)(2,1)S(1)}, u32[]{:S(2)}, u32[]{:S(2)}) %collective-permute-start) | collective-permute-done | bytes 270368 | tf_op jit(solution)/shard_map/ppermute | solution.py:361
  120.4 0.9 shard_map.193
  121.4 3.7 %all-to-all-start.5 = ((bf16[8,9,8,128]{3,2,1,0:T(8,128)(2,1)}), bf16[8,9,8,128]{3,2,1,0:T(8,128)(2,1)S(1)}, u32[]{:S(2)}, u32[]{:S(2)}) async-start(bf16[8,9,8,128]{3,2,1,0:T(8,128)(2,1)} %shard_map.193), calls=%async_computation.5 | async-start | bytes 294912 | tf_op jit(solution)/shard_map/all_to_all | solution.py:19
  125.1 3.8 %collective-permute-start.1 = (bf16[512,256]{1,0:T(8,128)(2,1)S(1)}, bf16[512,256]{1,0:T(8,128)(2,1)S(1)}, u32[]{:S(2)}, u32[]{:S(2)}) collective-permute-start(bf16[512,256]{1,0:T(8,128)(2,1)S(1)} %get-tuple-element.36), channel_id=1, source_target_pairs={{0,16},{16,0},{1,17},{17,1},{2,18},{18,2},{3,19},{19,3},{4,20},{20... | collective-permute-start | bytes 786440 | tf_op jit(solution)/shard_map/ppermute | solution.py:362
  128.9 9.4 %all-to-all-done.5.tiles = bf16[8,9,8,128]{3,2,1,0:T(8,128)(2,1)S(1)} async-done(((bf16[8,9,8,128]{3,2,1,0:T(8,128)(2,1)}), bf16[8,9,8,128]{3,2,1,0:T(8,128)(2,1)S(1)}, u32[]{:S(2)}, u32[]{:S(2)}) %all-to-all-start.5) | async-done | bytes 147488 | tf_op jit(solution)/shard_map/all_to_all | solution.py:19
  138.4 0.2 shard_map.194
  138.5 1.2 collective-permute-done.1.taken
  139.7 23.2 %all_to_all.44.hidden = bf16[8,16,512]{2,1,0:T(8,128)(2,1)S(1)} all-to-all(bf16[8,16,512]{2,1,0:T(8,128)(2,1)S(1)} %shard_map.194), channel_id=1, replica_groups=mesh['grp'=2,'kv_pair'=8,'kv_side'=2,'tp'=16] {'kv_pair'}, dimensions={0} | all-to-all | bytes 262144 | tf_op jit(solution)/shard_map/all_to_all | solution.py:19
  162.9 0.3 shard_map.195
  163.2 19.3 %all_to_all.45 = bf16[32,16,128]{2,1,0:T(8,128)(2,1)S(1)} all-to-all(bf16[32,16,128]{2,1,0:T(8,128)(2,1)S(1)} %shard_map.195), channel_id=1, replica_groups=mesh['grp'=2,'kv_pair'=8,'kv_side'=2,'tp'=16] {'kv_side','tp'}, dimensions={0} | all-to-all | bytes 262144 | tf_op jit(solution)/shard_map/all_to_all | solution.py:19
  182.5 0.6 fusion.1
  (15 shorter events, 0.1 us)
Async XLA Ops:
  0.6 93.1 %copy-start = (bf16[128,256]{1,0:T(8,128)(2,1)S(1)}, bf16[128,256]{1,0:T(8,128)(2,1)}, u32[]{:S(2)}) copy-start(bf16[128,256]{1,0:T(8,128)(2,1)} %param.30) | copy-start | bytes 196612
  1.8 51.9 %copy-start.4 = (bf16[256,128]{1,0:T(8,128)(2,1)S(1)}, bf16[256,128]{1,0:T(8,128)(2,1)}, u32[]{:S(2)}) copy-start(bf16[256,128]{1,0:T(8,128)(2,1)} %wv.1) | copy-start | bytes 196612
  1.9 51.9 %copy-start.5 = (bf16[256,128]{1,0:T(8,128)(2,1)S(1)}, bf16[256,128]{1,0:T(8,128)(2,1)}, u32[]{:S(2)}) copy-start(bf16[256,128]{1,0:T(8,128)(2,1)} %wo.1) | copy-start | bytes 196612
  53.8 20.1 %copy-start.3 = (f32[8,1,64,128]{3,2,1,0:T(8,128)S(1)}, f32[8,1,64,128]{3,2,1,0:T(8,128)}, u32[]{:S(2)}) copy-start(f32[8,1,64,128]{3,2,1,0:T(8,128)} %param.27) | copy-start | bytes 786436
  75.8 44.7 %copy-start.1 = (bf16[256,1024]{1,0:T(8,128)(2,1)S(1)}, bf16[256,1024]{1,0:T(8,128)(2,1)}, u32[]{:S(2)}) copy-start(bf16[256,1024]{1,0:T(8,128)(2,1)} %w_up.3) | copy-start | bytes 1572868
  107.0 13.4 %all-to-all-start.4 = ((bf16[32,16,128]{2,1,0:T(8,128)(2,1)}), bf16[32,16,128]{2,1,0:T(8,128)(2,1)S(1)}, u32[]{:S(2)}, u32[]{:S(2)}) async-start(bf16[32,16,128]{2,1,0:T(8,128)(2,1)} %broadcast_in_dim.9), calls=%async_computation.4 | async-start | bytes 262144 | tf_op jit(solution)/shard_map/all_to_all | solution.py:19
  111.1 9.3 %collective-permute-start = (bf16[264,512]{1,0:T(8,128)(2,1)S(1)}, bf16[264,512]{1,0:T(8,128)(2,1)S(1)}, u32[]{:S(2)}, u32[]{:S(2)}) collective-permute-start(bf16[264,512]{1,0:T(8,128)(2,1)S(1)} %get-tuple-element.35), channel_id=1, source_target_pairs={{0,16},{16,0},{1,17},{17,1},{2,18},{18,2},{3,19},{19,3},{4,20},{20... | collective-permute-start | bytes 811016 | tf_op jit(solution)/shard_map/ppermute | solution.py:361
  121.4 41.5 %copy-start.2 = (bf16[1024,256]{1,0:T(8,128)(2,1)S(1)}, bf16[1024,256]{1,0:T(8,128)(2,1)}, u32[]{:S(2)}) copy-start(bf16[1024,256]{1,0:T(8,128)(2,1)} %w_down.3) | copy-start | bytes 1572868
  121.4 17.0 %all-to-all-start.5 = ((bf16[8,9,8,128]{3,2,1,0:T(8,128)(2,1)}), bf16[8,9,8,128]{3,2,1,0:T(8,128)(2,1)S(1)}, u32[]{:S(2)}, u32[]{:S(2)}) async-start(bf16[8,9,8,128]{3,2,1,0:T(8,128)(2,1)} %shard_map.193), calls=%async_computation.5 | async-start | bytes 294912 | tf_op jit(solution)/shard_map/all_to_all | solution.py:19
  125.1 14.6 %collective-permute-start.1 = (bf16[512,256]{1,0:T(8,128)(2,1)S(1)}, bf16[512,256]{1,0:T(8,128)(2,1)S(1)}, u32[]{:S(2)}, u32[]{:S(2)}) collective-permute-start(bf16[512,256]{1,0:T(8,128)(2,1)S(1)} %get-tuple-element.36), channel_id=1, source_target_pairs={{0,16},{16,0},{1,17},{17,1},{2,18},{18,2},{3,19},{19,3},{4,20},{20... | collective-permute-start | bytes 786440 | tf_op jit(solution)/shard_map/ppermute | solution.py:362

commit v6 on v5

--- a/solution.py
+++ b/solution.py
@@ -203,10 +203,10 @@
         out[peer, tiles - 1] = extra.astype(jnp.bfloat16)
 
 
-def hidden_body(width, tiles, copies):
+def hidden_body(width, tiles, out):
     terms = jnp.sum(tiles[...].astype(jnp.float32), axis=0)
     count, lines, lanes = terms.shape
-    peers, own, half = copies.shape
+    own, half = out.shape
     across = half // lanes
     for part in range(own // lines):
         total = terms[count - 1, :, 2 * part : 2 * part + 1]
@@ -214,18 +214,16 @@
         scale = lax.rsqrt(total / width + EPSILON)
         for tile in range(across):
             upward = jnp.maximum(terms[part * across + tile] * scale, 0.0)
-            upward = (upward * upward).astype(jnp.bfloat16)
-            for peer in range(peers):
-                copies[
-                    peer, part * lines : (part + 1) * lines, tile * lanes : (tile + 1) * lanes
-                ] = upward
+            out[part * lines : (part + 1) * lines, tile * lanes : (tile + 1) * lanes] = (
+                upward * upward
+            ).astype(jnp.bfloat16)
 
 
 def down_body(hidden, w_down, taken, out):
     side = lax.axis_index("kv_side")
-    half = hidden.shape[2]
+    half = hidden.shape[1]
     count = out.shape[0] // 2
-    left = hidden[...].reshape(-1, half)
+    left = hidden[...]
     mine = contract(left, w_down[pl.ds(pl.multiple_of(side * half, half), half)], 1, 0)
     theirs = contract(left, taken[...], 1, 0)
     shape = (count, *out.shape[1:])
@@ -368,9 +366,9 @@
     tiles = 2 * own * half // (8 * LANES) + 1
     upward = in_vmem(up_body, (pairs, tiles, 8, LANES), middle, gain_mid, w_up, other_up)
     upward = exchange(upward, "kv_pair")
-    copies = in_vmem(functools.partial(hidden_body, width), (pairs, 2 * own, half), upward)
-    copies, other_down = lax.optimization_barrier((copies, other_down))
-    hidden = exchange(copies, "kv_pair")
+    hidden = in_vmem(functools.partial(hidden_body, width), (2 * own, half), upward)
+    hidden, other_down = lax.optimization_barrier((hidden, other_down))
+    hidden = lax.all_gather(hidden, "kv_pair", axis=0, tiled=True)
     down = in_vmem(down_body, (2 * tp, own_columns, seqs), hidden, w_down, other_down)
     down = exchange(down, ("kv_side", "tp"))
     mixed = own_middle.astype(jnp.float32) + jnp.sum(down.astype(jnp.float32), axis=0)

time: 184 us -> 189 us (1.027)
  blocking collectives: 144 us -> 150 us
    all_gather x0 -> x1, blocking collectives: none -> 24.9 us  [layer(): hidden = lax.all_gather(hidden, 'kv_pair', axis=0, tiled=True)]
    all_to_all x6 -> x5, blocking collectives: 144 us -> 125 us  [exchange(): return lax.all_to_all(tiles, axis, split_axis=0, concat_axis=0, tiled=True)]
where the time goes in v6:
time: 189 us
  blocking collectives  150 us (79%)
  waiting for transfers between devices  16.4 us (9%)
  starting transfers between devices  15.2 us (8%)
  Pallas kernels  4.91 us (3%)
    all_to_all x5, blocking collectives, exchange(): return lax.all_to_all(tiles, axis, split_axis=0, concat_axis=0, tiled=True)  125 us
    all_gather x1, blocking collectives, layer(): hidden = lax.all_gather(hidden, 'kv_pair', axis=0, tiled=True)  24.9 us
    all_to_all x2, waiting for transfers between devices, exchange(): return lax.all_to_all(tiles, axis, split_axis=0, concat_axis=0, tiled=True)  9.45 us
    all_to_all x2, starting transfers between devices, exchange(): return lax.all_to_all(tiles, axis, split_axis=0, concat_axis=0, tiled=True)  7.88 us
    ppermute x1, waiting for transfers between devices, layer(): other_up = lax.ppermute(sent_up, 'kv_side', swap)  5.75 us
    ppermute x1, starting transfers between devices, layer(): other_down = lax.ppermute(sent_down, 'kv_side', swap)  3.83 us
  transfers between devices with their start and end apart: 4, of which 3 were waited for; matrix products, arithmetic and copies ran while one was open for 0% of the time, Pallas kernels for 0%

profile of v6, /device:TPU:65, one launch (start us, length us, event | category | flops | bytes accessed | tf_op | source)
XLA Modules:
  0.0 188.7 jit_solution(16091370439206464653)
XLA Ops:
  0.6 0.0 copy-start
  0.7 1.2 stage.1
  1.9 51.9 %all_to_all.35.tokens = bf16[16,16,128]{2,1,0:T(8,128)(2,1)S(1)} all-to-all(bf16[16,16,128]{2,1,0:T(8,128)(2,1)S(1)} %get-tuple-element.24), channel_id=1, replica_groups=mesh['grp'=2,'kv_pair'=8,'kv_side'=2,'tp'=16] {'tp'}, dimensions={0} | all-to-all | bytes 131072 | tf_op jit(solution)/shard_map/all_to_all | solution.py:19
  53.8 0.4 shard_map.192
  54.2 19.7 %all_to_all.36.tiles = bf16[16,8,512]{2,1,0:T(8,128)(2,1)S(1)} all-to-all(bf16[16,8,512]{2,1,0:T(8,128)(2,1)S(1)} %shard_map.192), channel_id=1, replica_groups=mesh['grp'=2,'kv_pair'=8,'kv_side'=2,'tp'=16] {'kv_pair','kv_side'}, dimensions={0} | all-to-all | bytes 262144 | tf_op jit(solution)/shard_map/all_to_all | solution.py:19
  73.8 1.9 %memory.1 = (bf16[16,8,128]{2,1,0:T(8,128)(2,1)S(1)}, f32[8,64,128]{2,1,0:T(8,128)}, f32[8,64]{1,0:T(8,128)}, f32[1,8]{1,0:T(1,128)}, bf16[264,512]{1,0:T(8,128)(2,1)S(1)}, /*index=5*/bf16[512,256]{1,0:T(8,128)(2,1)S(1)}) custom-call(bf16[16,8,512]{2,1,0:T(8,128)(2,1)S(1)} %all_to_all.36.tiles, f32[8,64,128]{2,1,0:T(8,128)S(1)} %bitcast.27, ...), custom_call_target="tpu_custom_call" | custom-call | tf_op jit(solution)/shard_map/memory/pallas_call | solution.py:275
  75.8 17.9 %all_to_all.37 = bf16[16,8,128]{2,1,0:T(8,128)(2,1)S(1)} all-to-all(bf16[16,8,128]{2,1,0:T(8,128)(2,1)S(1)} %get-tuple-element.30), channel_id=1, replica_groups=mesh['grp'=2,'kv_pair'=8,'kv_side'=2,'tp'=16] {'kv_pair','kv_side'}, dimensions={0} | all-to-all | bytes 65536 | tf_op jit(solution)/shard_map/all_to_all | solution.py:19
  93.7 0.1 fusion
  93.8 0.1 copy.23
  94.0 12.3 %all_to_all.38 = bf16[16,16,128]{2,1,0:T(8,128)(2,1)S(1)} all-to-all(bf16[16,16,128]{2,1,0:T(8,128)(2,1)S(1)} %bitcast.28), channel_id=1, replica_groups=mesh['grp'=2,'kv_pair'=8,'kv_side'=2,'tp'=16] {'tp'}, dimensions={0} | all-to-all | bytes 131072 | tf_op jit(solution)/shard_map/all_to_all | solution.py:19
  106.3 0.7 broadcast_in_dim.9
  107.0 4.2 %all-to-all-start.4 = ((bf16[32,16,128]{2,1,0:T(8,128)(2,1)}), bf16[32,16,128]{2,1,0:T(8,128)(2,1)S(1)}, u32[]{:S(2)}, u32[]{:S(2)}) async-start(bf16[32,16,128]{2,1,0:T(8,128)(2,1)} %broadcast_in_dim.9), calls=%async_computation.4 | async-start | bytes 262144 | tf_op jit(solution)/shard_map/all_to_all | solution.py:19
  111.1 3.5 %collective-permute-start = (bf16[264,512]{1,0:T(8,128)(2,1)S(1)}, bf16[264,512]{1,0:T(8,128)(2,1)S(1)}, u32[]{:S(2)}, u32[]{:S(2)}) collective-permute-start(bf16[264,512]{1,0:T(8,128)(2,1)S(1)} %get-tuple-element.35), channel_id=1, source_target_pairs={{0,16},{16,0},{1,17},{17,1},{2,18},{18,2},{3,19},{19,3},{4,20},{20... | collective-permute-start | bytes 811016 | tf_op jit(solution)/shard_map/ppermute | solution.py:359
  114.7 5.7 %collective-permute-done.taken = bf16[264,512]{1,0:T(8,128)(2,1)S(1)} collective-permute-done((bf16[264,512]{1,0:T(8,128)(2,1)S(1)}, bf16[264,512]{1,0:T(8,128)(2,1)S(1)}, u32[]{:S(2)}, u32[]{:S(2)}) %collective-permute-start) | collective-permute-done | bytes 270368 | tf_op jit(solution)/shard_map/ppermute | solution.py:359
  120.4 0.9 shard_map.193
  121.4 3.7 %all-to-all-start.5 = ((bf16[8,9,8,128]{3,2,1,0:T(8,128)(2,1)}), bf16[8,9,8,128]{3,2,1,0:T(8,128)(2,1)S(1)}, u32[]{:S(2)}, u32[]{:S(2)}) async-start(bf16[8,9,8,128]{3,2,1,0:T(8,128)(2,1)} %shard_map.193), calls=%async_computation.5 | async-start | bytes 294912 | tf_op jit(solution)/shard_map/all_to_all | solution.py:19
  125.1 3.8 %collective-permute-start.1 = (bf16[512,256]{1,0:T(8,128)(2,1)S(1)}, bf16[512,256]{1,0:T(8,128)(2,1)S(1)}, u32[]{:S(2)}, u32[]{:S(2)}) collective-permute-start(bf16[512,256]{1,0:T(8,128)(2,1)S(1)} %get-tuple-element.36), channel_id=1, source_target_pairs={{0,16},{16,0},{1,17},{17,1},{2,18},{18,2},{3,19},{19,3},{4,20},{20... | collective-permute-start | bytes 786440 | tf_op jit(solution)/shard_map/ppermute | solution.py:360
  128.9 9.4 %all-to-all-done.5.tiles = bf16[8,9,8,128]{3,2,1,0:T(8,128)(2,1)S(1)} async-done(((bf16[8,9,8,128]{3,2,1,0:T(8,128)(2,1)}), bf16[8,9,8,128]{3,2,1,0:T(8,128)(2,1)S(1)}, u32[]{:S(2)}, u32[]{:S(2)}) %all-to-all-start.5) | async-done | bytes 147488 | tf_op jit(solution)/shard_map/all_to_all | solution.py:19
  138.4 0.2 shard_map.194
  138.5 1.2 collective-permute-done.1.taken
  139.7 24.9 %all_gather.3.hidden = bf16[128,512]{1,0:T(8,128)(2,1)S(1)} all-gather(bf16[16,512]{1,0:T(8,128)(2,1)S(1)} %shard_map.194), channel_id=1, replica_groups=mesh['grp'=2,'kv_pair'=8,'kv_side'=2,'tp'=16] {'kv_pair'}, dimensions={0}, use_global_device_ids=true | all-gather | bytes 147456 | tf_op jit(solution)/shard_map/all_gather | solution.py:371
  164.7 0.3 shard_map.195
  165.0 23.1 %all_to_all.39 = bf16[32,16,128]{2,1,0:T(8,128)(2,1)S(1)} all-to-all(bf16[32,16,128]{2,1,0:T(8,128)(2,1)S(1)} %shard_map.195), channel_id=1, replica_groups=mesh['grp'=2,'kv_pair'=8,'kv_side'=2,'tp'=16] {'kv_side','tp'}, dimensions={0} | all-to-all | bytes 262144 | tf_op jit(solution)/shard_map/all_to_all | solution.py:19
  188.1 0.6 fusion.1
  (15 shorter events, 0.1 us)
Async XLA Ops:
  0.6 93.1 %copy-start = (bf16[128,256]{1,0:T(8,128)(2,1)S(1)}, bf16[128,256]{1,0:T(8,128)(2,1)}, u32[]{:S(2)}) copy-start(bf16[128,256]{1,0:T(8,128)(2,1)} %param.30) | copy-start | bytes 196612
  1.8 51.9 %copy-start.4 = (bf16[256,128]{1,0:T(8,128)(2,1)S(1)}, bf16[256,128]{1,0:T(8,128)(2,1)}, u32[]{:S(2)}) copy-start(bf16[256,128]{1,0:T(8,128)(2,1)} %wv.1) | copy-start | bytes 196612
  1.9 51.9 %copy-start.5 = (bf16[256,128]{1,0:T(8,128)(2,1)S(1)}, bf16[256,128]{1,0:T(8,128)(2,1)}, u32[]{:S(2)}) copy-start(bf16[256,128]{1,0:T(8,128)(2,1)} %wo.1) | copy-start | bytes 196612
  53.8 20.1 %copy-start.3 = (f32[8,1,64,128]{3,2,1,0:T(8,128)S(1)}, f32[8,1,64,128]{3,2,1,0:T(8,128)}, u32[]{:S(2)}) copy-start(f32[8,1,64,128]{3,2,1,0:T(8,128)} %param.27) | copy-start | bytes 786436
  75.8 44.7 %copy-start.1 = (bf16[256,1024]{1,0:T(8,128)(2,1)S(1)}, bf16[256,1024]{1,0:T(8,128)(2,1)}, u32[]{:S(2)}) copy-start(bf16[256,1024]{1,0:T(8,128)(2,1)} %w_up.3) | copy-start | bytes 1572868
  107.0 13.4 %all-to-all-start.4 = ((bf16[32,16,128]{2,1,0:T(8,128)(2,1)}), bf16[32,16,128]{2,1,0:T(8,128)(2,1)S(1)}, u32[]{:S(2)}, u32[]{:S(2)}) async-start(bf16[32,16,128]{2,1,0:T(8,128)(2,1)} %broadcast_in_dim.9), calls=%async_computation.4 | async-start | bytes 262144 | tf_op jit(solution)/shard_map/all_to_all | solution.py:19
  111.1 9.3 %collective-permute-start = (bf16[264,512]{1,0:T(8,128)(2,1)S(1)}, bf16[264,512]{1,0:T(8,128)(2,1)S(1)}, u32[]{:S(2)}, u32[]{:S(2)}) collective-permute-start(bf16[264,512]{1,0:T(8,128)(2,1)S(1)} %get-tuple-element.35), channel_id=1, source_target_pairs={{0,16},{16,0},{1,17},{17,1},{2,18},{18,2},{3,19},{19,3},{4,20},{20... | collective-permute-start | bytes 811016 | tf_op jit(solution)/shard_map/ppermute | solution.py:359
  121.4 43.3 %copy-start.2 = (bf16[1024,256]{1,0:T(8,128)(2,1)S(1)}, bf16[1024,256]{1,0:T(8,128)(2,1)}, u32[]{:S(2)}) copy-start(bf16[1024,256]{1,0:T(8,128)(2,1)} %w_down.3) | copy-start | bytes 1572868
  121.4 17.0 %all-to-all-start.5 = ((bf16[8,9,8,128]{3,2,1,0:T(8,128)(2,1)}), bf16[8,9,8,128]{3,2,1,0:T(8,128)(2,1)S(1)}, u32[]{:S(2)}, u32[]{:S(2)}) async-start(bf16[8,9,8,128]{3,2,1,0:T(8,128)(2,1)} %shard_map.193), calls=%async_computation.5 | async-start | bytes 294912 | tf_op jit(solution)/shard_map/all_to_all | solution.py:19
  125.1 14.6 %collective-permute-start.1 = (bf16[512,256]{1,0:T(8,128)(2,1)S(1)}, bf16[512,256]{1,0:T(8,128)(2,1)S(1)}, u32[]{:S(2)}, u32[]{:S(2)}) collective-permute-start(bf16[512,256]{1,0:T(8,128)(2,1)S(1)} %get-tuple-element.36), channel_id=1, source_target_pairs={{0,16},{16,0},{1,17},{17,1},{2,18},{18,2},{3,19},{19,3},{4,20},{20... | collective-permute-start | bytes 786440 | tf_op jit(solution)/shard_map/ppermute | solution.py:360

commit v7 on v5

--- a/solution.py
+++ b/solution.py
@@ -229,8 +229,8 @@
     mine = contract(left, w_down[pl.ds(pl.multiple_of(side * half, half), half)], 1, 0)
     theirs = contract(left, taken[...], 1, 0)
     shape = (count, *out.shape[1:])
-    out[pl.ds(side * count, count)] = mine.T.astype(jnp.bfloat16).reshape(shape)
-    out[pl.ds((1 - side) * count, count)] = theirs.T.astype(jnp.bfloat16).reshape(shape)
+    out[pl.ds((1 - side) * count, count)] = mine.T.astype(jnp.bfloat16).reshape(shape)
+    out[pl.ds(side * count, count)] = theirs.T.astype(jnp.bfloat16).reshape(shape)
 
 
 def in_vmem(body, shape, *operands):
@@ -359,7 +359,8 @@
     heads = exchange(heads, KV).reshape(seqs, value_dim)
     heads, sent_up, sent_down = lax.optimization_barrier((heads, sent_up, sent_down))
     other_up = lax.ppermute(sent_up, "kv_side", swap)
-    other_down = lax.ppermute(sent_down, "kv_side", swap)
+    shifted = [(i, (i + 2 * (i % 2) - 1) % kv) for i in range(kv)]
+    other_down = lax.ppermute(sent_down, KV, shifted)
     branch = contract(w_proj, heads, 0, 1).astype(jnp.bfloat16)
     branch = exchange(branch.reshape(tp, own_columns, seqs), "tp")
     own_middle = residual + jnp.sum(branch.astype(jnp.float32), axis=0)
@@ -372,7 +373,10 @@
     copies, other_down = lax.optimization_barrier((copies, other_down))
     hidden = exchange(copies, "kv_pair")
     down = in_vmem(down_body, (2 * tp, own_columns, seqs), hidden, w_down, other_down)
-    down = exchange(down, ("kv_side", "tp"))
+    groups = [
+        [k % kv * tp + t for k in (odd, odd + 1) for t in range(tp)] for odd in range(1, kv, 2)
+    ]
+    down = lax.all_to_all(down, (*KV, "tp"), 0, 0, axis_index_groups=groups, tiled=True)
     mixed = own_middle.astype(jnp.float32) + jnp.sum(down.astype(jnp.float32), axis=0)
     mixed = mixed.astype(jnp.bfloat16).T
     return (mixed, cell_new[:, None], norm_new[:, None], max_new.reshape(own, 1))

time: 184 us -> 186 us (1.011)
  starting transfers between devices: 15.2 us -> 17.4 us
    all_to_all x0 -> x1, blocking collectives: none -> 21.5 us  [layer(): lax.all_to_all(down, (*KV, 'tp'), 0, 0, axis_index_groups=groups, tiled=T...]
    all_to_all x6 -> x5, blocking collectives: 144 us -> 123 us  [exchange(): return lax.all_to_all(tiles, axis, split_axis=0, concat_axis=0, tiled=True)]
    ppermute x1, starting transfers between devices: 3.83 us -> 6.03 us  [layer(): other_down = lax.ppermute(sent_down, KV, shifted)]
    all_to_all x2, waiting for transfers between devices: 9.45 us -> 7.25 us  [exchange(): return lax.all_to_all(tiles, axis, split_axis=0, concat_axis=0, tiled=True)]
where the time goes in v7:
time: 186 us; the launch traced here: 185 us
  blocking collectives  145 us (78%)
  starting transfers between devices  17.4 us (9%)
  waiting for transfers between devices  15.9 us (9%)
  Pallas kernels  4.92 us (3%)
    all_to_all x5, blocking collectives, exchange(): return lax.all_to_all(tiles, axis, split_axis=0, concat_axis=0, tiled=True)  123 us
    all_to_all x1, blocking collectives, layer(): lax.all_to_all(down, (*KV, 'tp'), 0, 0, axis_index_groups=groups, tiled=T...  21.5 us
    all_to_all x2, starting transfers between devices, exchange(): return lax.all_to_all(tiles, axis, split_axis=0, concat_axis=0, tiled=True)  7.88 us
    all_to_all x2, waiting for transfers between devices, exchange(): return lax.all_to_all(tiles, axis, split_axis=0, concat_axis=0, tiled=True)  7.25 us
    ppermute x1, starting transfers between devices, layer(): other_down = lax.ppermute(sent_down, KV, shifted)  6.03 us
    ppermute x1, waiting for transfers between devices, layer(): other_up = lax.ppermute(sent_up, 'kv_side', swap)  5.75 us
  transfers between devices with their start and end apart: 4, of which 3 were waited for; matrix products, arithmetic and copies ran while one was open for 0% of the time, Pallas kernels for 0%

profile of v7, /device:TPU:65, one launch (start us, length us, event | category | flops | bytes accessed | tf_op | source)
XLA Modules:
  0.0 185.2 jit_solution(4595842635648157625)
XLA Ops:
  0.6 0.0 copy-start
  0.7 1.2 stage.1
  1.9 51.9 %all_to_all.40.tokens = bf16[16,16,128]{2,1,0:T(8,128)(2,1)S(1)} all-to-all(bf16[16,16,128]{2,1,0:T(8,128)(2,1)S(1)} %get-tuple-element.24), channel_id=1, replica_groups=mesh['grp'=2,'kv_pair'=8,'kv_side'=2,'tp'=16] {'tp'}, dimensions={0} | all-to-all | bytes 131072 | tf_op jit(solution)/shard_map/all_to_all | solution.py:19
  53.8 0.4 shard_map.192
  54.2 19.7 %all_to_all.41.tiles = bf16[16,8,512]{2,1,0:T(8,128)(2,1)S(1)} all-to-all(bf16[16,8,512]{2,1,0:T(8,128)(2,1)S(1)} %shard_map.192), channel_id=1, replica_groups=mesh['grp'=2,'kv_pair'=8,'kv_side'=2,'tp'=16] {'kv_pair','kv_side'}, dimensions={0} | all-to-all | bytes 262144 | tf_op jit(solution)/shard_map/all_to_all | solution.py:19
  73.8 1.9 %memory.1 = (bf16[16,8,128]{2,1,0:T(8,128)(2,1)S(1)}, f32[8,64,128]{2,1,0:T(8,128)}, f32[8,64]{1,0:T(8,128)}, f32[1,8]{1,0:T(1,128)}, bf16[264,512]{1,0:T(8,128)(2,1)S(1)}, /*index=5*/bf16[512,256]{1,0:T(8,128)(2,1)S(1)}) custom-call(bf16[16,8,512]{2,1,0:T(8,128)(2,1)S(1)} %all_to_all.41.tiles, f32[8,64,128]{2,1,0:T(8,128)S(1)} %bitcast.27, ...), custom_call_target="tpu_custom_call" | custom-call | tf_op jit(solution)/shard_map/memory/pallas_call | solution.py:277
  75.8 17.9 %all_to_all.42 = bf16[16,8,128]{2,1,0:T(8,128)(2,1)S(1)} all-to-all(bf16[16,8,128]{2,1,0:T(8,128)(2,1)S(1)} %get-tuple-element.30), channel_id=1, replica_groups=mesh['grp'=2,'kv_pair'=8,'kv_side'=2,'tp'=16] {'kv_pair','kv_side'}, dimensions={0} | all-to-all | bytes 65536 | tf_op jit(solution)/shard_map/all_to_all | solution.py:19
  93.7 0.1 fusion
  93.8 0.1 copy.23
  94.0 12.3 %all_to_all.43 = bf16[16,16,128]{2,1,0:T(8,128)(2,1)S(1)} all-to-all(bf16[16,16,128]{2,1,0:T(8,128)(2,1)S(1)} %bitcast.28), channel_id=1, replica_groups=mesh['grp'=2,'kv_pair'=8,'kv_side'=2,'tp'=16] {'tp'}, dimensions={0} | all-to-all | bytes 131072 | tf_op jit(solution)/shard_map/all_to_all | solution.py:19
  106.3 0.7 broadcast_in_dim.9
  107.0 4.2 %all-to-all-start.4 = ((bf16[32,16,128]{2,1,0:T(8,128)(2,1)}), bf16[32,16,128]{2,1,0:T(8,128)(2,1)S(1)}, u32[]{:S(2)}, u32[]{:S(2)}) async-start(bf16[32,16,128]{2,1,0:T(8,128)(2,1)} %broadcast_in_dim.9), calls=%async_computation.4 | async-start | bytes 262144 | tf_op jit(solution)/shard_map/all_to_all | solution.py:19
  111.1 3.5 %collective-permute-start = (bf16[264,512]{1,0:T(8,128)(2,1)S(1)}, bf16[264,512]{1,0:T(8,128)(2,1)S(1)}, u32[]{:S(2)}, u32[]{:S(2)}) collective-permute-start(bf16[264,512]{1,0:T(8,128)(2,1)S(1)} %get-tuple-element.35), channel_id=1, source_target_pairs={{0,16},{16,0},{1,17},{17,1},{2,18},{18,2},{3,19},{19,3},{4,20},{20... | collective-permute-start | bytes 811016 | tf_op jit(solution)/shard_map/ppermute | solution.py:361
  114.7 5.7 %collective-permute-done.taken = bf16[264,512]{1,0:T(8,128)(2,1)S(1)} collective-permute-done((bf16[264,512]{1,0:T(8,128)(2,1)S(1)}, bf16[264,512]{1,0:T(8,128)(2,1)S(1)}, u32[]{:S(2)}, u32[]{:S(2)}) %collective-permute-start) | collective-permute-done | bytes 270368 | tf_op jit(solution)/shard_map/ppermute | solution.py:361
  120.4 0.9 shard_map.193
  121.4 3.7 %all-to-all-start.5 = ((bf16[8,9,8,128]{3,2,1,0:T(8,128)(2,1)}), bf16[8,9,8,128]{3,2,1,0:T(8,128)(2,1)S(1)}, u32[]{:S(2)}, u32[]{:S(2)}) async-start(bf16[8,9,8,128]{3,2,1,0:T(8,128)(2,1)} %shard_map.193), calls=%async_computation.5 | async-start | bytes 294912 | tf_op jit(solution)/shard_map/all_to_all | solution.py:19
  125.1 6.0 %collective-permute-start.1 = (bf16[512,256]{1,0:T(8,128)(2,1)S(1)}, bf16[512,256]{1,0:T(8,128)(2,1)S(1)}, u32[]{:S(2)}, u32[]{:S(2)}) collective-permute-start(bf16[512,256]{1,0:T(8,128)(2,1)S(1)} %get-tuple-element.36), channel_id=1, source_target_pairs={{0,240},{16,32},{32,16},{48,64},{64,48},{80,96},{96,80},{112,128},... | collective-permute-start | bytes 786440 | tf_op jit(solution)/shard_map/ppermute | solution.py:363
  131.1 7.2 %all-to-all-done.5.tiles = bf16[8,9,8,128]{3,2,1,0:T(8,128)(2,1)S(1)} async-done(((bf16[8,9,8,128]{3,2,1,0:T(8,128)(2,1)}), bf16[8,9,8,128]{3,2,1,0:T(8,128)(2,1)S(1)}, u32[]{:S(2)}, u32[]{:S(2)}) %all-to-all-start.5) | async-done | bytes 147488 | tf_op jit(solution)/shard_map/all_to_all | solution.py:19
  138.4 0.2 shard_map.194
  138.5 2.9 %collective-permute-done.1.taken = bf16[512,256]{1,0:T(8,128)(2,1)S(1)} collective-permute-done((bf16[512,256]{1,0:T(8,128)(2,1)S(1)}, bf16[512,256]{1,0:T(8,128)(2,1)S(1)}, u32[]{:S(2)}, u32[]{:S(2)}) %collective-permute-start.1) | collective-permute-done | bytes 262176 | tf_op jit(solution)/shard_map/ppermute | solution.py:363
  141.5 21.3 %all_to_all.44.hidden = bf16[8,16,512]{2,1,0:T(8,128)(2,1)S(1)} all-to-all(bf16[8,16,512]{2,1,0:T(8,128)(2,1)S(1)} %shard_map.194), channel_id=1, replica_groups=mesh['grp'=2,'kv_pair'=8,'kv_side'=2,'tp'=16] {'kv_pair'}, dimensions={0} | all-to-all | bytes 262144 | tf_op jit(solution)/shard_map/all_to_all | solution.py:19
  162.8 0.3 shard_map.195
  163.1 21.5 %all_to_all.45 = bf16[32,16,128]{2,1,0:T(8,128)(2,1)S(1)} all-to-all(bf16[32,16,128]{2,1,0:T(8,128)(2,1)S(1)} %shard_map.195), channel_id=1, replica_groups={{16,17,18,19,20,21,22,23,24,25,26,27,28,29,30,31,32,33,34,35,36,37,38,3..., dimensions={0} | all-to-all | bytes 262144 | tf_op jit(solution)/shard_map/all_to_all | solution.py:379
  184.6 0.6 fusion.1
  (15 shorter events, 0.1 us)
Async XLA Ops:
  0.6 93.1 %copy-start = (bf16[128,256]{1,0:T(8,128)(2,1)S(1)}, bf16[128,256]{1,0:T(8,128)(2,1)}, u32[]{:S(2)}) copy-start(bf16[128,256]{1,0:T(8,128)(2,1)} %param.30) | copy-start | bytes 196612
  1.8 51.9 %copy-start.4 = (bf16[256,128]{1,0:T(8,128)(2,1)S(1)}, bf16[256,128]{1,0:T(8,128)(2,1)}, u32[]{:S(2)}) copy-start(bf16[256,128]{1,0:T(8,128)(2,1)} %wv.1) | copy-start | bytes 196612
  1.9 51.9 %copy-start.5 = (bf16[256,128]{1,0:T(8,128)(2,1)S(1)}, bf16[256,128]{1,0:T(8,128)(2,1)}, u32[]{:S(2)}) copy-start(bf16[256,128]{1,0:T(8,128)(2,1)} %wo.1) | copy-start | bytes 196612
  53.8 20.1 %copy-start.3 = (f32[8,1,64,128]{3,2,1,0:T(8,128)S(1)}, f32[8,1,64,128]{3,2,1,0:T(8,128)}, u32[]{:S(2)}) copy-start(f32[8,1,64,128]{3,2,1,0:T(8,128)} %param.27) | copy-start | bytes 786436
  75.8 44.7 %copy-start.1 = (bf16[256,1024]{1,0:T(8,128)(2,1)S(1)}, bf16[256,1024]{1,0:T(8,128)(2,1)}, u32[]{:S(2)}) copy-start(bf16[256,1024]{1,0:T(8,128)(2,1)} %w_up.3) | copy-start | bytes 1572868
  107.0 13.4 %all-to-all-start.4 = ((bf16[32,16,128]{2,1,0:T(8,128)(2,1)}), bf16[32,16,128]{2,1,0:T(8,128)(2,1)S(1)}, u32[]{:S(2)}, u32[]{:S(2)}) async-start(bf16[32,16,128]{2,1,0:T(8,128)(2,1)} %broadcast_in_dim.9), calls=%async_computation.4 | async-start | bytes 262144 | tf_op jit(solution)/shard_map/all_to_all | solution.py:19
  111.1 9.3 %collective-permute-start = (bf16[264,512]{1,0:T(8,128)(2,1)S(1)}, bf16[264,512]{1,0:T(8,128)(2,1)S(1)}, u32[]{:S(2)}, u32[]{:S(2)}) collective-permute-start(bf16[264,512]{1,0:T(8,128)(2,1)S(1)} %get-tuple-element.35), channel_id=1, source_target_pairs={{0,16},{16,0},{1,17},{17,1},{2,18},{18,2},{3,19},{19,3},{4,20},{20... | collective-permute-start | bytes 811016 | tf_op jit(solution)/shard_map/ppermute | solution.py:361
  121.4 41.5 %copy-start.2 = (bf16[1024,256]{1,0:T(8,128)(2,1)S(1)}, bf16[1024,256]{1,0:T(8,128)(2,1)}, u32[]{:S(2)}) copy-start(bf16[1024,256]{1,0:T(8,128)(2,1)} %w_down.3) | copy-start | bytes 1572868
  121.4 17.0 %all-to-all-start.5 = ((bf16[8,9,8,128]{3,2,1,0:T(8,128)(2,1)}), bf16[8,9,8,128]{3,2,1,0:T(8,128)(2,1)S(1)}, u32[]{:S(2)}, u32[]{:S(2)}) async-start(bf16[8,9,8,128]{3,2,1,0:T(8,128)(2,1)} %shard_map.193), calls=%async_computation.5 | async-start | bytes 294912 | tf_op jit(solution)/shard_map/all_to_all | solution.py:19
  125.1 16.4 %collective-permute-start.1 = (bf16[512,256]{1,0:T(8,128)(2,1)S(1)}, bf16[512,256]{1,0:T(8,128)(2,1)S(1)}, u32[]{:S(2)}, u32[]{:S(2)}) collective-permute-start(bf16[512,256]{1,0:T(8,128)(2,1)S(1)} %get-tuple-element.36), channel_id=1, source_target_pairs={{0,240},{16,32},{32,16},{48,64},{64,48},{80,96},{96,80},{112,128},... | collective-permute-start | bytes 786440 | tf_op jit(solution)/shard_map/ppermute | solution.py:363

commit v8 on v5

--- a/solution.py
+++ b/solution.py
@@ -356,20 +356,21 @@
         exchange(terms, KV), cell_state[:, 0], aux, gains, w_up, w_down, width
     )
 
-    heads = exchange(heads, KV).reshape(seqs, value_dim)
-    heads, sent_up, sent_down = lax.optimization_barrier((heads, sent_up, sent_down))
+    heads = exchange(heads, KV)
     other_up = lax.ppermute(sent_up, "kv_side", swap)
     other_down = lax.ppermute(sent_down, "kv_side", swap)
+
+    heads = heads.reshape(seqs, value_dim)
     branch = contract(w_proj, heads, 0, 1).astype(jnp.bfloat16)
     branch = exchange(branch.reshape(tp, own_columns, seqs), "tp")
     own_middle = residual + jnp.sum(branch.astype(jnp.float32), axis=0)
     own_middle = own_middle.astype(jnp.bfloat16)
+    own_middle, other_up, other_down = lax.optimization_barrier((own_middle, other_up, other_down))
     middle = spread(own_middle, ("kv_side", "tp"))
     tiles = 2 * own * half // (8 * LANES) + 1
     upward = in_vmem(up_body, (pairs, tiles, 8, LANES), middle, gain_mid, w_up, other_up)
     upward = exchange(upward, "kv_pair")
     copies = in_vmem(functools.partial(hidden_body, width), (pairs, 2 * own, half), upward)
-    copies, other_down = lax.optimization_barrier((copies, other_down))
     hidden = exchange(copies, "kv_pair")
     down = in_vmem(down_body, (2 * tp, own_columns, seqs), hidden, w_down, other_down)
     down = exchange(down, ("kv_side", "tp"))

time: 184 us -> 184 us (level)
  blocking collectives: 144 us -> 156 us
  waiting for transfers between devices: 16.4 us -> 9.53 us
  starting transfers between devices: 15.2 us -> 10.6 us
    all_to_all x6 -> x7, blocking collectives: 144 us -> 156 us  [exchange(): return lax.all_to_all(tiles, axis, split_axis=0, concat_axis=0, tiled=True)]
    all_to_all x2 -> x1, waiting for transfers between devices: 9.45 us -> 2.57 us  [exchange(): return lax.all_to_all(tiles, axis, split_axis=0, concat_axis=0, tiled=True)]
    all_to_all x2 -> x1, starting transfers between devices: 7.88 us -> 5.27 us  [exchange(): return lax.all_to_all(tiles, axis, split_axis=0, concat_axis=0, tiled=True)]
  transfers between devices with their start and end apart: 4 -> 3, of which waited for: 3 -> 3; matrix products, arithmetic and copies ran while one was open for 0% -> 0% of each run, Pallas kernels for 0% -> 0%
where the time goes in v8:
time: 184 us; the launch traced here: 183 us
  blocking collectives  156 us (85%)
  starting transfers between devices  10.6 us (6%)
  waiting for transfers between devices  9.53 us (5%)
  Pallas kernels  4.26 us (2%)
    all_to_all x7, blocking collectives, exchange(): return lax.all_to_all(tiles, axis, split_axis=0, concat_axis=0, tiled=True)  156 us
    ppermute x1, waiting for transfers between devices, layer(): other_up = lax.ppermute(sent_up, 'kv_side', swap)  5.79 us
    all_to_all x1, starting transfers between devices, exchange(): return lax.all_to_all(tiles, axis, split_axis=0, concat_axis=0, tiled=True)  5.27 us
  transfers between devices with their start and end apart: 3, of which 3 were waited for; matrix products, arithmetic and copies ran while one was open for 0% of the time, Pallas kernels for 0%

profile of v8, /device:TPU:65, one launch (start us, length us, event | category | flops | bytes accessed | tf_op | source)
XLA Modules:
  0.0 183.1 jit_solution(16459681672083775865)
XLA Ops:
  0.6 0.0 copy-start
  0.7 1.2 stage.1
  1.8 0.0 copy-start.4
  1.9 51.9 %all_to_all.40.tokens = bf16[16,16,128]{2,1,0:T(8,128)(2,1)S(1)} all-to-all(bf16[16,16,128]{2,1,0:T(8,128)(2,1)S(1)} %get-tuple-element.22), channel_id=1, replica_groups=mesh['grp'=2,'kv_pair'=8,'kv_side'=2,'tp'=16] {'tp'}, dimensions={0} | all-to-all | bytes 131072 | tf_op jit(solution)/shard_map/all_to_all | solution.py:19
  53.8 0.4 shard_map.192
  54.2 19.7 %all_to_all.41.tiles = bf16[16,8,512]{2,1,0:T(8,128)(2,1)S(1)} all-to-all(bf16[16,8,512]{2,1,0:T(8,128)(2,1)S(1)} %shard_map.192), channel_id=1, replica_groups=mesh['grp'=2,'kv_pair'=8,'kv_side'=2,'tp'=16] {'kv_pair','kv_side'}, dimensions={0} | all-to-all | bytes 262144 | tf_op jit(solution)/shard_map/all_to_all | solution.py:19
  73.8 1.9 %memory.1 = (bf16[16,8,128]{2,1,0:T(8,128)(2,1)S(1)}, f32[8,64,128]{2,1,0:T(8,128)}, f32[8,64]{1,0:T(8,128)}, f32[1,8]{1,0:T(1,128)}, bf16[264,512]{1,0:T(8,128)(2,1)S(1)}, /*index=5*/bf16[512,256]{1,0:T(8,128)(2,1)S(1)}) custom-call(bf16[16,8,512]{2,1,0:T(8,128)(2,1)S(1)} %all_to_all.41.tiles, f32[8,64,128]{2,1,0:T(8,128)S(1)} %bitcast.28, ...), custom_call_target="tpu_custom_call" | custom-call | tf_op jit(solution)/shard_map/memory/pallas_call | solution.py:277
  75.8 17.9 %all_to_all.42 = bf16[16,8,128]{2,1,0:T(8,128)(2,1)S(1)} all-to-all(bf16[16,8,128]{2,1,0:T(8,128)(2,1)S(1)} %get-tuple-element.28), channel_id=1, replica_groups=mesh['grp'=2,'kv_pair'=8,'kv_side'=2,'tp'=16] {'kv_pair','kv_side'}, dimensions={0} | all-to-all | bytes 65536 | tf_op jit(solution)/shard_map/all_to_all | solution.py:19
  93.7 0.1 fusion
  93.8 0.7 copy.23
  94.6 5.3 %all-to-all-start.3 = ((bf16[16,16,128]{2,1,0:T(8,128)(2,1)}), bf16[16,16,128]{2,1,0:T(8,128)(2,1)S(1)}, u32[]{:S(2)}, u32[]{:S(2)}) async-start(bf16[16,16,128]{2,1,0:T(8,128)(2,1)} %bitcast.14), calls=%async_computation.3 | async-start | bytes 131072 | tf_op jit(solution)/shard_map/all_to_all | solution.py:19
  99.8 2.5 %collective-permute-start.1 = (bf16[512,256]{1,0:T(8,128)(2,1)S(1)}, bf16[512,256]{1,0:T(8,128)(2,1)S(1)}, u32[]{:S(2)}, u32[]{:S(2)}) collective-permute-start(bf16[512,256]{1,0:T(8,128)(2,1)S(1)} %get-tuple-element.30), channel_id=1, source_target_pairs={{0,16},{16,0},{1,17},{17,1},{2,18},{18,2},{3,19},{19,3},{4,20},{20... | collective-permute-start | bytes 786440 | tf_op jit(solution)/shard_map/ppermute | solution.py:361
  102.3 2.9 %collective-permute-start = (bf16[264,512]{1,0:T(8,128)(2,1)S(1)}, bf16[264,512]{1,0:T(8,128)(2,1)S(1)}, u32[]{:S(2)}, u32[]{:S(2)}) collective-permute-start(bf16[264,512]{1,0:T(8,128)(2,1)S(1)} %get-tuple-element.29), channel_id=1, source_target_pairs={{0,16},{16,0},{1,17},{17,1},{2,18},{18,2},{3,19},{19,3},{4,20},{20... | collective-permute-start | bytes 811016 | tf_op jit(solution)/shard_map/ppermute | solution.py:360
  105.2 2.6 %all-to-all-done.3 = bf16[16,16,128]{2,1,0:T(8,128)(2,1)S(1)} async-done(((bf16[16,16,128]{2,1,0:T(8,128)(2,1)}), bf16[16,16,128]{2,1,0:T(8,128)(2,1)S(1)}, u32[]{:S(2)}, u32[]{:S(2)}) %all-to-all-start.3) | async-done | bytes 65568 | tf_op jit(solution)/shard_map/all_to_all | solution.py:19
  107.8 1.2 collective-permute-done.1.taken
  109.0 5.8 %collective-permute-done.taken = bf16[264,512]{1,0:T(8,128)(2,1)S(1)} collective-permute-done((bf16[264,512]{1,0:T(8,128)(2,1)S(1)}, bf16[264,512]{1,0:T(8,128)(2,1)S(1)}, u32[]{:S(2)}, u32[]{:S(2)}) %collective-permute-start) | collective-permute-done | bytes 270368 | tf_op jit(solution)/shard_map/ppermute | solution.py:360
  114.8 17.0 %all_to_all.43.middle = bf16[32,16,128]{2,1,0:T(8,128)(2,1)S(1)} all-to-all(bf16[32,16,128]{2,1,0:T(8,128)(2,1)S(1)} %broadcast_in_dim.9), channel_id=1, replica_groups=mesh['grp'=2,'kv_pair'=8,'kv_side'=2,'tp'=16] {'kv_side','tp'}, dimensions={0} | all-to-all | bytes 262144 | tf_op jit(solution)/shard_map/all_to_all | solution.py:19
  131.8 0.3 shard_map.193
  132.1 17.0 %all_to_all.44.tiles = bf16[8,9,8,128]{3,2,1,0:T(8,128)(2,1)S(1)} all-to-all(bf16[8,9,8,128]{3,2,1,0:T(8,128)(2,1)S(1)} %shard_map.193), channel_id=1, replica_groups=mesh['grp'=2,'kv_pair'=8,'kv_side'=2,'tp'=16] {'kv_pair'}, dimensions={0} | all-to-all | bytes 294912 | tf_op jit(solution)/shard_map/all_to_all | solution.py:19
  149.1 0.2 shard_map.194
  149.2 17.9 %all_to_all.45.hidden = bf16[8,16,512]{2,1,0:T(8,128)(2,1)S(1)} all-to-all(bf16[8,16,512]{2,1,0:T(8,128)(2,1)S(1)} %shard_map.194), channel_id=1, replica_groups=mesh['grp'=2,'kv_pair'=8,'kv_side'=2,'tp'=16] {'kv_pair'}, dimensions={0} | all-to-all | bytes 262144 | tf_op jit(solution)/shard_map/all_to_all | solution.py:19
  167.1 0.3 shard_map.195
  167.4 15.0 %all_to_all.46 = bf16[32,16,128]{2,1,0:T(8,128)(2,1)S(1)} all-to-all(bf16[32,16,128]{2,1,0:T(8,128)(2,1)S(1)} %shard_map.195), channel_id=1, replica_groups=mesh['grp'=2,'kv_pair'=8,'kv_side'=2,'tp'=16] {'kv_side','tp'}, dimensions={0} | all-to-all | bytes 262144 | tf_op jit(solution)/shard_map/all_to_all | solution.py:19
  182.5 0.6 fusion.2
  (14 shorter events, 0.1 us)
Async XLA Ops:
  0.6 93.1 %copy-start = (bf16[128,256]{1,0:T(8,128)(2,1)S(1)}, bf16[128,256]{1,0:T(8,128)(2,1)}, u32[]{:S(2)}) copy-start(bf16[128,256]{1,0:T(8,128)(2,1)} %param.30) | copy-start | bytes 196612
  1.8 51.9 %copy-start.4 = (bf16[256,128]{1,0:T(8,128)(2,1)S(1)}, bf16[256,128]{1,0:T(8,128)(2,1)}, u32[]{:S(2)}) copy-start(bf16[256,128]{1,0:T(8,128)(2,1)} %wv.1) | copy-start | bytes 196612
  1.9 51.9 %copy-start.5 = (bf16[256,128]{1,0:T(8,128)(2,1)S(1)}, bf16[256,128]{1,0:T(8,128)(2,1)}, u32[]{:S(2)}) copy-start(bf16[256,128]{1,0:T(8,128)(2,1)} %wo.1) | copy-start | bytes 196612
  53.8 20.1 %copy-start.3 = (f32[8,1,64,128]{3,2,1,0:T(8,128)S(1)}, f32[8,1,64,128]{3,2,1,0:T(8,128)}, u32[]{:S(2)}) copy-start(f32[8,1,64,128]{3,2,1,0:T(8,128)} %param.27) | copy-start | bytes 786436
  75.8 56.0 %copy-start.1 = (bf16[256,1024]{1,0:T(8,128)(2,1)S(1)}, bf16[256,1024]{1,0:T(8,128)(2,1)}, u32[]{:S(2)}) copy-start(bf16[256,1024]{1,0:T(8,128)(2,1)} %w_up.3) | copy-start | bytes 1572868
  94.6 13.2 %all-to-all-start.3 = ((bf16[16,16,128]{2,1,0:T(8,128)(2,1)}), bf16[16,16,128]{2,1,0:T(8,128)(2,1)S(1)}, u32[]{:S(2)}, u32[]{:S(2)}) async-start(bf16[16,16,128]{2,1,0:T(8,128)(2,1)} %bitcast.14), calls=%async_computation.3 | async-start | bytes 131072 | tf_op jit(solution)/shard_map/all_to_all | solution.py:19
  99.8 9.1 %collective-permute-start.1 = (bf16[512,256]{1,0:T(8,128)(2,1)S(1)}, bf16[512,256]{1,0:T(8,128)(2,1)S(1)}, u32[]{:S(2)}, u32[]{:S(2)}) collective-permute-start(bf16[512,256]{1,0:T(8,128)(2,1)S(1)} %get-tuple-element.30), channel_id=1, source_target_pairs={{0,16},{16,0},{1,17},{17,1},{2,18},{18,2},{3,19},{19,3},{4,20},{20... | collective-permute-start | bytes 786440 | tf_op jit(solution)/shard_map/ppermute | solution.py:361
  102.3 12.4 %collective-permute-start = (bf16[264,512]{1,0:T(8,128)(2,1)S(1)}, bf16[264,512]{1,0:T(8,128)(2,1)S(1)}, u32[]{:S(2)}, u32[]{:S(2)}) collective-permute-start(bf16[264,512]{1,0:T(8,128)(2,1)S(1)} %get-tuple-element.29), channel_id=1, source_target_pairs={{0,16},{16,0},{1,17},{17,1},{2,18},{18,2},{3,19},{19,3},{4,20},{20... | collective-permute-start | bytes 811016 | tf_op jit(solution)/shard_map/ppermute | solution.py:360
  132.1 35.1 %copy-start.2 = (bf16[1024,256]{1,0:T(8,128)(2,1)S(1)}, bf16[1024,256]{1,0:T(8,128)(2,1)}, u32[]{:S(2)}) copy-start(bf16[1024,256]{1,0:T(8,128)(2,1)} %w_down.3) | copy-start | bytes 1572868

commit v9 on v8

--- a/solution.py
+++ b/solution.py
@@ -108,12 +108,13 @@
 
 def memory_body(
     width, tiles, cell, aux, gains, w_up, w_down,
-    heads, cell_out, norm_out, top_out, sent_up, sent_down, cell_new, norm_buf, top_buf, sems,
+    heads_out, cell_out, norm_out, top_out, sent_up, sent_down,
+    heads, cell_new, norm_buf, top_buf, sems,
 ):
     rows, columns = w_up.shape
     half = columns // 2
     at = pl.multiple_of((1 - lax.axis_index("kv_side")) * half, half)
-    last = sems.shape[0] - 1
+    last = sems.shape[0] - 2
     copies = [
         pltpu.make_async_copy(
             w_up.at[:, pl.ds(at, half)], sent_up.at[pl.ds(0, rows)], sems.at[last - 1]
@@ -163,6 +164,8 @@
     done = (numer * (1.0 / (1.0 + jnp.exp(-outgate))) / denom).astype(jnp.bfloat16)
     for peer in range(heads.shape[0]):
         heads[peer] = done
+    copies.append(pltpu.make_async_copy(heads, heads_out, sems.at[last + 1]))
+    copies[-1].start()
     for copy in copies:
         copy.wait()
 
@@ -277,7 +280,7 @@
     return pl.pallas_call(
         functools.partial(memory_body, width),
         out_shape=(
-            pltpu.VMEM((peers, own, value_dim), jnp.bfloat16),
+            jax.ShapeDtypeStruct((peers, own, value_dim), jnp.bfloat16),
             jax.ShapeDtypeStruct(cell.shape, jnp.float32),
             jax.ShapeDtypeStruct((own, key_dim), jnp.float32),
             jax.ShapeDtypeStruct((1, own), jnp.float32),
@@ -285,12 +288,13 @@
             pltpu.VMEM((columns // 2, rows), jnp.bfloat16),
         ),
         in_specs=[vmem] * 4 + [hbm] * 2,
-        out_specs=(vmem, hbm, hbm, hbm, vmem, vmem),
+        out_specs=(hbm, hbm, hbm, hbm, vmem, vmem),
         scratch_shapes=[
+            pltpu.VMEM((peers, own, value_dim), jnp.bfloat16),
             pltpu.VMEM(cell.shape, jnp.float32),
             pltpu.VMEM((own, key_dim), jnp.float32),
             pltpu.VMEM((1, own), jnp.float32),
-            pltpu.SemaphoreType.DMA((own + 4,)),
+            pltpu.SemaphoreType.DMA((own + 5,)),
         ],
         name="memory",
     )(*on_chip(tiles, cell, aux, gains), w_up, w_down)

time: 184 us -> 184 us (level)
  no operation moved by 1% of the time
where the time goes in v9:
time: 184 us; the launch traced here: 183 us
  blocking collectives  157 us (85%)
  starting transfers between devices  10.6 us (6%)
  waiting for transfers between devices  9.53 us (5%)
  Pallas kernels  4.29 us (2%)
    all_to_all x7, blocking collectives, exchange(): return lax.all_to_all(tiles, axis, split_axis=0, concat_axis=0, tiled=True)  157 us
    ppermute x1, waiting for transfers between devices, layer(): other_up = lax.ppermute(sent_up, 'kv_side', swap)  5.79 us
    all_to_all x1, starting transfers between devices, exchange(): return lax.all_to_all(tiles, axis, split_axis=0, concat_axis=0, tiled=True)  5.26 us
  transfers between devices with their start and end apart: 3, of which 3 were waited for; matrix products, arithmetic and copies ran while one was open for 0% of the time, Pallas kernels for 0%

profile of v9, /device:TPU:65, one launch (start us, length us, event | category | flops | bytes accessed | tf_op | source)
XLA Modules:
  0.0 183.3 jit_solution(4955215116864383274)
XLA Ops:
  0.6 0.0 copy-start
  0.7 1.2 stage.1
  1.8 0.0 copy-start.4
  1.9 51.9 %all_to_all.40.tokens = bf16[16,16,128]{2,1,0:T(8,128)(2,1)S(1)} all-to-all(bf16[16,16,128]{2,1,0:T(8,128)(2,1)S(1)} %get-tuple-element.22), channel_id=1, replica_groups=mesh['grp'=2,'kv_pair'=8,'kv_side'=2,'tp'=16] {'tp'}, dimensions={0} | all-to-all | bytes 131072 | tf_op jit(solution)/shard_map/all_to_all | solution.py:19
  53.8 0.4 shard_map.192
  54.2 19.7 %all_to_all.41.tiles = bf16[16,8,512]{2,1,0:T(8,128)(2,1)S(1)} all-to-all(bf16[16,8,512]{2,1,0:T(8,128)(2,1)S(1)} %shard_map.192), channel_id=1, replica_groups=mesh['grp'=2,'kv_pair'=8,'kv_side'=2,'tp'=16] {'kv_pair','kv_side'}, dimensions={0} | all-to-all | bytes 262144 | tf_op jit(solution)/shard_map/all_to_all | solution.py:19
  73.8 2.0 %memory.1 = (bf16[16,8,128]{2,1,0:T(8,128)(2,1)}, f32[8,64,128]{2,1,0:T(8,128)}, f32[8,64]{1,0:T(8,128)}, f32[1,8]{1,0:T(1,128)}, bf16[264,512]{1,0:T(8,128)(2,1)S(1)}, /*index=5*/bf16[512,256]{1,0:T(8,128)(2,1)S(1)}) custom-call(bf16[16,8,512]{2,1,0:T(8,128)(2,1)S(1)} %all_to_all.41.tiles, f32[8,64,128]{2,1,0:T(8,128)S(1)} %bitcast.28, ...), custom_call_target="tpu_custom_call" | custom-call | tf_op jit(solution)/shard_map/memory/pallas_call | solution.py:280
  75.8 18.1 %all_to_all.42 = bf16[16,8,128]{2,1,0:T(8,128)(2,1)S(1)} all-to-all(bf16[16,8,128]{2,1,0:T(8,128)(2,1)} %get-tuple-element.28), channel_id=1, replica_groups=mesh['grp'=2,'kv_pair'=8,'kv_side'=2,'tp'=16] {'kv_pair','kv_side'}, dimensions={0} | all-to-all | bytes 65536 | tf_op jit(solution)/shard_map/all_to_all | solution.py:19
  93.9 0.1 fusion
  94.1 0.7 copy.23
  94.8 5.3 %all-to-all-start.3 = ((bf16[16,16,128]{2,1,0:T(8,128)(2,1)}), bf16[16,16,128]{2,1,0:T(8,128)(2,1)S(1)}, u32[]{:S(2)}, u32[]{:S(2)}) async-start(bf16[16,16,128]{2,1,0:T(8,128)(2,1)} %bitcast.14), calls=%async_computation.3 | async-start | bytes 131072 | tf_op jit(solution)/shard_map/all_to_all | solution.py:19
  100.1 2.5 %collective-permute-start.1 = (bf16[512,256]{1,0:T(8,128)(2,1)S(1)}, bf16[512,256]{1,0:T(8,128)(2,1)S(1)}, u32[]{:S(2)}, u32[]{:S(2)}) collective-permute-start(bf16[512,256]{1,0:T(8,128)(2,1)S(1)} %get-tuple-element.30), channel_id=1, source_target_pairs={{0,16},{16,0},{1,17},{17,1},{2,18},{18,2},{3,19},{19,3},{4,20},{20... | collective-permute-start | bytes 786440 | tf_op jit(solution)/shard_map/ppermute | solution.py:365
  102.6 2.9 %collective-permute-start = (bf16[264,512]{1,0:T(8,128)(2,1)S(1)}, bf16[264,512]{1,0:T(8,128)(2,1)S(1)}, u32[]{:S(2)}, u32[]{:S(2)}) collective-permute-start(bf16[264,512]{1,0:T(8,128)(2,1)S(1)} %get-tuple-element.29), channel_id=1, source_target_pairs={{0,16},{16,0},{1,17},{17,1},{2,18},{18,2},{3,19},{19,3},{4,20},{20... | collective-permute-start | bytes 811016 | tf_op jit(solution)/shard_map/ppermute | solution.py:364
  105.4 2.6 %all-to-all-done.3 = bf16[16,16,128]{2,1,0:T(8,128)(2,1)S(1)} async-done(((bf16[16,16,128]{2,1,0:T(8,128)(2,1)}), bf16[16,16,128]{2,1,0:T(8,128)(2,1)S(1)}, u32[]{:S(2)}, u32[]{:S(2)}) %all-to-all-start.3) | async-done | bytes 65568 | tf_op jit(solution)/shard_map/all_to_all | solution.py:19
  108.0 1.2 collective-permute-done.1.taken
  109.2 5.8 %collective-permute-done.taken = bf16[264,512]{1,0:T(8,128)(2,1)S(1)} collective-permute-done((bf16[264,512]{1,0:T(8,128)(2,1)S(1)}, bf16[264,512]{1,0:T(8,128)(2,1)S(1)}, u32[]{:S(2)}, u32[]{:S(2)}) %collective-permute-start) | collective-permute-done | bytes 270368 | tf_op jit(solution)/shard_map/ppermute | solution.py:364
  115.0 17.0 %all_to_all.43.middle = bf16[32,16,128]{2,1,0:T(8,128)(2,1)S(1)} all-to-all(bf16[32,16,128]{2,1,0:T(8,128)(2,1)S(1)} %broadcast_in_dim.9), channel_id=1, replica_groups=mesh['grp'=2,'kv_pair'=8,'kv_side'=2,'tp'=16] {'kv_side','tp'}, dimensions={0} | all-to-all | bytes 262144 | tf_op jit(solution)/shard_map/all_to_all | solution.py:19
  132.0 0.3 shard_map.193
  132.3 17.0 %all_to_all.44.tiles = bf16[8,9,8,128]{3,2,1,0:T(8,128)(2,1)S(1)} all-to-all(bf16[8,9,8,128]{3,2,1,0:T(8,128)(2,1)S(1)} %shard_map.193), channel_id=1, replica_groups=mesh['grp'=2,'kv_pair'=8,'kv_side'=2,'tp'=16] {'kv_pair'}, dimensions={0} | all-to-all | bytes 294912 | tf_op jit(solution)/shard_map/all_to_all | solution.py:19
  149.3 0.2 shard_map.194
  149.5 17.3 %all_to_all.45.hidden = bf16[8,16,512]{2,1,0:T(8,128)(2,1)S(1)} all-to-all(bf16[8,16,512]{2,1,0:T(8,128)(2,1)S(1)} %shard_map.194), channel_id=1, replica_groups=mesh['grp'=2,'kv_pair'=8,'kv_side'=2,'tp'=16] {'kv_pair'}, dimensions={0} | all-to-all | bytes 262144 | tf_op jit(solution)/shard_map/all_to_all | solution.py:19
  166.8 0.3 shard_map.195
  167.1 15.6 %all_to_all.46 = bf16[32,16,128]{2,1,0:T(8,128)(2,1)S(1)} all-to-all(bf16[32,16,128]{2,1,0:T(8,128)(2,1)S(1)} %shard_map.195), channel_id=1, replica_groups=mesh['grp'=2,'kv_pair'=8,'kv_side'=2,'tp'=16] {'kv_side','tp'}, dimensions={0} | all-to-all | bytes 262144 | tf_op jit(solution)/shard_map/all_to_all | solution.py:19
  182.7 0.6 fusion.2
  (14 shorter events, 0.1 us)
Async XLA Ops:
  0.6 93.3 %copy-start = (bf16[128,256]{1,0:T(8,128)(2,1)S(1)}, bf16[128,256]{1,0:T(8,128)(2,1)}, u32[]{:S(2)}) copy-start(bf16[128,256]{1,0:T(8,128)(2,1)} %param.30) | copy-start | bytes 196612
  1.8 51.9 %copy-start.4 = (bf16[256,128]{1,0:T(8,128)(2,1)S(1)}, bf16[256,128]{1,0:T(8,128)(2,1)}, u32[]{:S(2)}) copy-start(bf16[256,128]{1,0:T(8,128)(2,1)} %wv.1) | copy-start | bytes 196612
  1.9 51.9 %copy-start.5 = (bf16[256,128]{1,0:T(8,128)(2,1)S(1)}, bf16[256,128]{1,0:T(8,128)(2,1)}, u32[]{:S(2)}) copy-start(bf16[256,128]{1,0:T(8,128)(2,1)} %wo.1) | copy-start | bytes 196612
  53.8 20.1 %copy-start.3 = (f32[8,1,64,128]{3,2,1,0:T(8,128)S(1)}, f32[8,1,64,128]{3,2,1,0:T(8,128)}, u32[]{:S(2)}) copy-start(f32[8,1,64,128]{3,2,1,0:T(8,128)} %param.27) | copy-start | bytes 786436
  75.8 56.2 %copy-start.1 = (bf16[256,1024]{1,0:T(8,128)(2,1)S(1)}, bf16[256,1024]{1,0:T(8,128)(2,1)}, u32[]{:S(2)}) copy-start(bf16[256,1024]{1,0:T(8,128)(2,1)} %w_up.3) | copy-start | bytes 1572868
  94.8 13.2 %all-to-all-start.3 = ((bf16[16,16,128]{2,1,0:T(8,128)(2,1)}), bf16[16,16,128]{2,1,0:T(8,128)(2,1)S(1)}, u32[]{:S(2)}, u32[]{:S(2)}) async-start(bf16[16,16,128]{2,1,0:T(8,128)(2,1)} %bitcast.14), calls=%async_computation.3 | async-start | bytes 131072 | tf_op jit(solution)/shard_map/all_to_all | solution.py:19
  100.1 9.1 %collective-permute-start.1 = (bf16[512,256]{1,0:T(8,128)(2,1)S(1)}, bf16[512,256]{1,0:T(8,128)(2,1)S(1)}, u32[]{:S(2)}, u32[]{:S(2)}) collective-permute-start(bf16[512,256]{1,0:T(8,128)(2,1)S(1)} %get-tuple-element.30), channel_id=1, source_target_pairs={{0,16},{16,0},{1,17},{17,1},{2,18},{18,2},{3,19},{19,3},{4,20},{20... | collective-permute-start | bytes 786440 | tf_op jit(solution)/shard_map/ppermute | solution.py:365
  102.6 12.4 %collective-permute-start = (bf16[264,512]{1,0:T(8,128)(2,1)S(1)}, bf16[264,512]{1,0:T(8,128)(2,1)S(1)}, u32[]{:S(2)}, u32[]{:S(2)}) collective-permute-start(bf16[264,512]{1,0:T(8,128)(2,1)S(1)} %get-tuple-element.29), channel_id=1, source_target_pairs={{0,16},{16,0},{1,17},{17,1},{2,18},{18,2},{3,19},{19,3},{4,20},{20... | collective-permute-start | bytes 811016 | tf_op jit(solution)/shard_map/ppermute | solution.py:364
  132.3 34.5 %copy-start.2 = (bf16[1024,256]{1,0:T(8,128)(2,1)S(1)}, bf16[1024,256]{1,0:T(8,128)(2,1)}, u32[]{:S(2)}) copy-start(bf16[1024,256]{1,0:T(8,128)(2,1)} %w_down.3) | copy-start | bytes 1572868
